TPU v7x, 128 devices: a whole 4x4x4 slice. The times are simulated.
128 devices in a mesh: st: 16 (over z, x), tp: 8 (over y, core).
Axes of the slice: x: 4, y: 4, z: 4, core: 2. Of those that a mesh axis runs over, the one named last changes fastest.
Arguments:
- tokens: bfloat16 [32768, 2048], P('st', 'tp'), may hold values from -48 to 48
- store: bfloat16 [512, 64, 2048], P('st'), may hold values from -48 to 48
- passage_holder_index: int32 [256, 2], P('st'), may hold values from 0 to 15, all different within a row; in each aligned block of 16 rows (0 to 15, 16 to 31, ...) at most 4 rows name the same one
- passage_slot: int32 [256, 2], P('st'), may hold values from 0 to 31
- query_weight: bfloat16 [2048, 1024], P(None, 'tp'), may hold values from -0.125 to 0.125
- key_matrix: bfloat16 [2048, 1024], P(None, 'tp'), may hold values from -0.125 to 0.125
- value_weight: bfloat16 [2048, 1024], P(None, 'tp'), may hold values from -0.125 to 0.125
- outer_gate: bfloat16 [2048, 1024], P(None, 'tp'), may hold values from -0.125 to 0.125
- inner_gate: bfloat16 [2048, 1024], P(None, 'tp'), may hold values from -0.125 to 0.125
- conv_input: bfloat16 [2048, 1024], P(None, 'tp'), may hold values from -0.125 to 0.125
- conv_taps: bfloat16 [3, 1024], P(None, 'tp'), may hold values from -3.5 to 3.5
- route_gate_projection: bfloat16 [2048, 2], replicated, may hold values from -0.125 to 0.125
- conv_out: bfloat16 [1024, 2048], P('tp'), may hold values from -0.1875 to 0.1875
- memory_out: bfloat16 [1024, 2048], P('tp'), may hold values from -0.1875 to 0.1875
Outputs:
- mixed: bfloat16 [32768, 2048], P(('st', 'tp'))
Inputs may be any that keep to these rules, and one draw needn't show every extreme that they name: `passage_holder_index`: each row names 2 different owners; among the rows of one index of st (16 aligned rows) no owner is named more than 4 times, a bound that some index of st reaches.
All inputs are finite; a program needn't handle non-finite values.
Results may differ from a plain program's by a relative error of at most 0.014.
Values may be sent and summed in bfloat16 or wider, within the bound.
No kernel may reach another device: no remote copies, remote signals or barrier semaphores. Data moves between devices by JAX's collectives and lax.ppermute only.
A program may use at most 128 MiB of HBM per device.

v0:
```python
import jax
import jax.numpy as jnp
from jax import lax
from jax.sharding import PartitionSpec as P

HEAD_SIZE = 128
CONV_K = 3
SEQ_LEN = 256
BLOCK = 128
NPB = 2
PLEN = 64


def local(
    tokens,
    store,
    passage_holder_index,
    passage_slot,
    query_weight,
    key_matrix,
    value_weight,
    outer_gate,
    inner_gate,
    conv_input,
    conv_taps,
    route_gate_projection,
    conv_out,
    memory_out,
):
    row_count = tokens.shape[0]
    head_width = query_weight.shape[1]
    local_heads = head_width // HEAD_SIZE
    conv_cols = outer_gate.shape[1]
    local_weight = jnp.concatenate([query_weight, outer_gate, inner_gate, conv_input], axis=1)
    pieces = lax.all_gather(tokens, "tp", axis=1, tiled=True)
    projected = jnp.dot(pieces, local_weight, preferred_element_type=jnp.float32)
    gate_logits = jnp.dot(pieces, route_gate_projection, preferred_element_type=jnp.float32)
    queries = projected[:, :head_width].astype(jnp.bfloat16)
    outer_part = projected[:, head_width : head_width + conv_cols]
    inner_part = projected[:, head_width + conv_cols : head_width + 2 * conv_cols]
    value_part = projected[:, head_width + 2 * conv_cols :]
    branch_mix = jax.nn.sigmoid(gate_logits)
    seq_count = row_count // SEQ_LEN
    mixed_input = (inner_part * value_part).reshape(seq_count, SEQ_LEN, conv_cols)
    padded_input = jnp.pad(mixed_input, ((0, 0), (CONV_K - 1, 0), (0, 0)))
    tap_values = conv_taps.astype(jnp.float32)
    filtered_signal = tap_values[0] * padded_input[:, 0:SEQ_LEN]
    for offset in range(1, CONV_K):
        filtered_signal = (
            filtered_signal + tap_values[offset] * padded_input[:, offset : offset + SEQ_LEN]
        )
    conv_branch = (outer_part * filtered_signal.reshape(row_count, conv_cols)).astype(jnp.bfloat16)
    owners = passage_holder_index.reshape(-1)
    local_slots = passage_slot.reshape(-1)
    block_count = passage_holder_index.shape[0]
    owner_count = lax.axis_size("st")
    request_count = owners.shape[0]
    capacity = max(2, 2 * request_count // owner_count)
    one_hot = (owners[:, None] == jnp.arange(owner_count, dtype=jnp.int32)[None, :]).astype(
        jnp.int32
    )
    before = jnp.cumsum(one_hot, axis=0) - one_hot
    position = jnp.sum(before * one_hot, axis=1)
    target = owners * capacity + position
    matches = (
        target[:, None] == jnp.arange(owner_count * capacity, dtype=jnp.int32)[None, :]
    ).astype(jnp.int32)
    outgoing = jnp.sum(matches * local_slots[:, None], axis=0).reshape(owner_count, capacity)
    wanted = lax.all_to_all(outgoing, "st", split_axis=0, concat_axis=0, tiled=True)
    flat_rows = store.reshape(-1, store.shape[-1])
    key_part = jnp.dot(flat_rows, key_matrix, preferred_element_type=jnp.float32).astype(
        jnp.bfloat16
    )
    retrieved_content_vectors = jnp.dot(
        flat_rows, value_weight, preferred_element_type=jnp.float32
    ).astype(jnp.bfloat16)
    joined = jnp.concatenate([key_part, retrieved_content_vectors], axis=1)
    table = joined.reshape(store.shape[:-1] + (2 * head_width,))
    chosen = table[wanted.reshape(-1)].reshape(wanted.shape + table.shape[1:])
    served = lax.all_to_all(chosen, "st", split_axis=0, concat_axis=0, tiled=True)
    slot_table = served.reshape(owner_count * capacity, PLEN, 2 * head_width)
    picked = slot_table[target].reshape(block_count, NPB * PLEN, 2 * head_width)
    passage_key_rows = picked[:, :, :head_width].reshape(
        block_count, NPB * PLEN, local_heads, HEAD_SIZE
    )
    retrieved_content_vectors = picked[:, :, head_width:].reshape(
        block_count, NPB * PLEN, local_heads, HEAD_SIZE
    )
    query_block_rows = queries.reshape(block_count, BLOCK, local_heads, HEAD_SIZE)
    scores = jnp.einsum(
        "xuhd,xkhd->xhuk", query_block_rows, passage_key_rows, preferred_element_type=jnp.float32
    ) * HEAD_SIZE ** (-0.5)
    softmax_shares = jax.nn.softmax(scores, axis=-1).astype(jnp.bfloat16)
    memory_branch = jnp.einsum(
        "xhuk,xkhd->xuhd",
        softmax_shares,
        retrieved_content_vectors,
        preferred_element_type=jnp.float32,
    )
    memory_branch = memory_branch.reshape(row_count, head_width).astype(jnp.bfloat16)
    return lax.psum_scatter(
        (
            branch_mix[:, 0:1] * jnp.dot(conv_branch, conv_out, preferred_element_type=jnp.float32)
            + branch_mix[:, 1:2]
            * jnp.dot(memory_branch, memory_out, preferred_element_type=jnp.float32)
        ).astype(jnp.bfloat16),
        "tp",
        scatter_dimension=0,
        tiled=True,
    )


def solution(mesh):
    return jax.shard_map(
        local,
        mesh=mesh,
        in_specs=(
            P("st", "tp"),
            P("st", None, None),
            P("st", None),
            P("st", None),
            P(None, "tp"),
            P(None, "tp"),
            P(None, "tp"),
            P(None, "tp"),
            P(None, "tp"),
            P(None, "tp"),
            P(None, "tp"),
            P(),
            P("tp", None),
            P("tp", None),
        ),
        out_specs=P(("st", "tp"), None),
        check_vma=False,
    )
```

profile of v0, /device:TPU:1, one launch (start us, length us, event | category | flops | bytes accessed | tf_op | source)
XLA Modules:
  0.0 160.1 jit_solution(17596449766068690858)
XLA Ops:
  6.5 0.7 all-gather.2.cloned.1.call-update
  7.3 0.8 copy.35
  8.0 0.1 mul.118
  8.1 0.8 copy.34
  8.9 0.1 reshape.135
  9.0 0.1 fusion.23
  9.0 0.1 reduce_window_sum.11
  9.1 0.2 select_reduce_fusion.1
  9.3 0.1 select_reduce_fusion
  9.4 0.7 all_to_all.9
  10.1 8.4 %all-to-all-start = ((s32[16,1,4]{2,1,0:T(1,128)}), s32[16,1,4]{2,1,0:T(1,128)S(1)}, u32[]{:S(2)}, u32[]{:S(2)}) async-start(s32[16,1,4]{2,1,0:T(1,128)} %bitcast.8), calls=%async_computation | async-start | bytes 16384 | tf_op jit(solution)/shard_map/all_to_all | solution.py:69
  18.5 0.0 copy-start.1
  18.5 0.0 copy-start.5
  18.5 6.8 %convolution_convert_fusion = bf16[2048,128]{0,1:T(8,128)(2,1)S(1)} fusion(bf16[2048,2048]{1,0:T(8,128)(2,1)} %bitcast.51, bf16[2048,128]{1,0:T(8,128)(2,1)} %param.20), kind=kOutput, calls=%fused_computation.5 | convolution fusion | flops 1074003968 | bytes 9437184 | tf_op jit(solution)/shard_map/dot_general | solution.py:74
  25.4 0.2 copy-done.1
  25.6 0.1 copy-done.5
  25.6 2.9 %convolution_convert_fusion.1 = bf16[2048,128]{0,1:T(8,128)(2,1)S(1)} fusion(bf16[2048,2048]{1,0:T(8,128)(2,1)S(1)} %bitcast.52, bf16[2048,128]{1,0:T(8,128)(2,1)S(1)} %copy-done.5), kind=kOutput, calls=%fused_computation.6 | convolution fusion | flops 1074003968 | bytes 9437184 | tf_op jit(solution)/shard_map/dot_general | solution.py:71
  28.5 0.1 pad_maximum_fusion
  28.7 0.5 copy.33
  29.2 0.5 broadcast.75
  29.7 0.7 reduce.7
  30.4 0.1 reshape.136
  30.5 0.0 copy-start.8
  30.5 0.0 copy-start.7
  30.5 2.1 %gather_fusion = bf16[64,64,256]{2,1,0:T(8,128)(2,1)} fusion(bf16[32,64,256]{2,1,0:T(8,128)(2,1)S(1)} %bitcast.53, s32[1024]{0:T(1024)S(1)} %pad_clamp_fusion.1), kind=kCustom, calls=%fused_computation | custom fusion | bytes 4194560 | tf_op jit(solution)/shard_map/gather | solution.py:79
  32.6 6.8 %all-to-all-start.1 = ((bf16[16,4,64,256]{3,2,1,0:T(8,128)(2,1)}), bf16[16,4,64,256]{3,2,1,0:T(8,128)(2,1)S(1)}, u32[]{:S(2)}, u32[]{:S(2)}) async-start(bf16[16,4,64,256]{3,2,1,0:T(8,128)(2,1)} %bitcast.54), calls=%async_computation.1 | async-start | bytes 4194304 | tf_op jit(solution)/shard_map/all_to_all | solution.py:80
  39.4 0.2 reduce-scatter.2.cloned.1.call-start
  39.6 0.1 copy.37
  39.7 0.1 mul.123
  39.9 28.3 %all-to-all-done.1 = bf16[16,4,64,256]{3,2,1,0:T(8,128)(2,1)S(1)} async-done(((bf16[16,4,64,256]{3,2,1,0:T(8,128)(2,1)}), bf16[16,4,64,256]{3,2,1,0:T(8,128)(2,1)S(1)}, u32[]{:S(2)}, u32[]{:S(2)}) %all-to-all-start.1) | async-done | bytes 2097184 | tf_op jit(solution)/shard_map/all_to_all | solution.py:80
  68.2 1.6 gather_fusion.1
  69.8 7.6 %convolution_bitcast_fusion = f32[2048,512]{0,1:T(8,128)S(1)} fusion(bf16[2048,2048]{1,0:T(8,128)(2,1)} %all-gather.2.cloned.1.call-done, bf16[2048,128]{1,0:T(8,128)(2,1)S(1)} %copy-done.9, bf16[2048,128]{1,0:T(8,128)(2,1)} %param.22, bf16[2048,128]{1,0:T(8,128)(2,1)} %param.21, bf16[2048,128]{1,0:T(8,128)(2,1)} %param.18), kind=kOutput, calls=%fused_computation.4 | convolution fusion | flops 4303355904 | bytes 14680064 | tf_op jit(solution)/shard_map/dot_general | solution.py:36
  77.4 2.0 %copy-done.2 = f32[2048,512]{0,1:T(8,128)} copy-done((f32[2048,512]{0,1:T(8,128)}, f32[2048,512]{0,1:T(8,128)S(1)}, u32[]{:S(2)}) %copy-start.2) | copy-done | bytes 4194328
  79.3 0.1 slice.94
  79.4 0.0 copy-start.6
  79.4 0.3 copy.41
  79.7 0.5 fusion.32
  80.2 1.4 convolution_multiply_fusion
  81.7 1.7 %slice_multiply_fusion = f32[2048,128]{0,1:T(8,128)S(1)} fusion(f32[2048,512]{0,1:T(8,128)} %copy-done.2), kind=kLoop, calls=%fused_computation.29 | loop fusion | flops 262144 | bytes 3145728 | tf_op jit(solution)/shard_map/mul | solution.py:44
  83.4 5.7 %fusion.3 = f32[2048,2]{0,1:T(2,128)S(1)} fusion(bf16[2048,2048]{1,0:T(8,128)(2,1)} %all-gather.2.cloned.1.call-done, bf16[2048,2]{0,1:T(2,128)(2,1)S(1)} %copy-done.6), kind=kOutput, calls=%fused_computation.10 | convolution fusion | flops 16789504 | bytes 8413184 | tf_op jit(solution)/shard_map/dot_general | solution.py:37
  89.1 0.3 copy.42
  89.4 1.0 fusion.15
  90.4 0.3 copy.43
  90.8 2.0 %convolution_convert_fusion.2 = bf16[16,128,128]{1,2,0:T(8,128)(2,1)S(1)} fusion(bf16[16,128,256]{2,1,0:T(8,128)(2,1)S(1)} %bitcast.62, f32[16,128]{1,0:T(8,128)S(1)} %fusion.32, f32[16,128,128]{1,2,0:T(8,128)} %convolution_multiply_fusion), kind=kOutput, calls=%fused_computation.23 | convolution fusion | flops 68159616 | bytes 3153920 | tf_op jit(solution)/shard_map/xhuk,xkhd->xuhd/dot_general | solution.py:94
  92.8 3.7 %fusion.18 = f32[2048,2048]{1,0:T(8,128)S(1)} fusion(bf16[128,2048]{1,0:T(8,128)(2,1)S(1)} %copy-done, f32[2048,128]{0,1:T(8,128)S(1)} %bitcast.55, f32[2048,512]{0,1:T(8,128)} %copy-done.2), kind=kOutput, calls=%fused_computation.34 | convolution fusion | flops 1074266112 | bytes 19398656 | tf_op jit(solution)/shard_map/dot_general | solution.py:103
  96.5 4.7 %add_convert_fusion = bf16[2048,2048]{1,0:T(8,128)(2,1)} fusion(f32[2048,2048]{1,0:T(8,128)S(1)} %fusion.18, bf16[2048,128]{1,0:T(8,128)(2,1)S(1)} %bitcast.65, bf16[128,2048]{1,0:T(8,128)(2,1)S(1)} %copy-done.4, f32[2048]{0:T(1024)S(1)} %bitcast.67, f32[2048]{0:T(1024)S(1)} %bitcast.66), kind=kOutput, calls=%fused_computation.3 | convolution fusion | flops 1090519040 | bytes 26230784 | tf_op jit(solution)/shard_map/dot_general | solution.py:105
  101.1 0.0 reduce-scatter.2.cloned.1.call-update
  101.2 52.1 %reduce-scatter.2.cloned.1.call-done = bf16[256,2048]{1,0:T(8,128)(2,1)} async-done(((bf16[2048,2048]{1,0:T(8,128)(2,1)}), bf16[256,2048]{1,0:T(8,128)(2,1)}) %reduce-scatter.2.cloned.1.call-update) | async-done | bytes 1048592 | tf_op jit(solution)/shard_map/reduce_scatter | solution.py:101
  (24 shorter events, 0.1 us)
Async XLA Ops:
  6.5 86.3 %copy-start = (bf16[128,2048]{1,0:T(8,128)(2,1)S(1)}, bf16[128,2048]{1,0:T(8,128)(2,1)}, u32[]{:S(2)}) copy-start(bf16[128,2048]{1,0:T(8,128)(2,1)} %param.26) | copy-start | bytes 1572868
  6.5 63.2 %all-gather.2.cloned.1.call-start = ((), (), s32[]{:S(2)}) async-start(), calls=%async_computation.3 | async-start | bytes 9437184 | tf_op jit(solution)/shard_map/all_gather | solution.py:35
  10.1 19.1 %all-to-all-start = ((s32[16,1,4]{2,1,0:T(1,128)}), s32[16,1,4]{2,1,0:T(1,128)S(1)}, u32[]{:S(2)}, u32[]{:S(2)}) async-start(s32[16,1,4]{2,1,0:T(1,128)} %bitcast.8), calls=%async_computation | async-start | bytes 16384 | tf_op jit(solution)/shard_map/all_to_all | solution.py:69
  18.5 7.1 %copy-start.1 = (bf16[32,64,2048]{2,1,0:T(8,128)(2,1)S(1)}, bf16[32,64,2048]{2,1,0:T(8,128)(2,1)}, u32[]{:S(2)}) copy-start(bf16[32,64,2048]{2,1,0:T(8,128)(2,1)} %param.15) | copy-start | bytes 25165828
  18.5 7.1 %copy-start.5 = (bf16[2048,128]{1,0:T(8,128)(2,1)S(1)}, bf16[2048,128]{1,0:T(8,128)(2,1)}, u32[]{:S(2)}) copy-start(bf16[2048,128]{1,0:T(8,128)(2,1)} %param.19) | copy-start | bytes 1572868
  30.5 9.1 %copy-start.8 = (bf16[3,128]{1,0:T(4,128)(2,1)S(1)}, bf16[3,128]{1,0:T(4,128)(2,1)}, u32[]{:S(2)}) copy-start(bf16[3,128]{1,0:T(4,128)(2,1)} %param.24) | copy-start | bytes 2308
  30.5 9.1 %copy-start.7 = (s32[16,2]{0,1:T(2,128)S(1)}, s32[16,2]{0,1:T(2,128)}, u32[]{:S(2)}) copy-start(s32[16,2]{0,1:T(2,128)} %param.16) | copy-start | bytes 388
  32.6 37.2 %copy-start.9 = (bf16[2048,128]{1,0:T(8,128)(2,1)S(1)}, bf16[2048,128]{1,0:T(8,128)(2,1)}, u32[]{:S(2)}) copy-start(bf16[2048,128]{1,0:T(8,128)(2,1)} %param.23) | copy-start | bytes 1572868
  32.6 35.6 %all-to-all-start.1 = ((bf16[16,4,64,256]{3,2,1,0:T(8,128)(2,1)}), bf16[16,4,64,256]{3,2,1,0:T(8,128)(2,1)S(1)}, u32[]{:S(2)}, u32[]{:S(2)}) async-start(bf16[16,4,64,256]{3,2,1,0:T(8,128)(2,1)} %bitcast.54), calls=%async_computation.1 | async-start | bytes 4194304 | tf_op jit(solution)/shard_map/all_to_all | solution.py:80
  39.4 113.9 %reduce-scatter.2.cloned.1.call-start = ((), (), s32[]{:S(2)}) async-start(), calls=%async_computation.4 | async-start | bytes 9437184 | tf_op jit(solution)/shard_map/reduce_scatter | solution.py:101
  69.8 9.9 %copy-start.3 = (bf16[32,64,256]{2,1,0:T(8,128)(2,1)S(1)}, bf16[32,64,256]{2,1,0:T(8,128)(2,1)}, u32[]{:S(2)}) copy-start(bf16[32,64,256]{2,1,0:T(8,128)(2,1)} %gather_fusion.1) | copy-start | bytes 3145732
  77.4 2.0 %copy-start.2 = (f32[2048,512]{0,1:T(8,128)}, f32[2048,512]{0,1:T(8,128)S(1)}, u32[]{:S(2)}) copy-start(f32[2048,512]{0,1:T(8,128)S(1)} %convolution_bitcast_fusion) | copy-start | bytes 12582916
  79.4 4.0 %copy-start.6 = (bf16[2048,2]{0,1:T(2,128)(2,1)S(1)}, bf16[2048,2]{0,1:T(2,128)(2,1)}, u32[]{:S(2)}) copy-start(bf16[2048,2]{0,1:T(2,128)(2,1)} %param.25) | copy-start | bytes 24580
  92.8 3.7 %copy-start.4 = (bf16[128,2048]{1,0:T(8,128)(2,1)S(1)}, bf16[128,2048]{1,0:T(8,128)(2,1)}, u32[]{:S(2)}) copy-start(bf16[128,2048]{1,0:T(8,128)(2,1)} %param.27) | copy-start | bytes 1572868
Sparse Core Ops, SparseCore 0:
  9.0 57.0 all-gather.1
  101.3 51.9 reduce-scatter.1
where the time goes:
time: 160 us
  waiting for transfers between devices  81.2 us (51%)
  matrix products  35.3 us (22%)
  starting transfers between devices  15.4 us (10%)
  between operations  13.7 us (9%)
  local copies, waits for them, and re-layouts  10.7 us (7%)
  other arithmetic  3.89 us (2%)
    reduce_scatter x1, waiting for transfers between devices, local(): lax.psum_scatter((branch_mix[:, 0:1] * jnp.dot(conv_branch, conv_out, pre...  52.1 us
    all_to_all x1, waiting for transfers between devices, local(): lax.all_to_all(chosen, 'st', split_axis=0, concat_axis=0, tiled=True)  28.3 us
    all_to_all x1, starting transfers between devices, local(): lax.all_to_all(outgoing, 'st', split_axis=0, concat_axis=0, tiled=True)  8.42 us
    dot_general x1, matrix products, local(): jnp.dot(pieces, local_weight, preferred_element_type=jnp.float32)  7.57 us
    dot_general x1, matrix products, local(): jnp.dot(flat_rows, value_weight, preferred_element_type=jnp.float32)  6.83 us
    all_to_all x1, starting transfers between devices, local(): lax.all_to_all(chosen, 'st', split_axis=0, concat_axis=0, tiled=True)  6.77 us
    dot_general x1, matrix products, local(): jnp.dot(pieces, route_gate_projection, preferred_element_type=jnp.float32)  5.66 us
    dot_general x1, matrix products, local(): jnp.dot(memory_branch, memory_out, preferred_element_type=jnp.float32)  4.67 us
  transfers between devices with their start and end apart: 4, of which 2 were waited for; matrix products, arithmetic and copies ran while one was open for 11% of the time, Pallas kernels for 0%

commit v1 on v0

v1 whole, which is shorter than its diff:
```python
import jax
import jax.numpy as jnp
from jax import lax
from jax.experimental import pallas as pl
from jax.experimental.pallas import tpu as pltpu
from jax.sharding import PartitionSpec as P

HEAD_SIZE = 128
SEQ_LEN = 256
BLOCK = 128
PLEN = 64
N_Y = 4
N_X = 4
N_Z = 4
BF = jnp.bfloat16
F32 = jnp.float32


SHIFT = {
    s: [(2 * y + c, 2 * ((y + s) % N_Y) + c) for y in range(N_Y) for c in range(2)]
    for s in (1, -1, 2)
}
SWAP = [(2 * y + c, 2 * y + 1 - c) for y in range(N_Y) for c in range(2)]


def plane_shift(s):
    pairs = []
    for z in range(N_Z):
        for x in range(N_X):
            for y in range(N_Y):
                for c in range(2):
                    z2, x2 = (z, (x + s) % N_X) if c == 0 else ((z + s) % N_Z, x)
                    pairs.append(((z * N_X + x) * 8 + 2 * y + c, (z2 * N_X + x2) * 8 + 2 * y + c))
    return pairs


def shift(a, s):
    return lax.ppermute(a, "tp", SHIFT[s])


def swap(a):
    return lax.ppermute(a, "tp", SWAP)


def plane(a, s):
    return lax.ppermute(a, ("st", "tp"), plane_shift(s))


def pick(a, index, axis=0):
    return lax.dynamic_index_in_dim(a, index, axis, keepdims=False)


def dot(a, b):
    return jnp.dot(a, b, preferred_element_type=F32)


def project_kernel(sc, *refs):
    pieces = refs[:8]
    wm, wo, gate, tm, to = refs[8:13]
    q_ref = refs[13]
    conv_refs = refs[14:18]
    logit_ref = refs[18]
    j = pl.program_id(0)
    acc_m = acc_o = None
    for k in range(8):
        row = pl.ds(pl.multiple_of(sc[k] * 256, 256), 256)
        x = pieces[k][...]
        am, ao = dot(x, wm[row, :]), dot(x, wo[row, :])
        acc_m = am if acc_m is None else acc_m + am
        acc_o = ao if acc_o is None else acc_o + ao
    H = HEAD_SIZE
    q_ref[:, :H] = acc_m[:, :H].astype(BF)
    q_ref[:, H:] = acc_o[:, :H].astype(BF)
    ids = lax.broadcasted_iota(jnp.int32, (SEQ_LEN, H), 0)

    def conv(acc, taps):
        t = taps[...].astype(F32)
        prod = acc[:, 2 * H : 3 * H] * acc[:, 3 * H :]
        back1 = jnp.where(ids >= 1, pltpu.roll(prod, 1, 0), 0.0)
        back2 = jnp.where(ids >= 2, pltpu.roll(prod, 2, 0), 0.0)
        filtered = t[0:1] * back2 + t[1:2] * back1 + t[2:3] * prod
        return (acc[:, H : 2 * H] * filtered).astype(BF)

    cm, co = conv(acc_m, tm), conv(acc_o, to)
    for i in range(4):

        @pl.when(j == i)
        def _(i=i):
            conv_refs[i][:, :H] = cm
            conv_refs[i][:, H:] = co

    @pl.when(j == 3)
    def _():
        acc = None
        for k in range(8):
            row = pl.ds(pl.multiple_of(sc[k] * 256, 256), 256)
            a = dot(pieces[k][...], gate[row, :])
            acc = a if acc is None else acc + a
        logit_ref[...] = acc


def project(sc, pieces, wm, wo, gate, tm, to):
    rows = pieces[0].shape[0]
    whole = lambda a: pl.BlockSpec(a.shape, lambda j, s: (0, 0))
    tile = pl.BlockSpec((SEQ_LEN, 256), lambda j, s: (s[8 + j], 0))
    fixed = lambda n: pl.BlockSpec((SEQ_LEN, n), lambda j, s: (0, 0))
    return pl.pallas_call(
        project_kernel,
        grid_spec=pltpu.PrefetchScalarGridSpec(
            num_scalar_prefetch=1,
            grid=(4,),
            in_specs=[tile] * 8 + [whole(a) for a in (wm, wo, gate, tm, to)],
            out_specs=[tile] + [fixed(256)] * 4 + [fixed(128)],
        ),
        out_shape=[jax.ShapeDtypeStruct((rows, 256), BF)]
        + [jax.ShapeDtypeStruct((SEQ_LEN, 256), BF)] * 4
        + [jax.ShapeDtypeStruct((SEQ_LEN, 128), F32)],
        compiler_params=pltpu.CompilerParams(vmem_limit_bytes=40 * 2**20),
        cost_estimate=pl.CostEstimate(
            flops=2 * rows * 2048 * 1024, bytes_accessed=9 * 2**20, transcendentals=0
        ),
        name="project",
    )(sc, *pieces, wm, wo, gate, tm, to)


def attend_kernel(sc, q, tab_m, tab_o, *outs):
    H = HEAD_SIZE
    for j in range(4):
        for half in range(2):
            b = sc[16 + j] * 2 + half
            t0, t1 = sc[2 * b], sc[2 * b + 1]
            rows = pl.ds(pl.multiple_of(b * BLOCK, BLOCK), BLOCK)
            for h, tab in enumerate((tab_m, tab_o)):
                kv = jnp.concatenate([tab[t0], tab[t1]], axis=0)
                qb = q[rows, h * H : (h + 1) * H]
                s = lax.dot_general(
                    qb, kv[:, :H], (((1,), (1,)), ((), ())), preferred_element_type=F32
                ) * (H**-0.5)
                e = jnp.exp(s - jnp.max(s, axis=-1, keepdims=True))
                p = (e / jnp.sum(e, axis=-1, keepdims=True)).astype(BF)
                o = dot(p, kv[:, H:])
                outs[j][half * BLOCK : (half + 1) * BLOCK, h * H : (h + 1) * H] = o.astype(BF)


def attend(sc, q, tab_m, tab_o):
    whole = lambda a: pl.BlockSpec(a.shape, lambda i, s, n=a.ndim: (0,) * n)
    return pl.pallas_call(
        attend_kernel,
        grid_spec=pltpu.PrefetchScalarGridSpec(
            num_scalar_prefetch=1,
            grid=(1,),
            in_specs=[whole(q), whole(tab_m), whole(tab_o)],
            out_specs=[pl.BlockSpec((SEQ_LEN, 256), lambda i, s: (0, 0))] * 4,
        ),
        out_shape=[jax.ShapeDtypeStruct((SEQ_LEN, 256), BF)] * 4,
        compiler_params=pltpu.CompilerParams(vmem_limit_bytes=40 * 2**20),
        cost_estimate=pl.CostEstimate(
            flops=3 * 10**9, bytes_accessed=5 * 2**20, transcendentals=2**18
        ),
        name="attend",
    )(sc, q, tab_m, tab_o)


def finish_kernel(sc, *refs):
    sides = (refs[0:5], refs[5:10])
    convs, mems, logits = refs[10:14], refs[14:18], refs[18]
    out = refs[19]
    w, sems = refs[20], refs[21]
    copies = []
    n = 0
    for side in range(2):
        own, e, r1, r2, r3 = sides[side]
        base = side * 128
        for branch in range(2):
            copies.append(
                pltpu.make_async_copy(
                    own.at[pl.ds(branch * 128, 128)],
                    w.at[0, branch, pl.ds(base, 128)],
                    sems.at[n],
                )
            )
            n += 1
        for src, back in ((e, 0), (r1, 3), (r2, 1), (r3, 2)):
            quarter = lax.rem(sc[side] + back, 4)
            branch = lax.div(quarter, 2)
            row = pl.multiple_of(base + lax.rem(quarter, 2) * 64, 64)
            for d in range(3):
                copies.append(
                    pltpu.make_async_copy(
                        src.at[pl.ds(d * 64, 64)],
                        w.at[1 + d, branch, pl.ds(row, 64)],
                        sems.at[n],
                    )
                )
                n += 1
    for c in copies:
        c.start()
    mix = jax.nn.sigmoid(logits[...])
    m0, m1 = mix[:, 0:1], mix[:, 1:2]
    for c in copies:
        c.wait()

    def step(i, carry):
        cols = pl.ds(pl.multiple_of(i * 512, 512), 512)
        a0 = a1 = None
        for d in range(4):
            x0 = dot(convs[d][...], w[d, 0, :, cols])
            x1 = dot(mems[d][...], w[d, 1, :, cols])
            a0 = x0 if a0 is None else a0 + x0
            a1 = x1 if a1 is None else a1 + x1
        out[:, cols] = (m0 * a0 + m1 * a1).astype(BF)
        return carry

    lax.fori_loop(0, 4, step, 0)


def finish(sc, mine, other, convs, mems, logits):
    width = mine[0].shape[1]
    hbm = pl.BlockSpec(memory_space=pl.ANY)
    whole = lambda a: pl.BlockSpec(a.shape, lambda i, s: (0, 0))
    vm = list(convs) + list(mems) + [logits]
    return pl.pallas_call(
        finish_kernel,
        grid_spec=pltpu.PrefetchScalarGridSpec(
            num_scalar_prefetch=1,
            grid=(1,),
            in_specs=[hbm] * 10 + [whole(a) for a in vm],
            out_specs=pl.BlockSpec((SEQ_LEN, width), lambda i, s: (0, 0)),
            scratch_shapes=[
                pltpu.VMEM((4, 2, 256, width), BF),
                pltpu.SemaphoreType.DMA((28,)),
            ],
        ),
        out_shape=jax.ShapeDtypeStruct((SEQ_LEN, width), BF),
        compiler_params=pltpu.CompilerParams(vmem_limit_bytes=40 * 2**20),
        cost_estimate=pl.CostEstimate(
            flops=2 * SEQ_LEN * 2048 * 2048, bytes_accessed=10 * 2**20, transcendentals=0
        ),
        name="finish",
    )(sc, *mine, *other, *vm)


def local(
    tokens,
    store,
    passage_holder_index,
    passage_slot,
    query_weight,
    key_matrix,
    value_weight,
    outer_gate,
    inner_gate,
    conv_input,
    conv_taps,
    route_gate_projection,
    conv_out,
    memory_out,
):
    me = lax.axis_index("tp")
    st = lax.axis_index("st")
    y, c = me // 2, me % 2
    z, x = st // N_X, st % N_X
    D = query_weight.shape[0]
    KS = tokens.shape[1]
    HW = query_weight.shape[1]
    i32 = jnp.int32

    o_mine = jnp.concatenate([conv_out, memory_out], axis=0)
    quarter = jnp.where(c == 0, x, z)
    quarter_other = jnp.where(c == 0, z, x)
    part = pick(o_mine.reshape(4, 64, D), quarter)
    ys = [shift(part, s) for s in (1, -1, 2)]
    e = jnp.concatenate(ys, axis=0)
    r1, r2, r3 = plane(e, 1), plane(e, -1), plane(e, 2)
    w_own = [o_mine, e, r1, r2, r3]
    w_other = [swap(a) for a in w_own]

    owners = passage_holder_index.reshape(-1)
    local_slots = passage_slot.reshape(-1)
    owner_count = lax.axis_size("st")
    request_count = owners.shape[0]
    capacity = max(2, 2 * request_count // owner_count)
    one_hot = (owners[:, None] == jnp.arange(owner_count, dtype=i32)[None, :]).astype(i32)
    before = jnp.cumsum(one_hot, axis=0) - one_hot
    position = jnp.sum(before * one_hot, axis=1)
    target = owners * capacity + position
    matches = (target[:, None] == jnp.arange(owner_count * capacity, dtype=i32)[None, :]).astype(i32)
    outgoing = jnp.sum(matches * local_slots[:, None], axis=0).reshape(owner_count, capacity)
    wanted = lax.all_to_all(outgoing, "st", split_axis=0, concat_axis=0, tiled=True)

    rows = tokens.reshape(N_Y, 2, SEQ_LEN, KS)
    h0 = pick(rows, c, 1).reshape(N_Y * SEQ_LEN, KS)
    other = pick(rows, 1 - c, 1).reshape(N_Y * SEQ_LEN, KS)
    a0, b0 = shift(h0, 1), shift(h0, -1)
    h1 = swap(other)
    a1, b1 = shift(h1, 1), shift(h1, -1)
    c0, c1 = shift(a0, 1), shift(b1, -1)
    pieces = (h0, h1, a0, b0, a1, b1, c0, c1)

    def slice_of(dy, flip):
        return 2 * ((y + dy) % N_Y) + (1 - c if flip else c)

    flips = ((0, False), (0, True), (-1, False), (1, False), (-1, True), (1, True), (2, False), (2, True))
    yord = [(y + d) % N_Y for d in (2, 1, -1, 0)]
    sc_project = jnp.stack([slice_of(*f) for f in flips] + yord).astype(i32)

    flat_rows = store.reshape(-1, D)
    kv = dot(flat_rows, jnp.concatenate([key_matrix, value_weight], axis=1)).astype(BF)
    table = kv.reshape(store.shape[0], PLEN, 2 * HW)
    chosen = table[wanted.reshape(-1)].reshape(owner_count, capacity, PLEN, 2 * HW)
    served = lax.all_to_all(chosen, "st", split_axis=0, concat_axis=0, tiled=True)
    tab_m = served.reshape(owner_count * capacity, PLEN, 2 * HW)
    tab_o = swap(tab_m)
    mine = pick(target.reshape(N_Y, 2, -1), c, 1).reshape(-1)
    sc_attend = jnp.concatenate([mine, jnp.stack(yord)]).astype(i32)

    w_mine = jnp.concatenate([query_weight, outer_gate, inner_gate, conv_input], axis=1)
    w_part = swap(w_mine)
    taps_part = swap(conv_taps)
    gate = jnp.pad(route_gate_projection, ((0, 0), (0, HW - 2)))

    q, *convs, logits = project(sc_project, pieces, w_mine, w_part, gate, conv_taps, taps_part)
    conv_all = [convs[3], shift(convs[1], 1), shift(convs[2], -1), shift(convs[0], 2)]
    mems = attend(sc_attend, q, tab_m, tab_o)
    mem_all = [mems[3], shift(mems[1], 1), shift(mems[2], -1), shift(mems[0], 2)]
    return finish(
        jnp.stack([quarter, quarter_other]).astype(i32), w_own, w_other, conv_all, mem_all, logits
    )


def solution(mesh):
    return jax.shard_map(
        local,
        mesh=mesh,
        in_specs=(
            P("st", "tp"),
            P("st", None, None),
            P("st", None),
            P("st", None),
            P(None, "tp"),
            P(None, "tp"),
            P(None, "tp"),
            P(None, "tp"),
            P(None, "tp"),
            P(None, "tp"),
            P(None, "tp"),
            P(),
            P("tp", None),
            P("tp", None),
        ),
        out_specs=P(("st", "tp"), None),
        check_vma=False,
    )
```

time: 160 us -> 159 us (level); the launches traced: 160 us -> 157 us
  waiting for transfers between devices: 81.2 us -> 36.1 us
  starting transfers between devices: 15.4 us -> 54.8 us
  matrix products: 35.3 us -> 5.77 us
  Pallas kernels: 0 us -> 25 us
  local copies, waits for them, and re-layouts: 10.7 us -> 33.5 us
  between operations: 13.7 us -> 0.55 us
  other arithmetic: 3.89 us -> 1.19 us
    reduce_scatter x1 -> x0, waiting for transfers between devices: 52.1 us -> none  [local(): lax.psum_scatter((branch_mix[:, 0:1] * jnp.dot(conv_branch, conv_out, pre...]
    ppermute x0 -> x27, starting transfers between devices: none -> 39.8 us  [the longest x15 21.5 us: shift(): return lax.ppermute(a, 'tp', SHIFT[s])]
    ppermute x0 -> x27, waiting for transfers between devices: none -> 36.1 us  [the longest x15 31 us: shift(): return lax.ppermute(a, 'tp', SHIFT[s])]
    dot_general x8 -> x1, matrix products: 34.7 us -> 5.77 us  [dot(): return jnp.dot(a, b, preferred_element_type=F32)]
    all_to_all x1, waiting for transfers between devices: 28.3 us -> 0.01 us  [local(): lax.all_to_all(chosen, 'st', split_axis=0, concat_axis=0, tiled=True)]
    pallas_call x0 -> x3, Pallas kernels: none -> 25 us  [the longest x1 9.5 us: project(): pl.pallas_call(project_kernel, grid_spec=pltpu.PrefetchScalarGridSpec(num...]
    unnamed x24 -> x57, local copies, waits for them, and re-layouts: 4.49 us -> 22 us
    concatenate x1 -> x4, local copies, waits for them, and re-layouts: 0.52 us -> 3.72 us  [the longest x1 1.67 us: local(): e = jnp.concatenate(ys, axis=0)]
  transfers between devices with their start and end apart: 4 -> 29, of which waited for: 2 -> 8; matrix products, arithmetic and copies ran while one was open for 11% -> 14% of each run, Pallas kernels for 0% -> 11%
where the time goes in v1:
time: 159 us; the launch traced here: 157 us
  starting transfers between devices  54.8 us (34%)
  waiting for transfers between devices  36.1 us (23%)
  local copies, waits for them, and re-layouts  33.5 us (21%)
  Pallas kernels  25 us (16%)
  matrix products  5.77 us (4%)
    ppermute x15, waiting for transfers between devices, shift(): return lax.ppermute(a, 'tp', SHIFT[s])  31 us
    unnamed x57, local copies, waits for them, and re-layouts  22 us
    ppermute x15, starting transfers between devices, shift(): return lax.ppermute(a, 'tp', SHIFT[s])  21.5 us
    ppermute x9, starting transfers between devices, swap(): return lax.ppermute(a, 'tp', SWAP)  11.1 us
    pallas_call x1, Pallas kernels, project(): pl.pallas_call(project_kernel, grid_spec=pltpu.PrefetchScalarGridSpec(num...  9.5 us
    all_to_all x1, starting transfers between devices, local(): lax.all_to_all(outgoing, 'st', split_axis=0, concat_axis=0, tiled=True)  8.42 us
    pallas_call x1, Pallas kernels, attend(): pl.pallas_call(attend_kernel, grid_spec=pltpu.PrefetchScalarGridSpec(num_...  7.85 us
    pallas_call x1, Pallas kernels, finish(): pl.pallas_call(finish_kernel, grid_spec=pltpu.PrefetchScalarGridSpec(num_...  7.66 us
  transfers between devices with their start and end apart: 29, of which 8 were waited for; matrix products, arithmetic and copies ran while one was open for 14% of the time, Pallas kernels for 11%

profile of v1, /device:TPU:1, one launch (start us, length us, event | category | flops | bytes accessed | tf_op | source)
XLA Modules:
  0.0 157.0 jit_solution(12979132082944673684)
XLA Ops:
  2.9 8.4 %all-to-all-start = ((s32[16,1,4]{2,1,0:T(1,128)}), s32[16,1,4]{2,1,0:T(1,128)S(1)}, u32[]{:S(2)}, u32[]{:S(2)}) async-start(s32[16,1,4]{2,1,0:T(1,128)} %bitcast.22), calls=%async_computation | async-start | bytes 16384 | tf_op jit(solution)/shard_map/all_to_all | solution.py:289
  11.4 1.1 constant_dynamic-update-slice_fusion.1
  12.5 1.1 constant_dynamic-update-slice_fusion.refs_0_
  13.6 5.8 %fusion = bf16[2048,256]{0,1:T(8,128)(2,1)S(1)} fusion(bf16[2048,2048]{1,0:T(8,128)(2,1)} %bitcast.44, bf16[2048,128]{1,0:T(8,128)(2,1)S(1)} %copy-done.22, bf16[2048,128]{1,0:T(8,128)(2,1)S(1)} %copy-done.23), kind=kOutput, calls=%fused_computation.2 | convolution fusion | flops 2150105088 | bytes 10485760 | tf_op jit(solution)/shard_map/dot_general | solution.py:54
  21.2 2.0 %gather_fusion = bf16[64,64,256]{2,1,0:T(8,128)(2,1)} fusion(bf16[32,64,256]{2,1,0:T(8,128)(2,1)S(1)} %bitcast.40, s32[1024]{0:T(1024)S(1)} %pad_clamp_fusion), kind=kCustom, calls=%fused_computation | custom fusion | bytes 4194560 | tf_op jit(solution)/shard_map/gather | solution.py:310
  23.2 6.6 %all-to-all-start.1 = ((bf16[16,4,64,256]{3,2,1,0:T(8,128)(2,1)}), bf16[16,4,64,256]{3,2,1,0:T(8,128)(2,1)S(1)}, u32[]{:S(2)}, u32[]{:S(2)}) async-start(bf16[16,4,64,256]{3,2,1,0:T(8,128)(2,1)} %bitcast.41), calls=%async_computation.1 | async-start | bytes 4194304 | tf_op jit(solution)/shard_map/all_to_all | solution.py:311
  29.9 1.4 collective-permute-start
  31.3 1.5 collective-permute-start.1
  32.8 1.6 collective-permute-start.2
  34.4 1.4 constant_dynamic-slice_fusion
  35.8 2.4 %collective-permute-start.11 = (bf16[1024,256]{1,0:T(8,128)(2,1)S(1)}, bf16[1024,256]{1,0:T(8,128)(2,1)}, u32[]{:S(2)}, u32[]{:S(2)}) collective-permute-start(bf16[1024,256]{1,0:T(8,128)(2,1)S(1)} %bitcast.43), channel_id=1, source_target_pairs={{0,1},{1,0},{2,3},{3,2},{4,5},{5,4},{6,7},{7,6},{8,9},{9,8},{10,11... | collective-permute-start | bytes 1572872 | tf_op jit(solution)/shard_map/ppermute | solution.py:42
  43.0 1.7 %constant_dynamic-update-slice_fusion.4 = bf16[192,2048]{1,0:T(8,128)(2,1)} fusion(bf16[64,2048]{1,0:T(8,128)(2,1)} %collective-permute-done), kind=kLoop, calls=%fused_computation.11 | loop fusion | bytes 524288
  44.6 2.3 %collective-permute-start.13 = (bf16[1024,256]{1,0:T(8,128)(2,1)S(1)}, bf16[1024,256]{1,0:T(8,128)(2,1)S(1)}, u32[]{:S(2)}, u32[]{:S(2)}) collective-permute-start(bf16[1024,256]{1,0:T(8,128)(2,1)S(1)} %bitcast.38), channel_id=1, source_target_pairs={{0,6},{1,7},{2,0},{3,1},{4,2},{5,3},{6,4},{7,5},{8,14},{9,15},{10,... | collective-permute-start | bytes 1572872 | tf_op jit(solution)/shard_map/ppermute | solution.py:38
  46.9 2.2 %collective-permute-start.15 = (bf16[1024,256]{1,0:T(8,128)(2,1)}, bf16[1024,256]{1,0:T(8,128)(2,1)}, u32[]{:S(2)}, u32[]{:S(2)}) collective-permute-start(bf16[1024,256]{1,0:T(8,128)(2,1)} %collective-permute-done.11.refs_1_), channel_id=1, source_target_pairs={{0,6},{1,7},{2,0},{3,1},{4,2},{5,3},{6,4},{7,5},{8,14},{9,15},{10,... | collective-permute-start | bytes 1572872 | tf_op jit(solution)/shard_map/ppermute | solution.py:38
  49.1 1.7 %constant_dynamic-update-slice_fusion.3 = bf16[192,2048]{1,0:T(8,128)(2,1)} fusion(bf16[192,2048]{1,0:T(8,128)(2,1)} %constant_dynamic-update-slice_fusion.4, bf16[64,2048]{1,0:T(8,128)(2,1)} %collective-permute-done.1), kind=kLoop, calls=%fused_computation.10 | loop fusion | bytes 524288
  50.8 1.7 %constant_dynamic-update-slice_fusion.2.refs_1_ = bf16[192,2048]{1,0:T(8,128)(2,1)} fusion(bf16[192,2048]{1,0:T(8,128)(2,1)} %constant_dynamic-update-slice_fusion.3, bf16[64,2048]{1,0:T(8,128)(2,1)} %collective-permute-done.2), kind=kLoop, calls=%fused_computation.9 | loop fusion | bytes 524288 | tf_op jit(solution)/shard_map/concatenate | solution.py:273
  52.5 5.0 %collective-permute-done.12.refs_2_ = bf16[1024,256]{1,0:T(8,128)(2,1)S(1)} collective-permute-done((bf16[1024,256]{1,0:T(8,128)(2,1)S(1)}, bf16[1024,256]{1,0:T(8,128)(2,1)S(1)}, u32[]{:S(2)}, u32[]{:S(2)}) %collective-permute-start.12) | collective-permute-done | bytes 524320 | tf_op jit(solution)/shard_map/ppermute | solution.py:38
  57.5 2.9 %collective-permute-start.5 = (bf16[192,2048]{1,0:T(8,128)(2,1)}, bf16[192,2048]{1,0:T(8,128)(2,1)}, u32[]{:S(2)}, u32[]{:S(2)}) collective-permute-start(bf16[192,2048]{1,0:T(8,128)(2,1)} %constant_dynamic-update-slice_fusion.2.refs_1_), channel_id=1, source_target_pairs={{0,16},{1,65},{2,18},{3,67},{4,20},{5,69},{6,22},{7,71},{8,24},{9,... | collective-permute-start | bytes 2359304 | tf_op jit(solution)/shard_map/ppermute | solution.py:46
  61.2 1.5 collective-permute-start.23
  62.8 6.4 %collective-permute-done.15.refs_5_ = bf16[1024,256]{1,0:T(8,128)(2,1)} collective-permute-done((bf16[1024,256]{1,0:T(8,128)(2,1)}, bf16[1024,256]{1,0:T(8,128)(2,1)}, u32[]{:S(2)}, u32[]{:S(2)}) %collective-permute-start.15) | collective-permute-done | bytes 524320 | tf_op jit(solution)/shard_map/ppermute | solution.py:38
  69.2 3.0 %collective-permute-start.16 = (bf16[1024,256]{1,0:T(8,128)(2,1)}, bf16[1024,256]{1,0:T(8,128)(2,1)S(1)}, u32[]{:S(2)}, u32[]{:S(2)}) collective-permute-start(bf16[1024,256]{1,0:T(8,128)(2,1)} %copy-done.7), channel_id=1, source_target_pairs={{0,2},{1,3},{2,4},{3,5},{4,6},{5,7},{6,0},{7,1},{8,10},{9,11},{10,... | collective-permute-start | bytes 1572872 | tf_op jit(solution)/shard_map/ppermute | solution.py:38
  72.1 1.6 collective-permute-start.3
  73.7 9.4 %collective-permute-done.16.refs_6_ = bf16[1024,256]{1,0:T(8,128)(2,1)S(1)} collective-permute-done((bf16[1024,256]{1,0:T(8,128)(2,1)}, bf16[1024,256]{1,0:T(8,128)(2,1)S(1)}, u32[]{:S(2)}, u32[]{:S(2)}) %collective-permute-start.16) | collective-permute-done | bytes 524320 | tf_op jit(solution)/shard_map/ppermute | solution.py:38
  83.9 2.8 %collective-permute-start.4 = (bf16[192,2048]{1,0:T(8,128)(2,1)}, bf16[192,2048]{1,0:T(8,128)(2,1)}, u32[]{:S(2)}, u32[]{:S(2)}) collective-permute-start(bf16[192,2048]{1,0:T(8,128)(2,1)} %constant_dynamic-update-slice_fusion.2.refs_1_), channel_id=1, source_target_pairs={{0,24},{1,97},{2,26},{3,99},{4,28},{5,101},{6,30},{7,103},{8,0},{9... | collective-permute-start | bytes 2359304 | tf_op jit(solution)/shard_map/ppermute | solution.py:46
  86.7 2.4 %collective-permute-start.7 = (bf16[192,2048]{1,0:T(8,128)(2,1)}, bf16[192,2048]{1,0:T(8,128)(2,1)S(1)}, u32[]{:S(2)}, u32[]{:S(2)}) collective-permute-start(bf16[192,2048]{1,0:T(8,128)(2,1)} %constant_dynamic-update-slice_fusion.2.refs_1_), channel_id=1, source_target_pairs={{0,1},{1,0},{2,3},{3,2},{4,5},{5,4},{6,7},{7,6},{8,9},{9,8},{10,11... | collective-permute-start | bytes 2359304 | tf_op jit(solution)/shard_map/ppermute | solution.py:42
  89.1 1.7 %collective-permute-start.17 = (bf16[1024,256]{1,0:T(8,128)(2,1)}, bf16[1024,256]{1,0:T(8,128)(2,1)S(1)}, u32[]{:S(2)}, u32[]{:S(2)}) collective-permute-start(bf16[1024,256]{1,0:T(8,128)(2,1)} %collective-permute-done.15.refs_5_), channel_id=1, source_target_pairs={{0,6},{1,7},{2,0},{3,1},{4,2},{5,3},{6,4},{7,5},{8,14},{9,15},{10,... | collective-permute-start | bytes 1572872 | tf_op jit(solution)/shard_map/ppermute | solution.py:38
  90.9 5.1 %collective-permute-done.4.refs_3_ = bf16[192,2048]{1,0:T(8,128)(2,1)} collective-permute-done((bf16[192,2048]{1,0:T(8,128)(2,1)}, bf16[192,2048]{1,0:T(8,128)(2,1)}, u32[]{:S(2)}, u32[]{:S(2)}) %collective-permute-start.4) | collective-permute-done | bytes 786464 | tf_op jit(solution)/shard_map/ppermute | solution.py:46
  96.0 3.0 %collective-permute-start.6 = (bf16[256,2048]{1,0:T(8,128)(2,1)S(1)}, bf16[256,2048]{1,0:T(8,128)(2,1)}, u32[]{:S(2)}, u32[]{:S(2)}) collective-permute-start(bf16[256,2048]{1,0:T(8,128)(2,1)S(1)} %constant_dynamic-update-slice_fusion.refs_0_), channel_id=1, source_target_pairs={{0,1},{1,0},{2,3},{3,2},{4,5},{5,4},{6,7},{7,6},{8,9},{9,8},{10,11... | collective-permute-start | bytes 3145736 | tf_op jit(solution)/shard_map/ppermute | solution.py:42
  99.8 2.9 %collective-permute-done.17.refs_7_ = bf16[1024,256]{1,0:T(8,128)(2,1)S(1)} collective-permute-done((bf16[1024,256]{1,0:T(8,128)(2,1)}, bf16[1024,256]{1,0:T(8,128)(2,1)S(1)}, u32[]{:S(2)}, u32[]{:S(2)}) %collective-permute-start.17) | collective-permute-done | bytes 524320 | tf_op jit(solution)/shard_map/ppermute | solution.py:38
  104.7 1.1 copy.39
  106.0 2.0 %pad.4.refs_10_ = bf16[2048,128]{1,0:T(8,128)(2,1)} pad(bf16[2048,2]{1,0:T(8,128)(2,1)} %copy.39, bf16[]{:T(256)} %constant.110.clone.1), padding=0_0x0_126 | pad | bytes 532482 | tf_op jit(solution)/shard_map/jit(_pad)/pad | solution.py:320
  108.2 1.0 copy-done.2
  109.2 1.0 copy-done.4
  110.3 1.0 copy-done.8
  111.3 1.0 copy-done.10
  112.3 1.0 copy-done.12
  113.4 1.0 copy-done.14
  114.4 9.5 %project.1 = (bf16[1024,256]{1,0:T(8,128)(2,1)S(1)}, bf16[256,256]{1,0:T(8,128)(2,1)}, bf16[256,256]{1,0:T(8,128)(2,1)S(1)}, bf16[256,256]{1,0:T(8,128)(2,1)}, b...) custom-call(s32[12]{0:T(128)S(1)} %stack.67.sc, bf16[1024,256]{1,0:T(8,128)(2,1)S(1)} %bitcast.39, ...), custom_call_target="tpu_custom_call" | custom-call | flops 4294967296 | bytes 9437184 | tf_op jit(solution)/shard_map/project/pallas_call | solution.py:107
  123.9 1.4 collective-permute-start.20
  125.4 7.9 %attend.1 = (bf16[256,256]{1,0:T(8,128)(2,1)}, bf16[256,256]{1,0:T(8,128)(2,1)}, bf16[256,256]{1,0:T(8,128)(2,1)}, bf16[256,256]{1,0:T(8,128)(2,1)S(1)}) custom-call(s32[20]{0:T(128)S(1)} %concatenate.18.sc, bf16[1024,256]{1,0:T(8,128)(2,1)S(1)} %get-tuple-element.19.q, bf16[64,64,256]{2,1,0:T(8,128)(2,1)S(1)} %bitcast.36, ...), custom_call_target="tpu_custom_call" | custom-call | flops 3000000000 | bytes 5242880 | tf_op jit(solution)/shard_map/attend/pallas_call | solution.py:147
  133.9 1.5 collective-permute-start.21
  135.4 1.4 collective-permute-start.22
  137.5 2.1 %collective-permute-start.25 = (bf16[256,256]{1,0:T(8,128)(2,1)}, bf16[256,256]{1,0:T(8,128)(2,1)S(1)}, u32[]{:S(2)}, u32[]{:S(2)}) collective-permute-start(bf16[256,256]{1,0:T(8,128)(2,1)} %get-tuple-element.22), channel_id=1, source_target_pairs={{0,6},{1,7},{2,0},{3,1},{4,2},{5,3},{6,4},{7,5},{8,14},{9,15},{10,... | collective-permute-start | bytes 393224 | tf_op jit(solution)/shard_map/ppermute | solution.py:38
  139.9 1.6 collective-permute-done.22.refs_13_
  141.5 3.9 %collective-permute-done.24.refs_15_ = bf16[256,256]{1,0:T(8,128)(2,1)S(1)} collective-permute-done((bf16[256,256]{1,0:T(8,128)(2,1)}, bf16[256,256]{1,0:T(8,128)(2,1)S(1)}, u32[]{:S(2)}, u32[]{:S(2)}) %collective-permute-start.24) | collective-permute-done | bytes 131104 | tf_op jit(solution)/shard_map/ppermute | solution.py:38
  145.4 1.7 %collective-permute-done.26.refs_17_ = bf16[256,256]{1,0:T(8,128)(2,1)S(1)} collective-permute-done((bf16[256,256]{1,0:T(8,128)(2,1)}, bf16[256,256]{1,0:T(8,128)(2,1)S(1)}, u32[]{:S(2)}, u32[]{:S(2)}) %collective-permute-start.26) | collective-permute-done | bytes 131104 | tf_op jit(solution)/shard_map/ppermute | solution.py:38
  147.1 1.1 copy-done.1
  149.2 7.7 %finish.1 = bf16[256,2048]{1,0:T(8,128)(2,1)} custom-call(s32[2]{0:T(128)S(1)} %pad_add_fusion.sc, bf16[256,2048]{1,0:T(8,128)(2,1)S(1)} %constant_dynamic-update-slice_fusion.refs_0_, bf16[192,2048]{1,0:T(8,128)(2,1)} %constant_dynamic-update-slice_fusion.2.refs_1_, bf16[192,2048]{1,0:T(8,128)(2,1)} %collective-permute-done.3.refs_2_, ...), custom_call_target="tpu_custom_call" | custom-call | flops 2147483648 | bytes 10485760 | tf_op jit(solution)/shard_map/finish/pallas_call | solution.py:222
  (101 shorter events, 16.9 us)
Async XLA Ops:
  0.0 13.6 %copy-start.23 = (bf16[2048,128]{1,0:T(8,128)(2,1)S(1)}, bf16[2048,128]{1,0:T(8,128)(2,1)}, u32[]{:S(2)}) copy-start(bf16[2048,128]{1,0:T(8,128)(2,1)} %param.19) | copy-start | bytes 1572868
  0.0 13.6 %copy-start.22 = (bf16[2048,128]{1,0:T(8,128)(2,1)S(1)}, bf16[2048,128]{1,0:T(8,128)(2,1)}, u32[]{:S(2)}) copy-start(bf16[2048,128]{1,0:T(8,128)(2,1)} %param.20) | copy-start | bytes 1572868
  2.9 17.0 %all-to-all-start = ((s32[16,1,4]{2,1,0:T(1,128)}), s32[16,1,4]{2,1,0:T(1,128)S(1)}, u32[]{:S(2)}, u32[]{:S(2)}) async-start(s32[16,1,4]{2,1,0:T(1,128)} %bitcast.22), calls=%async_computation | async-start | bytes 16384 | tf_op jit(solution)/shard_map/all_to_all | solution.py:289
  23.2 38.0 %all-to-all-start.1 = ((bf16[16,4,64,256]{3,2,1,0:T(8,128)(2,1)}), bf16[16,4,64,256]{3,2,1,0:T(8,128)(2,1)S(1)}, u32[]{:S(2)}, u32[]{:S(2)}) async-start(bf16[16,4,64,256]{3,2,1,0:T(8,128)(2,1)} %bitcast.41), calls=%async_computation.1 | async-start | bytes 4194304 | tf_op jit(solution)/shard_map/all_to_all | solution.py:311
  29.9 8.4 %copy-start.15 = (bf16[3,128]{1,0:T(4,128)(2,1)S(1)}, bf16[3,128]{1,0:T(4,128)(2,1)}, u32[]{:S(2)}) copy-start(bf16[3,128]{1,0:T(4,128)(2,1)} %refs_11_.1) | copy-start | bytes 2308
  29.9 12.4 %collective-permute-start = (bf16[64,2048]{1,0:T(8,128)(2,1)S(1)}, bf16[64,2048]{1,0:T(8,128)(2,1)}, u32[]{:S(2)}, u32[]{:S(2)}) collective-permute-start(bf16[64,2048]{1,0:T(8,128)(2,1)S(1)} %dynamic-slice_bitcast_fusion), channel_id=1, source_target_pairs={{0,2},{1,3},{2,4},{3,5},{4,6},{5,7},{6,0},{7,1},{8,10},{9,11},{10,... | collective-permute-start | bytes 786440 | tf_op jit(solution)/shard_map/ppermute | solution.py:38
  31.3 13.4 %collective-permute-start.1 = (bf16[64,2048]{1,0:T(8,128)(2,1)S(1)}, bf16[64,2048]{1,0:T(8,128)(2,1)}, u32[]{:S(2)}, u32[]{:S(2)}) collective-permute-start(bf16[64,2048]{1,0:T(8,128)(2,1)S(1)} %dynamic-slice_bitcast_fusion), channel_id=1, source_target_pairs={{0,6},{1,7},{2,0},{3,1},{4,2},{5,3},{6,4},{7,5},{8,14},{9,15},{10,... | collective-permute-start | bytes 786440 | tf_op jit(solution)/shard_map/ppermute | solution.py:38
  32.8 16.3 %collective-permute-start.2 = (bf16[64,2048]{1,0:T(8,128)(2,1)S(1)}, bf16[64,2048]{1,0:T(8,128)(2,1)}, u32[]{:S(2)}, u32[]{:S(2)}) collective-permute-start(bf16[64,2048]{1,0:T(8,128)(2,1)S(1)} %dynamic-slice_bitcast_fusion), channel_id=1, source_target_pairs={{0,4},{1,5},{2,6},{3,7},{4,0},{5,1},{6,2},{7,3},{8,12},{9,13},{10,... | collective-permute-start | bytes 786440 | tf_op jit(solution)/shard_map/ppermute | solution.py:38
  34.4 4.0 %copy-start.16 = (bf16[2048,128]{1,0:T(8,128)(2,1)S(1)}, bf16[2048,128]{1,0:T(8,128)(2,1)}, u32[]{:S(2)}) copy-start(bf16[2048,128]{1,0:T(8,128)(2,1)} %param.18) | copy-start | bytes 1572868
  34.4 4.8 %copy-start.17 = (bf16[2048,128]{1,0:T(8,128)(2,1)S(1)}, bf16[2048,128]{1,0:T(8,128)(2,1)}, u32[]{:S(2)}) copy-start(bf16[2048,128]{1,0:T(8,128)(2,1)} %param.21) | copy-start | bytes 1572868
  34.4 5.7 %copy-start.18 = (bf16[2048,128]{1,0:T(8,128)(2,1)S(1)}, bf16[2048,128]{1,0:T(8,128)(2,1)}, u32[]{:S(2)}) copy-start(bf16[2048,128]{1,0:T(8,128)(2,1)} %param.22) | copy-start | bytes 1572868
  35.7 8.9 %copy-start.3 = (bf16[4,1,256,256]{3,2,1,0:T(8,128)(2,1)}, bf16[4,1,256,256]{3,2,1,0:T(8,128)(2,1)S(1)}, u32[]{:S(2)}) copy-start(bf16[4,1,256,256]{3,2,1,0:T(8,128)(2,1)S(1)} %get-tuple-element.26) | copy-start | bytes 1572868
  35.8 5.2 %copy-start.19 = (bf16[2048,128]{1,0:T(8,128)(2,1)S(1)}, bf16[2048,128]{1,0:T(8,128)(2,1)}, u32[]{:S(2)}) copy-start(bf16[2048,128]{1,0:T(8,128)(2,1)} %param.23) | copy-start | bytes 1572868
  35.8 11.2 %collective-permute-start.11 = (bf16[1024,256]{1,0:T(8,128)(2,1)S(1)}, bf16[1024,256]{1,0:T(8,128)(2,1)}, u32[]{:S(2)}, u32[]{:S(2)}) collective-permute-start(bf16[1024,256]{1,0:T(8,128)(2,1)S(1)} %bitcast.43), channel_id=1, source_target_pairs={{0,1},{1,0},{2,3},{3,2},{4,5},{5,4},{6,7},{7,6},{8,9},{9,8},{10,11... | collective-permute-start | bytes 1572872 | tf_op jit(solution)/shard_map/ppermute | solution.py:42
  38.2 3.7 %collective-permute-start.19 = (bf16[3,128]{1,0:T(4,128)(2,1)S(1)}, bf16[3,128]{1,0:T(4,128)(2,1)S(1)}, u32[]{:S(2)}, u32[]{:S(2)}) collective-permute-start(bf16[3,128]{1,0:T(4,128)(2,1)S(1)} %copy-done.15), channel_id=1, source_target_pairs={{0,1},{1,0},{2,3},{3,2},{4,5},{5,4},{6,7},{7,6},{8,9},{9,8},{10,11... | collective-permute-start | bytes 2312 | tf_op jit(solution)/shard_map/ppermute | solution.py:42
  40.1 64.4 %copy-start.21 = (s32[16,2]{0,1:T(2,128)S(1)}, s32[16,2]{0,1:T(2,128)}, u32[]{:S(2)}) copy-start(s32[16,2]{0,1:T(2,128)} %param.16) | copy-start | bytes 388
  40.1 64.6 %copy-start.20 = (bf16[2048,2]{0,1:T(2,128)(2,1)S(1)}, bf16[2048,2]{0,1:T(2,128)(2,1)}, u32[]{:S(2)}) copy-start(bf16[2048,2]{0,1:T(2,128)(2,1)} %param.25) | copy-start | bytes 24580
  41.9 15.6 %collective-permute-start.12 = (bf16[1024,256]{1,0:T(8,128)(2,1)S(1)}, bf16[1024,256]{1,0:T(8,128)(2,1)S(1)}, u32[]{:S(2)}, u32[]{:S(2)}) collective-permute-start(bf16[1024,256]{1,0:T(8,128)(2,1)S(1)} %bitcast.37), channel_id=1, source_target_pairs={{0,2},{1,3},{2,4},{3,5},{4,6},{5,7},{6,0},{7,1},{8,10},{9,11},{10,... | collective-permute-start | bytes 1572872 | tf_op jit(solution)/shard_map/ppermute | solution.py:38
  42.3 62.2 %collective-permute-start.18 = (bf16[2048,512]{1,0:T(8,128)(2,1)}, bf16[2048,512]{1,0:T(8,128)(2,1)}, u32[]{:S(2)}, u32[]{:S(2)}) collective-permute-start(bf16[2048,512]{1,0:T(8,128)(2,1)} %constant_dynamic-update-slice_fusion.5.refs_8_), channel_id=1, source_target_pairs={{0,1},{1,0},{2,3},{3,2},{4,5},{5,4},{6,7},{7,6},{8,9},{9,8},{10,11... | collective-permute-start | bytes 6291464 | tf_op jit(solution)/shard_map/ppermute | solution.py:42
  44.6 15.8 %collective-permute-start.13 = (bf16[1024,256]{1,0:T(8,128)(2,1)S(1)}, bf16[1024,256]{1,0:T(8,128)(2,1)S(1)}, u32[]{:S(2)}, u32[]{:S(2)}) collective-permute-start(bf16[1024,256]{1,0:T(8,128)(2,1)S(1)} %bitcast.38), channel_id=1, source_target_pairs={{0,6},{1,7},{2,0},{3,1},{4,2},{5,3},{6,4},{7,5},{8,14},{9,15},{10,... | collective-permute-start | bytes 1572872 | tf_op jit(solution)/shard_map/ppermute | solution.py:38
  46.9 22.2 %collective-permute-start.15 = (bf16[1024,256]{1,0:T(8,128)(2,1)}, bf16[1024,256]{1,0:T(8,128)(2,1)}, u32[]{:S(2)}, u32[]{:S(2)}) collective-permute-start(bf16[1024,256]{1,0:T(8,128)(2,1)} %collective-permute-done.11.refs_1_), channel_id=1, source_target_pairs={{0,6},{1,7},{2,0},{3,1},{4,2},{5,3},{6,4},{7,5},{8,14},{9,15},{10,... | collective-permute-start | bytes 1572872 | tf_op jit(solution)/shard_map/ppermute | solution.py:38
  49.1 23.0 %collective-permute-start.14 = (bf16[1024,256]{1,0:T(8,128)(2,1)}, bf16[1024,256]{1,0:T(8,128)(2,1)}, u32[]{:S(2)}, u32[]{:S(2)}) collective-permute-start(bf16[1024,256]{1,0:T(8,128)(2,1)} %collective-permute-done.11.refs_1_), channel_id=1, source_target_pairs={{0,2},{1,3},{2,4},{3,5},{4,6},{5,7},{6,0},{7,1},{8,10},{9,11},{10,... | collective-permute-start | bytes 1572872 | tf_op jit(solution)/shard_map/ppermute | solution.py:38
  57.5 2.9 %copy-start.7 = (bf16[1024,256]{1,0:T(8,128)(2,1)}, bf16[1024,256]{1,0:T(8,128)(2,1)S(1)}, u32[]{:S(2)}) copy-start(bf16[1024,256]{1,0:T(8,128)(2,1)S(1)} %collective-permute-done.12.refs_2_) | copy-start | bytes 1572868
  57.5 29.2 %collective-permute-start.5 = (bf16[192,2048]{1,0:T(8,128)(2,1)}, bf16[192,2048]{1,0:T(8,128)(2,1)}, u32[]{:S(2)}, u32[]{:S(2)}) collective-permute-start(bf16[192,2048]{1,0:T(8,128)(2,1)} %constant_dynamic-update-slice_fusion.2.refs_1_), channel_id=1, source_target_pairs={{0,16},{1,65},{2,18},{3,67},{4,20},{5,69},{6,22},{7,71},{8,24},{9,... | collective-permute-start | bytes 2359304 | tf_op jit(solution)/shard_map/ppermute | solution.py:46
  61.2 62.7 %collective-permute-start.23 = (bf16[64,64,256]{2,1,0:T(8,128)(2,1)S(1)}, bf16[64,64,256]{2,1,0:T(8,128)(2,1)}, u32[]{:S(2)}, u32[]{:S(2)}) collective-permute-start(bf16[64,64,256]{2,1,0:T(8,128)(2,1)S(1)} %bitcast.35), channel_id=1, source_target_pairs={{0,1},{1,0},{2,3},{3,2},{4,5},{5,4},{6,7},{7,6},{8,9},{9,8},{10,11... | collective-permute-start | bytes 6291464 | tf_op jit(solution)/shard_map/ppermute | solution.py:42
  69.2 14.0 %collective-permute-start.16 = (bf16[1024,256]{1,0:T(8,128)(2,1)}, bf16[1024,256]{1,0:T(8,128)(2,1)S(1)}, u32[]{:S(2)}, u32[]{:S(2)}) collective-permute-start(bf16[1024,256]{1,0:T(8,128)(2,1)} %copy-done.7), channel_id=1, source_target_pairs={{0,2},{1,3},{2,4},{3,5},{4,6},{5,7},{6,0},{7,1},{8,10},{9,11},{10,... | collective-permute-start | bytes 1572872 | tf_op jit(solution)/shard_map/ppermute | solution.py:38
  72.1 17.0 %collective-permute-start.3 = (bf16[192,2048]{1,0:T(8,128)(2,1)}, bf16[192,2048]{1,0:T(8,128)(2,1)}, u32[]{:S(2)}, u32[]{:S(2)}) collective-permute-start(bf16[192,2048]{1,0:T(8,128)(2,1)} %constant_dynamic-update-slice_fusion.2.refs_1_), channel_id=1, source_target_pairs={{0,8},{1,33},{2,10},{3,35},{4,12},{5,37},{6,14},{7,39},{8,16},{9,4... | collective-permute-start | bytes 2359304 | tf_op jit(solution)/shard_map/ppermute | solution.py:46
  83.9 12.0 %collective-permute-start.4 = (bf16[192,2048]{1,0:T(8,128)(2,1)}, bf16[192,2048]{1,0:T(8,128)(2,1)}, u32[]{:S(2)}, u32[]{:S(2)}) collective-permute-start(bf16[192,2048]{1,0:T(8,128)(2,1)} %constant_dynamic-update-slice_fusion.2.refs_1_), channel_id=1, source_target_pairs={{0,24},{1,97},{2,26},{3,99},{4,28},{5,101},{6,30},{7,103},{8,0},{9... | collective-permute-start | bytes 2359304 | tf_op jit(solution)/shard_map/ppermute | solution.py:46
  86.7 12.2 %collective-permute-start.7 = (bf16[192,2048]{1,0:T(8,128)(2,1)}, bf16[192,2048]{1,0:T(8,128)(2,1)S(1)}, u32[]{:S(2)}, u32[]{:S(2)}) collective-permute-start(bf16[192,2048]{1,0:T(8,128)(2,1)} %constant_dynamic-update-slice_fusion.2.refs_1_), channel_id=1, source_target_pairs={{0,1},{1,0},{2,3},{3,2},{4,5},{5,4},{6,7},{7,6},{8,9},{9,8},{10,11... | collective-permute-start | bytes 2359304 | tf_op jit(solution)/shard_map/ppermute | solution.py:42
  89.1 13.6 %collective-permute-start.17 = (bf16[1024,256]{1,0:T(8,128)(2,1)}, bf16[1024,256]{1,0:T(8,128)(2,1)S(1)}, u32[]{:S(2)}, u32[]{:S(2)}) collective-permute-start(bf16[1024,256]{1,0:T(8,128)(2,1)} %collective-permute-done.15.refs_5_), channel_id=1, source_target_pairs={{0,6},{1,7},{2,0},{3,1},{4,2},{5,3},{6,4},{7,5},{8,14},{9,15},{10,... | collective-permute-start | bytes 1572872 | tf_op jit(solution)/shard_map/ppermute | solution.py:38
  96.0 37.9 %collective-permute-start.6 = (bf16[256,2048]{1,0:T(8,128)(2,1)S(1)}, bf16[256,2048]{1,0:T(8,128)(2,1)}, u32[]{:S(2)}, u32[]{:S(2)}) collective-permute-start(bf16[256,2048]{1,0:T(8,128)(2,1)S(1)} %constant_dynamic-update-slice_fusion.refs_0_), channel_id=1, source_target_pairs={{0,1},{1,0},{2,3},{3,2},{4,5},{5,4},{6,7},{7,6},{8,9},{9,8},{10,11... | collective-permute-start | bytes 3145736 | tf_op jit(solution)/shard_map/ppermute | solution.py:42
  99.8 35.6 %collective-permute-start.10 = (bf16[192,2048]{1,0:T(8,128)(2,1)}, bf16[192,2048]{1,0:T(8,128)(2,1)}, u32[]{:S(2)}, u32[]{:S(2)}) collective-permute-start(bf16[192,2048]{1,0:T(8,128)(2,1)} %collective-permute-done.5.refs_4_), channel_id=1, source_target_pairs={{0,1},{1,0},{2,3},{3,2},{4,5},{5,4},{6,7},{7,6},{8,9},{9,8},{10,11... | collective-permute-start | bytes 2359304 | tf_op jit(solution)/shard_map/ppermute | solution.py:42
  103.5 33.3 %collective-permute-start.8 = (bf16[192,2048]{1,0:T(8,128)(2,1)}, bf16[192,2048]{1,0:T(8,128)(2,1)}, u32[]{:S(2)}, u32[]{:S(2)}) collective-permute-start(bf16[192,2048]{1,0:T(8,128)(2,1)} %collective-permute-done.3.refs_2_), channel_id=1, source_target_pairs={{0,1},{1,0},{2,3},{3,2},{4,5},{5,4},{6,7},{7,6},{8,9},{9,8},{10,11... | collective-permute-start | bytes 2359304 | tf_op jit(solution)/shard_map/ppermute | solution.py:42
  104.5 33.0 %collective-permute-start.9 = (bf16[192,2048]{1,0:T(8,128)(2,1)}, bf16[192,2048]{1,0:T(8,128)(2,1)}, u32[]{:S(2)}, u32[]{:S(2)}) collective-permute-start(bf16[192,2048]{1,0:T(8,128)(2,1)} %collective-permute-done.4.refs_3_), channel_id=1, source_target_pairs={{0,1},{1,0},{2,3},{3,2},{4,5},{5,4},{6,7},{7,6},{8,9},{9,8},{10,11... | collective-permute-start | bytes 2359304 | tf_op jit(solution)/shard_map/ppermute | solution.py:42
  108.2 1.0 copy-start.2
  109.2 1.0 copy-start.4
  110.3 1.0 copy-start.8
  111.3 1.0 copy-start.10
  112.3 1.0 copy-start.12
  113.4 1.0 copy-start.14
  123.9 15.6 %collective-permute-start.20 = (bf16[256,256]{1,0:T(8,128)(2,1)S(1)}, bf16[256,256]{1,0:T(8,128)(2,1)S(1)}, u32[]{:S(2)}, u32[]{:S(2)}) collective-permute-start(bf16[256,256]{1,0:T(8,128)(2,1)S(1)} %get-tuple-element.16), channel_id=1, source_target_pairs={{0,2},{1,3},{2,4},{3,5},{4,6},{5,7},{6,0},{7,1},{8,10},{9,11},{10,... | collective-permute-start | bytes 393224 | tf_op jit(solution)/shard_map/ppermute | solution.py:38
  133.9 6.1 %collective-permute-start.21 = (bf16[256,256]{1,0:T(8,128)(2,1)}, bf16[256,256]{1,0:T(8,128)(2,1)S(1)}, u32[]{:S(2)}, u32[]{:S(2)}) collective-permute-start(bf16[256,256]{1,0:T(8,128)(2,1)} %get-tuple-element.17), channel_id=1, source_target_pairs={{0,6},{1,7},{2,0},{3,1},{4,2},{5,3},{6,4},{7,5},{8,14},{9,15},{10,... | collective-permute-start | bytes 393224 | tf_op jit(solution)/shard_map/ppermute | solution.py:38
  135.4 6.1 %collective-permute-start.22 = (bf16[256,256]{1,0:T(8,128)(2,1)}, bf16[256,256]{1,0:T(8,128)(2,1)S(1)}, u32[]{:S(2)}, u32[]{:S(2)}) collective-permute-start(bf16[256,256]{1,0:T(8,128)(2,1)} %get-tuple-element.18), channel_id=1, source_target_pairs={{0,4},{1,5},{2,6},{3,7},{4,0},{5,1},{6,2},{7,3},{8,12},{9,13},{10,... | collective-permute-start | bytes 393224 | tf_op jit(solution)/shard_map/ppermute | solution.py:38
  136.8 8.6 %collective-permute-start.24 = (bf16[256,256]{1,0:T(8,128)(2,1)}, bf16[256,256]{1,0:T(8,128)(2,1)S(1)}, u32[]{:S(2)}, u32[]{:S(2)}) collective-permute-start(bf16[256,256]{1,0:T(8,128)(2,1)} %get-tuple-element.21), channel_id=1, source_target_pairs={{0,2},{1,3},{2,4},{3,5},{4,6},{5,7},{6,0},{7,1},{8,10},{9,11},{10,... | collective-permute-start | bytes 393224 | tf_op jit(solution)/shard_map/ppermute | solution.py:38
  137.5 8.0 %collective-permute-start.25 = (bf16[256,256]{1,0:T(8,128)(2,1)}, bf16[256,256]{1,0:T(8,128)(2,1)S(1)}, u32[]{:S(2)}, u32[]{:S(2)}) collective-permute-start(bf16[256,256]{1,0:T(8,128)(2,1)} %get-tuple-element.22), channel_id=1, source_target_pairs={{0,6},{1,7},{2,0},{3,1},{4,2},{5,3},{6,4},{7,5},{8,14},{9,15},{10,... | collective-permute-start | bytes 393224 | tf_op jit(solution)/shard_map/ppermute | solution.py:38
  139.5 7.6 %collective-permute-start.26 = (bf16[256,256]{1,0:T(8,128)(2,1)}, bf16[256,256]{1,0:T(8,128)(2,1)S(1)}, u32[]{:S(2)}, u32[]{:S(2)}) collective-permute-start(bf16[256,256]{1,0:T(8,128)(2,1)} %get-tuple-element.23), channel_id=1, source_target_pairs={{0,4},{1,5},{2,6},{3,7},{4,0},{5,1},{6,2},{7,3},{8,12},{9,13},{10,... | collective-permute-start | bytes 393224 | tf_op jit(solution)/shard_map/ppermute | solution.py:38
  147.1 1.1 copy-start.1
  148.3 0.9 copy-start.6
  (5 other events, 3.9 us)

commit v2 on v1

v2 whole, which is shorter than its diff:
```python
import functools

import jax
import jax.numpy as jnp
from jax import lax
from jax.experimental import pallas as pl
from jax.experimental.pallas import tpu as pltpu
from jax.sharding import PartitionSpec as P

HEAD_SIZE = 128
SEQ_LEN = 256
BLOCK = 128
PLEN = 64
N_Y = 4
N_X = 4
N_Z = 4
BF = jnp.bfloat16
F32 = jnp.float32


SHIFT = {
    s: [(2 * y + c, 2 * ((y + s) % N_Y) + c) for y in range(N_Y) for c in range(2)]
    for s in (1, -1, 2)
}
SWAP = [(2 * y + c, 2 * y + 1 - c) for y in range(N_Y) for c in range(2)]


def plane_shift(s):
    pairs = []
    for z in range(N_Z):
        for x in range(N_X):
            for y in range(N_Y):
                for c in range(2):
                    z2, x2 = (z, (x + s) % N_X) if c == 0 else ((z + s) % N_Z, x)
                    pairs.append(((z * N_X + x) * 8 + 2 * y + c, (z2 * N_X + x2) * 8 + 2 * y + c))
    return pairs


def shift(a, s):
    return lax.ppermute(a, "tp", SHIFT[s])


def swap(a):
    return lax.ppermute(a, "tp", SWAP)


def plane(a, s):
    return lax.ppermute(a, ("st", "tp"), plane_shift(s))


def pick(a, index, axis=0):
    return lax.dynamic_index_in_dim(a, index, axis, keepdims=False)


def dot(a, b):
    return jnp.dot(a, b, preferred_element_type=F32)


def call(body, sc, ins, in_specs, outs, out_specs, scratch=(), grid=(1,), flops=0, bytes_=0, vmem=62):
    return pl.pallas_call(
        body,
        grid_spec=pltpu.PrefetchScalarGridSpec(
            num_scalar_prefetch=1,
            grid=grid,
            in_specs=in_specs,
            out_specs=out_specs,
            scratch_shapes=list(scratch),
        ),
        out_shape=[jax.ShapeDtypeStruct(shape, dtype) for shape, dtype in outs],
        compiler_params=pltpu.CompilerParams(vmem_limit_bytes=vmem * 2**20),
        cost_estimate=pl.CostEstimate(flops=flops, bytes_accessed=bytes_, transcendentals=0),
    )(sc, *ins)


def whole(a):
    return pl.BlockSpec(a.shape, lambda *_, n=a.ndim: (0,) * n)


def fixed(*shape):
    return pl.BlockSpec(shape, lambda *_, n=len(shape): (0,) * n)


HBM = pl.BlockSpec(memory_space=pl.ANY)


def part_kernel(sc, a, b, out):
    n = a.shape[0]
    out[:n] = a[...]
    out[n:] = b[...]


def weight_part(sc, conv_out, memory_out):
    n, d = conv_out.shape[0] // 4, conv_out.shape[1]
    spec = pl.BlockSpec((n, d), lambda i, s: (s[0], 0))
    return call(
        part_kernel, sc, (conv_out, memory_out), [spec, spec],
        [((2 * n, d), BF)], [fixed(2 * n, d)], bytes_=2**19, flops=10**8,
    )[0]


def pack_kernel(sc, a, b, c, out):
    n = a.shape[0]
    out[:n] = a[...]
    out[n : 2 * n] = b[...]
    out[2 * n :] = c[...]


def pack(sc, parts):
    n, d = parts[0].shape
    return call(
        pack_kernel, sc, parts, [whole(p) for p in parts],
        [((3 * n, d), BF)], [fixed(3 * n, d)], bytes_=2**20, flops=10**8,
    )[0]


def serve_kernel(sc, rows, kw, vw, out, table, w, sems):
    j = pl.program_id(0)
    H = kw.shape[1]

    @pl.when(j == 0)
    def _():
        w[:, :H] = kw[...]
        w[:, H:] = vw[...]

    per = rows.shape[0] // PLEN
    kv = dot(rows[...], w[...]).astype(BF)
    table[pl.ds(j * per, per)] = kv.reshape(per, PLEN, 2 * H)

    @pl.when(j == pl.num_programs(0) - 1)
    def _():
        n_own, cap = out.shape[0], out.shape[1]
        copies = [
            pltpu.make_async_copy(table.at[sc[o, k]], out.at[o, k], sems.at[o * cap + k])
            for o in range(n_own)
            for k in range(cap)
        ]
        for c in copies:
            c.start()
        for c in copies:
            c.wait()


def serve(wanted, store, kw, vw):
    n_own, cap = wanted.shape
    flat = store.reshape(-1, store.shape[-1])
    rows, d = flat.shape
    H = kw.shape[1]
    block = 256
    return call(
        serve_kernel, wanted, (flat, kw, vw),
        [pl.BlockSpec((block, d), lambda j, s: (j, 0)), whole(kw), whole(vw)],
        [((n_own, cap, PLEN, 2 * H), BF)], [HBM],
        scratch=[
            pltpu.VMEM((store.shape[0], PLEN, 2 * H), BF),
            pltpu.VMEM((d, 2 * H), BF),
            pltpu.SemaphoreType.DMA((n_own * cap,)),
        ],
        grid=(rows // block,), flops=2 * rows * d * 2 * H, bytes_=11 * 2**20,
    )[0]


def load_weights(sc, first, count, weights, w, sems):
    copies = []
    for k in range(count):
        row = pl.ds(pl.multiple_of(sc[first + k] * 256, 256), 256)
        for n, ref in enumerate(weights):
            copies.append(
                pltpu.make_async_copy(
                    ref.at[row], w.at[k, :, pl.ds(n * 128, 128)], sems.at[k * 8 + n]
                )
            )
    for c in copies:
        c.start()
    for c in copies:
        c.wait()


def gate_part(sc, first, pieces, gate):
    acc = None
    for k, p in enumerate(pieces):
        cols = pl.ds(pl.multiple_of(sc[first + k] * 256, 256), 256)
        a = lax.dot_general(
            p[...], gate[:, cols], (((1,), (1,)), ((), ())), preferred_element_type=F32
        )
        acc = a if acc is None else acc + a
    return acc


def project1_kernel(sc, *refs):
    pieces, weights = refs[:6], refs[6:14]
    gate, acc_ref, logit_ref, w, sems = refs[14:]
    j = pl.program_id(0)

    @pl.when(j == 0)
    def _():
        load_weights(sc, 0, 6, weights, w, sems)

    acc = None
    for k in range(6):
        a = dot(pieces[k][...], w[k])
        acc = a if acc is None else acc + a
    acc_ref[...] = acc

    @pl.when(j == 3)
    def _():
        logit_ref[...] = gate_part(sc, 0, pieces, gate)


def project2_kernel(sc, *refs):
    pieces, acc_in, weights = refs[:2], refs[2], refs[3:11]
    gate, tm, to, logit_in = refs[11:15]
    q_ref, conv_refs, logit_ref, w, sems = refs[15], refs[16:20], refs[20], refs[21], refs[22]
    j = pl.program_id(0)

    @pl.when(j == 0)
    def _():
        load_weights(sc, 6, 2, weights, w, sems)

    acc = acc_in[...]
    for k in range(2):
        acc = acc + dot(pieces[k][...], w[k])
    H = HEAD_SIZE
    ids = lax.broadcasted_iota(jnp.int32, (SEQ_LEN, H), 0)

    def conv(a, taps):
        t = taps[...].astype(F32)
        prod = a[:, 2 * H : 3 * H] * a[:, 3 * H :]
        back1 = jnp.where(ids >= 1, pltpu.roll(prod, 1, 0), 0.0)
        back2 = jnp.where(ids >= 2, pltpu.roll(prod, 2, 0), 0.0)
        filtered = t[0:1] * back2 + t[1:2] * back1 + t[2:3] * prod
        return (a[:, H : 2 * H] * filtered).astype(BF)

    q_ref[:, :H] = acc[:, :H].astype(BF)
    q_ref[:, H:] = acc[:, 4 * H : 5 * H].astype(BF)
    cm, co = conv(acc[:, : 4 * H], tm), conv(acc[:, 4 * H :], to)
    for i in range(4):

        @pl.when(j == i)
        def _(i=i):
            conv_refs[i][:, :H] = cm
            conv_refs[i][:, H:] = co

    @pl.when(j == 3)
    def _():
        logit_ref[...] = logit_in[...] + gate_part(sc, 6, pieces, gate)


TILE = lambda n: pl.BlockSpec((SEQ_LEN, n), lambda j, s: (s[8 + j], 0))


def project1(sc, pieces, weights, gate):
    rows = pieces[0].shape[0]
    return call(
        project1_kernel, sc, (*pieces, *weights, gate),
        [TILE(256)] * 6 + [HBM] * 8 + [whole(gate)],
        [((rows, 1024), F32), ((SEQ_LEN, 2), F32)], [TILE(1024), fixed(SEQ_LEN, 2)],
        scratch=[pltpu.VMEM((6, 256, 1024), BF), pltpu.SemaphoreType.DMA((48,))],
        grid=(4,), flops=2 * rows * 1536 * 1024, bytes_=10 * 2**20,
    )


def project2(sc, pieces, acc, weights, gate, tm, to, logits):
    rows = pieces[0].shape[0]
    return call(
        project2_kernel, sc, (*pieces, acc, *weights, gate, tm, to, logits),
        [TILE(256)] * 2 + [TILE(1024)] + [HBM] * 8 + [whole(a) for a in (gate, tm, to, logits)],
        [((rows, 256), BF)] + [((SEQ_LEN, 256), BF)] * 4 + [((SEQ_LEN, 2), F32)],
        [TILE(256)] + [fixed(SEQ_LEN, 256)] * 4 + [fixed(SEQ_LEN, 2)],
        scratch=[pltpu.VMEM((2, 256, 1024), BF), pltpu.SemaphoreType.DMA((16,))],
        grid=(4,), flops=2 * rows * 512 * 1024, bytes_=8 * 2**20,
    )


def attend_kernel(sc, q, tab_m, tab_o, o0, o1, o2, o3, s_ref, p_ref):
    H = HEAD_SIZE
    outs = (o0, o1, o2, o3)
    work = []
    for j in range(4):
        for half in range(2):
            b = sc[16 + j] * 2 + half
            rows = pl.ds(pl.multiple_of(b * BLOCK, BLOCK), BLOCK)
            for h, tab in enumerate((tab_m, tab_o)):
                work.append((j, half, h, tab, sc[2 * b], sc[2 * b + 1], rows))
    n = len(work)
    for i, (j, half, h, tab, t0, t1, rows) in enumerate(work):
        k = jnp.concatenate([tab[t0, :, :H], tab[t1, :, :H]], axis=0)
        s_ref[i * BLOCK : (i + 1) * BLOCK] = lax.dot_general(
            q[rows, h * H : (h + 1) * H], k, (((1,), (1,)), ((), ())), preferred_element_type=F32
        )
    for i in range(0, n, 4):
        part = slice(i * BLOCK, (i + 4) * BLOCK)
        s = s_ref[part] * (H**-0.5)
        e = jnp.exp(s - jnp.max(s, axis=-1, keepdims=True))
        p_ref[part] = (e / jnp.sum(e, axis=-1, keepdims=True)).astype(BF)
    for i, (j, half, h, tab, t0, t1, rows) in enumerate(work):
        v = jnp.concatenate([tab[t0, :, H:], tab[t1, :, H:]], axis=0)
        o = dot(p_ref[i * BLOCK : (i + 1) * BLOCK], v)
        outs[j][half * BLOCK : (half + 1) * BLOCK, h * H : (h + 1) * H] = o.astype(BF)


def attend(sc, q, tab_m, tab_o):
    return call(
        attend_kernel, sc, (q, tab_m, tab_o), [whole(q), whole(tab_m), whole(tab_o)],
        [((SEQ_LEN, 256), BF)] * 4, [fixed(SEQ_LEN, 256)] * 4,
        scratch=[pltpu.VMEM((16 * BLOCK, BLOCK), F32), pltpu.VMEM((16 * BLOCK, BLOCK), BF)],
        flops=10**9, bytes_=5 * 2**20,
    )


def finish_kernel(branch, sc, *refs):
    sides = (refs[0:5], refs[5:10])
    parts, logits = refs[10:14], refs[14]
    if branch == 0:
        before, (out, w, sems) = None, refs[15:]
    else:
        before, (out, w, sems) = refs[15], refs[16:]
    copies = []
    for side in range(2):
        own, e, r1, r2, r3 = sides[side]
        base = side * 128
        copies.append((own, w.at[0, pl.ds(base, 128)]))
        for src, back in ((e, 0), (r1, 3), (r2, 1), (r3, 2)):
            quarter = lax.rem(sc[side] + back, 4)
            row = pl.multiple_of(base + quarter * 32, 32)
            for d in range(3):
                copies.append(
                    (src.at[pl.ds(d * 64 + branch * 32, 32)], w.at[1 + d, pl.ds(row, 32)])
                )
    copies = [pltpu.make_async_copy(a, b, sems.at[n]) for n, (a, b) in enumerate(copies)]
    for c in copies:
        c.start()
    mix = jax.nn.sigmoid(logits[:, branch : branch + 1])
    for c in copies:
        c.wait()

    def step(i, carry):
        cols = pl.ds(pl.multiple_of(i * 512, 512), 512)
        acc = None
        for d in range(4):
            a = dot(parts[d][...], w[d, :, cols])
            acc = a if acc is None else acc + a
        if before is None:
            out[:, cols] = mix * acc
        else:
            out[:, cols] = (before[:, cols] + mix * acc).astype(BF)
        return carry

    lax.fori_loop(0, 4, step, 0)


def finish(branch, sc, mine, other, parts, logits, before=None):
    width = mine[0].shape[1]
    vm = list(parts) + [logits] + ([] if before is None else [before])
    return call(
        functools.partial(finish_kernel, branch), sc, (*mine, *other, *vm),
        [HBM] * 10 + [whole(a) for a in vm],
        [((SEQ_LEN, width), F32 if before is None else BF)], [fixed(SEQ_LEN, width)],
        scratch=[pltpu.VMEM((4, 256, width), BF), pltpu.SemaphoreType.DMA((26,))],
        flops=SEQ_LEN * 2048 * 2048, bytes_=7 * 2**20,
    )[0]


def local(
    tokens,
    store,
    passage_holder_index,
    passage_slot,
    query_weight,
    key_matrix,
    value_weight,
    outer_gate,
    inner_gate,
    conv_input,
    conv_taps,
    route_gate_projection,
    conv_out,
    memory_out,
):
    me = lax.axis_index("tp")
    st = lax.axis_index("st")
    y, c = me // 2, me % 2
    z, x = st // N_X, st % N_X
    KS = tokens.shape[1]
    HW = query_weight.shape[1]
    i32 = jnp.int32

    quarter = jnp.where(c == 0, x, z)
    quarter_other = jnp.where(c == 0, z, x)
    sc_quarter = jnp.stack([quarter, quarter_other]).astype(i32)
    part = weight_part(sc_quarter, conv_out, memory_out)
    ys = [shift(part, s) for s in (1, -1, 2)]
    e = pack(sc_quarter, ys)
    ring = [e, plane(e, 1), plane(e, -1), plane(e, 2)]
    ring_other = [swap(a) for a in ring]
    conv_out_other, memory_out_other = swap(conv_out), swap(memory_out)

    owners = passage_holder_index.reshape(-1)
    local_slots = passage_slot.reshape(-1)
    owner_count = lax.axis_size("st")
    request_count = owners.shape[0]
    capacity = max(2, 2 * request_count // owner_count)
    one_hot = (owners[:, None] == jnp.arange(owner_count, dtype=i32)[None, :]).astype(i32)
    before = jnp.cumsum(one_hot, axis=0) - one_hot
    position = jnp.sum(before * one_hot, axis=1)
    target = owners * capacity + position
    matches = (target[:, None] == jnp.arange(owner_count * capacity, dtype=i32)[None, :]).astype(i32)
    outgoing = jnp.sum(matches * local_slots[:, None], axis=0).reshape(owner_count, capacity)
    wanted = lax.all_to_all(outgoing, "st", split_axis=0, concat_axis=0)

    rows = tokens.reshape(N_Y, 2, SEQ_LEN, KS)
    h0 = pick(rows, c, 1).reshape(N_Y * SEQ_LEN, KS)
    other = pick(rows, 1 - c, 1).reshape(N_Y * SEQ_LEN, KS)
    a0, b0 = shift(h0, 1), shift(h0, -1)
    h1 = swap(other)
    a1, b1 = shift(h1, 1), shift(h1, -1)
    c0, c1 = shift(a0, 1), shift(b1, -1)
    pieces = (h0, h1, a0, b0, a1, b1, c0, c1)

    def slice_of(dy, flip):
        return 2 * ((y + dy) % N_Y) + (1 - c if flip else c)

    flips = ((0, False), (0, True), (-1, False), (1, False), (-1, True), (1, True), (2, False), (2, True))
    yord = [(y + d) % N_Y for d in (2, 1, -1, 0)]
    sc_project = jnp.stack([slice_of(*f) for f in flips] + yord).astype(i32)

    chosen = serve(wanted, store, key_matrix, value_weight)
    served = lax.all_to_all(chosen, "st", split_axis=0, concat_axis=0)
    tab_m = served.reshape(owner_count * capacity, PLEN, 2 * HW)
    tab_o = swap(tab_m)
    mine = pick(target.reshape(N_Y, 2, -1), c, 1).reshape(-1)
    sc_attend = jnp.concatenate([mine, jnp.stack(yord)]).astype(i32)

    w_mine = [query_weight, outer_gate, inner_gate, conv_input]
    weights = w_mine + [swap(w) for w in w_mine]
    taps_part = swap(conv_taps)
    gate = route_gate_projection.T

    acc, logits = project1(sc_project, pieces[:6], weights, gate)
    q, *convs, logits = project2(
        sc_project, pieces[6:], acc, weights, gate, conv_taps, taps_part, logits
    )
    conv_all = [convs[3], shift(convs[1], 1), shift(convs[2], -1), shift(convs[0], 2)]
    half = finish(0, sc_quarter, [conv_out] + ring, [conv_out_other] + ring_other, conv_all, logits)
    mems = attend(sc_attend, q, tab_m, tab_o)
    mem_all = [mems[3], shift(mems[1], 1), shift(mems[2], -1), shift(mems[0], 2)]
    return finish(
        1, sc_quarter, [memory_out] + ring, [memory_out_other] + ring_other, mem_all, logits, half
    )


def solution(mesh):
    return jax.shard_map(
        local,
        mesh=mesh,
        in_specs=(
            P("st", "tp"),
            P("st", None, None),
            P("st", None),
            P("st", None),
            P(None, "tp"),
            P(None, "tp"),
            P(None, "tp"),
            P(None, "tp"),
            P(None, "tp"),
            P(None, "tp"),
            P(None, "tp"),
            P(),
            P("tp", None),
            P("tp", None),
        ),
        out_specs=P(("st", "tp"), None),
        check_vma=False,
    )
```

time: 159 us -> 159 us (level)
  Pallas kernels: 25 us -> 53.3 us
  local copies, waits for them, and re-layouts: 33.5 us -> 6.71 us
  starting transfers between devices: 54.8 us -> 37.7 us
  blocking collectives: 0 us -> 14.8 us
  waiting for transfers between devices: 36.1 us -> 44.1 us
  matrix products: 5.77 us -> 0 us
    pallas_call x3 -> x8, Pallas kernels: 25 us -> 53.3 us  [call(): pl.pallas_call(body, grid_spec=pltpu.PrefetchScalarGridSpec(num_scalar_pr...]
    unnamed x57 -> x46, local copies, waits for them, and re-layouts: 22 us -> 3.81 us
    all_to_all x0 -> x1, blocking collectives: none -> 14.8 us  [local(): wanted = lax.all_to_all(outgoing, 'st', split_axis=0, concat_axis=0)]
    ppermute x15, waiting for transfers between devices: 31 us -> 43.2 us  [shift(): return lax.ppermute(a, 'tp', SHIFT[s])]
    all_to_all x2 -> x1, starting transfers between devices: 15 us -> 4.6 us  [local(): served = lax.all_to_all(chosen, 'st', split_axis=0, concat_axis=0)]
    ppermute x15, starting transfers between devices: 21.5 us -> 13 us  [shift(): return lax.ppermute(a, 'tp', SHIFT[s])]
    dot_general x1 -> x0, matrix products: 5.77 us -> none  [dot(): return jnp.dot(a, b, preferred_element_type=F32)]
    ppermute x3, waiting for transfers between devices: 5.11 us -> 0.01 us  [plane(): return lax.ppermute(a, ('st', 'tp'), plane_shift(s))]
  transfers between devices with their start and end apart: 29 -> 32, of which waited for: 8 -> 11; matrix products, arithmetic and copies ran while one was open for 14% -> 2% of each run, Pallas kernels for 11% -> 22%
where the time goes in v2:
time: 159 us; the launch traced here: 158 us
  Pallas kernels  53.3 us (34%)
  waiting for transfers between devices  44.1 us (28%)
  starting transfers between devices  37.7 us (24%)
  blocking collectives  14.8 us (9%)
  local copies, waits for them, and re-layouts  6.71 us (4%)
    pallas_call x8, Pallas kernels, call(): pl.pallas_call(body, grid_spec=pltpu.PrefetchScalarGridSpec(num_scalar_pr...  53.3 us
    ppermute x15, waiting for transfers between devices, shift(): return lax.ppermute(a, 'tp', SHIFT[s])  43.2 us
    all_to_all x1, blocking collectives, local(): wanted = lax.all_to_all(outgoing, 'st', split_axis=0, concat_axis=0)  14.8 us
    ppermute x15, starting transfers between devices, shift(): return lax.ppermute(a, 'tp', SHIFT[s])  13 us
    ppermute x13, starting transfers between devices, swap(): return lax.ppermute(a, 'tp', SWAP)  12.9 us
    ppermute x3, starting transfers between devices, plane(): return lax.ppermute(a, ('st', 'tp'), plane_shift(s))  7.24 us
    all_to_all x1, starting transfers between devices, local(): served = lax.all_to_all(chosen, 'st', split_axis=0, concat_axis=0)  4.6 us
    unnamed x46, local copies, waits for them, and re-layouts  3.81 us
  transfers between devices with their start and end apart: 32, of which 11 were waited for; matrix products, arithmetic and copies ran while one was open for 2% of the time, Pallas kernels for 22%

profile of v2, /device:TPU:1, one launch (start us, length us, event | category | flops | bytes accessed | tf_op | source)
XLA Modules:
  0.0 158.2 jit_solution(11367531564596470648)
XLA Ops:
  0.0 0.8 copy.38
  1.2 0.8 copy.41
  2.2 14.8 %all_to_all.16 = s32[16,1,4]{2,1,0:T(1,128)} all-to-all(s32[16,1,4]{2,1,0:T(1,128)S(1)} %bitcast.32), channel_id=1, replica_groups=mesh['st'=16,'tp'=8] {'st'}, dimensions={0} | all-to-all | bytes 512 | tf_op jit(solution)/shard_map/all_to_all | solution.py:408
  17.0 10.6 %shard_map.140 = bf16[16,4,64,256]{3,2,1,0:T(8,128)(2,1)} custom-call(s32[16,4]{1,0:T(8,128)} %bitcast.31, bf16[2048,2048]{1,0:T(8,128)(2,1)} %bitcast.26, bf16[2048,128]{1,0:T(8,128)(2,1)} %kw.1, bf16[2048,128]{1,0:T(8,128)(2,1)} %vw.1), custom_call_target="tpu_custom_call" | custom-call | flops 2147483648 | bytes 11534336 | tf_op jit(solution)/shard_map/pallas_call | solution.py:60
  27.6 4.6 %all-to-all-start.1 = ((bf16[16,4,64,256]{3,2,1,0:T(8,128)(2,1)}), bf16[16,4,64,256]{3,2,1,0:T(8,128)(2,1)}, u32[]{:S(2)}, u32[]{:S(2)}) async-start(bf16[16,4,64,256]{3,2,1,0:T(8,128)(2,1)} %shard_map.140), calls=%async_computation.1 | async-start | bytes 4194304 | tf_op jit(solution)/shard_map/all_to_all | solution.py:427
  32.3 1.0 constant_dynamic-slice_fusion
  33.3 2.0 %collective-permute-start.13 = (bf16[1024,256]{1,0:T(8,128)(2,1)}, bf16[1024,256]{1,0:T(8,128)(2,1)}, u32[]{:S(2)}, u32[]{:S(2)}) collective-permute-start(bf16[1024,256]{1,0:T(8,128)(2,1)} %bitcast.16), channel_id=1, source_target_pairs={{0,1},{1,0},{2,3},{3,2},{4,5},{5,4},{6,7},{7,6},{8,9},{9,8},{10,11... | collective-permute-start | bytes 1572872 | tf_op jit(solution)/shard_map/ppermute | solution.py:44
  35.9 2.4 %shard_map.136 = bf16[64,2048]{1,0:T(8,128)(2,1)} custom-call(s32[2]{0:T(128)} %pad_add_fusion.sc, bf16[128,2048]{1,0:T(8,128)(2,1)} %refs_0_.2, bf16[128,2048]{1,0:T(8,128)(2,1)} %refs_0_.3), custom_call_target="tpu_custom_call" | custom-call | flops 100000000 | bytes 524288 | tf_op jit(solution)/shard_map/pallas_call | solution.py:60
  38.3 1.3 collective-permute-start
  39.5 1.4 collective-permute-start.1
  41.0 1.6 %collective-permute-start.2 = (bf16[64,2048]{1,0:T(8,128)(2,1)}, bf16[64,2048]{1,0:T(8,128)(2,1)S(1)}, u32[]{:S(2)}, u32[]{:S(2)}) collective-permute-start(bf16[64,2048]{1,0:T(8,128)(2,1)} %shard_map.136), channel_id=1, source_target_pairs={{0,4},{1,5},{2,6},{3,7},{4,0},{5,1},{6,2},{7,3},{8,12},{9,13},{10,... | collective-permute-start | bytes 786440 | tf_op jit(solution)/shard_map/ppermute | solution.py:40
  42.6 0.8 collective-permute-start.22
  43.5 0.8 collective-permute-done.22.refs_13_
  44.7 3.0 %collective-permute-done.a = bf16[64,2048]{1,0:T(8,128)(2,1)S(1)} collective-permute-done((bf16[64,2048]{1,0:T(8,128)(2,1)}, bf16[64,2048]{1,0:T(8,128)(2,1)S(1)}, u32[]{:S(2)}, u32[]{:S(2)}) %collective-permute-start) | collective-permute-done | bytes 262176 | tf_op jit(solution)/shard_map/ppermute | solution.py:40
  47.7 1.4 collective-permute-start.16
  49.2 1.6 collective-permute-start.18
  50.7 3.8 %collective-permute-done.2.c = bf16[64,2048]{1,0:T(8,128)(2,1)S(1)} collective-permute-done((bf16[64,2048]{1,0:T(8,128)(2,1)}, bf16[64,2048]{1,0:T(8,128)(2,1)S(1)}, u32[]{:S(2)}, u32[]{:S(2)}) %collective-permute-start.2) | collective-permute-done | bytes 262176 | tf_op jit(solution)/shard_map/ppermute | solution.py:40
  54.5 1.2 collective-permute-start.19
  55.9 8.8 %collective-permute-done.11.refs_2_ = bf16[1024,256]{1,0:T(8,128)(2,1)S(1)} collective-permute-done((bf16[1024,256]{1,0:T(8,128)(2,1)}, bf16[1024,256]{1,0:T(8,128)(2,1)S(1)}, u32[]{:S(2)}, u32[]{:S(2)}) %collective-permute-start.11) | collective-permute-done | bytes 524320 | tf_op jit(solution)/shard_map/ppermute | solution.py:40
  64.7 1.0 collective-permute-start.21
  65.8 0.7 copy-done.21
  66.7 0.8 copy-done.6
  67.4 2.1 %collective-permute-start.14 = (bf16[1024,256]{1,0:T(8,128)(2,1)}, bf16[1024,256]{1,0:T(8,128)(2,1)}, u32[]{:S(2)}, u32[]{:S(2)}) collective-permute-start(bf16[1024,256]{1,0:T(8,128)(2,1)} %collective-permute-done.13.refs_1_), channel_id=1, source_target_pairs={{0,6},{1,7},{2,0},{3,1},{4,2},{5,3},{6,4},{7,5},{8,14},{9,15},{10,... | collective-permute-start | bytes 1572872 | tf_op jit(solution)/shard_map/ppermute | solution.py:40
  69.6 2.7 %shard_map.137.refs_1_ = bf16[192,2048]{1,0:T(8,128)(2,1)} custom-call(s32[2]{0:T(128)} %pad_add_fusion.sc, bf16[64,2048]{1,0:T(8,128)(2,1)} %copy-done.8, bf16[64,2048]{1,0:T(8,128)(2,1)} %copy-done.9, bf16[64,2048]{1,0:T(8,128)(2,1)} %copy-done.10), custom_call_target="tpu_custom_call" | custom-call | flops 100000000 | bytes 1048576 | tf_op jit(solution)/shard_map/pallas_call | solution.py:60
  72.3 3.0 %collective-permute-start.5 = (bf16[192,2048]{1,0:T(8,128)(2,1)}, bf16[192,2048]{1,0:T(8,128)(2,1)S(1)}, u32[]{:S(2)}, u32[]{:S(2)}) collective-permute-start(bf16[192,2048]{1,0:T(8,128)(2,1)} %shard_map.137.refs_1_), channel_id=1, source_target_pairs={{0,16},{1,65},{2,18},{3,67},{4,20},{5,69},{6,22},{7,71},{8,24},{9,... | collective-permute-start | bytes 2359304 | tf_op jit(solution)/shard_map/ppermute | solution.py:48
  75.3 0.7 collective-permute-start.12
  76.1 5.1 %collective-permute-done.14.refs_5_ = bf16[1024,256]{1,0:T(8,128)(2,1)} collective-permute-done((bf16[1024,256]{1,0:T(8,128)(2,1)}, bf16[1024,256]{1,0:T(8,128)(2,1)}, u32[]{:S(2)}, u32[]{:S(2)}) %collective-permute-start.14) | collective-permute-done | bytes 524320 | tf_op jit(solution)/shard_map/ppermute | solution.py:40
  81.2 1.5 collective-permute-start.3
  82.6 1.7 %collective-permute-done.17.refs_4_ = bf16[1024,256]{1,0:T(8,128)(2,1)} collective-permute-done((bf16[1024,256]{1,0:T(8,128)(2,1)}, bf16[1024,256]{1,0:T(8,128)(2,1)}, u32[]{:S(2)}, u32[]{:S(2)}) %collective-permute-start.17) | collective-permute-done | bytes 524320 | tf_op jit(solution)/shard_map/ppermute | solution.py:40
  84.3 2.7 %collective-permute-start.4 = (bf16[192,2048]{1,0:T(8,128)(2,1)}, bf16[192,2048]{1,0:T(8,128)(2,1)}, u32[]{:S(2)}, u32[]{:S(2)}) collective-permute-start(bf16[192,2048]{1,0:T(8,128)(2,1)} %shard_map.137.refs_1_), channel_id=1, source_target_pairs={{0,24},{1,97},{2,26},{3,99},{4,28},{5,101},{6,30},{7,103},{8,0},{9... | collective-permute-start | bytes 2359304 | tf_op jit(solution)/shard_map/ppermute | solution.py:48
  87.1 8.4 %collective-permute-done.12.refs_0_ = bf16[1024,256]{1,0:T(8,128)(2,1)S(1)} collective-permute-done((bf16[1024,256]{1,0:T(8,128)(2,1)}, bf16[1024,256]{1,0:T(8,128)(2,1)S(1)}, u32[]{:S(2)}, u32[]{:S(2)}) %collective-permute-start.12) | collective-permute-done | bytes 524320 | tf_op jit(solution)/shard_map/ppermute | solution.py:40
  95.4 1.2 collective-permute-start.7
  96.8 0.7 stack.67.sc
  97.5 0.7 collective-permute-start.10
  98.2 0.8 collective-permute-start.8
  99.0 10.1 %shard_map.138 = (f32[1024,1024]{1,0:T(8,128)}, f32[256,2]{1,0:T(8,128)}) custom-call(s32[12]{0:T(128)} %stack.67.sc, bf16[1024,256]{1,0:T(8,128)(2,1)} %bitcast.30, bf16[1024,256]{1,0:T(8,128)(2,1)} %collective-permute-done.13.refs_1_, bf16[1024,256]{1,0:T(8,128)(2,1)} %copy-done.20, bf16[1024,256]{1,0:T(8,128)(2,1)} %copy-done.21, ...), custom_call_target="tpu_custom_call" | custom-call | flops 3221225472 | bytes 10485760 | tf_op jit(solution)/shard_map/pallas_call | solution.py:60
  109.7 1.6 collective-permute-start.9
  111.3 7.7 %shard_map.139 = (bf16[1024,256]{1,0:T(8,128)(2,1)}, bf16[256,256]{1,0:T(8,128)(2,1)}, bf16[256,256]{1,0:T(8,128)(2,1)}, bf16[256,256]{1,0:T(8,128)(2,1)}, bf16[256,256]{1,0:T(8,128)(2,1)}, /*index=5*/f32[256,2]{1,0:T(8,128)}) custom-call(s32[12]{0:T(128)} %stack.67.sc, bf16[1024,256]{1,0:T(8,128)(2,1)} %copy-done.7, ...), custom_call_target="tpu_custom_call" | custom-call | flops 1073741824 | bytes 8388608 | tf_op jit(solution)/shard_map/pallas_call | solution.py:60
  119.3 6.5 %collective-permute-done.28.refs_11_ = bf16[256,256]{1,0:T(8,128)(2,1)S(1)} collective-permute-done((bf16[256,256]{1,0:T(8,128)(2,1)}, bf16[256,256]{1,0:T(8,128)(2,1)S(1)}, u32[]{:S(2)}, u32[]{:S(2)}) %collective-permute-start.28) | collective-permute-done | bytes 131104 | tf_op jit(solution)/shard_map/ppermute | solution.py:40
  125.8 4.4 %collective-permute-done.29.refs_12_ = bf16[256,256]{1,0:T(8,128)(2,1)S(1)} collective-permute-done((bf16[256,256]{1,0:T(8,128)(2,1)}, bf16[256,256]{1,0:T(8,128)(2,1)S(1)}, u32[]{:S(2)}, u32[]{:S(2)}) %collective-permute-start.29) | collective-permute-done | bytes 131104 | tf_op jit(solution)/shard_map/ppermute | solution.py:40
  130.2 1.7 %collective-permute-start.6 = (bf16[128,2048]{1,0:T(8,128)(2,1)}, bf16[128,2048]{1,0:T(8,128)(2,1)}, u32[]{:S(2)}, u32[]{:S(2)}) collective-permute-start(bf16[128,2048]{1,0:T(8,128)(2,1)} %refs_0_.3), channel_id=1, source_target_pairs={{0,1},{1,0},{2,3},{3,2},{4,5},{5,4},{6,7},{7,6},{8,9},{9,8},{10,11... | collective-permute-start | bytes 1572872 | tf_op jit(solution)/shard_map/ppermute | solution.py:44
  132.9 4.8 %shard_map.141 = (bf16[256,256]{1,0:T(8,128)(2,1)}, bf16[256,256]{1,0:T(8,128)(2,1)}, bf16[256,256]{1,0:T(8,128)(2,1)}, bf16[256,256]{1,0:T(8,128)(2,1)}) custom-call(s32[20]{0:T(128)} %concatenate.3.sc, bf16[1024,256]{1,0:T(8,128)(2,1)} %get-tuple-element.19.q, bf16[64,64,256]{2,1,0:T(8,128)(2,1)} %bitcast.21.tab_m, ...), custom_call_target="tpu_custom_call" | custom-call | flops 1000000000 | bytes 5242880 | tf_op jit(solution)/shard_map/pallas_call | solution.py:60
  137.7 0.9 collective-permute-done.30.refs_13_
  138.6 0.9 collective-permute-start.24
  139.6 1.7 %collective-permute-start.25 = (bf16[256,256]{1,0:T(8,128)(2,1)}, bf16[256,256]{1,0:T(8,128)(2,1)S(1)}, u32[]{:S(2)}, u32[]{:S(2)}) collective-permute-start(bf16[256,256]{1,0:T(8,128)(2,1)} %get-tuple-element.22), channel_id=1, source_target_pairs={{0,6},{1,7},{2,0},{3,1},{4,2},{5,3},{6,4},{7,5},{8,14},{9,15},{10,... | collective-permute-start | bytes 393224 | tf_op jit(solution)/shard_map/ppermute | solution.py:40
  141.3 0.9 collective-permute-start.26
  142.2 7.3 %shard_map.142.refs_15_ = f32[256,2048]{1,0:T(8,128)} custom-call(s32[2]{0:T(128)} %pad_add_fusion.sc, bf16[128,2048]{1,0:T(8,128)(2,1)} %refs_0_.2, bf16[192,2048]{1,0:T(8,128)(2,1)} %shard_map.137.refs_1_, bf16[192,2048]{1,0:T(8,128)(2,1)} %copy-done.1, bf16[192,2048]{1,0:T(8,128)(2,1)} %collective-permute-done.4.refs_3_, bf16[192,2048]{1,0:T(8,128)(2,1)} %copy-done, ...), custom_call_target="tpu_custom_call" | custom-call | flops 1073741824 | bytes 7340032 | tf_op jit(solution)/shard_map/pallas_call | solution.py:60
  150.3 7.7 %shard_map.143 = bf16[256,2048]{1,0:T(8,128)(2,1)} custom-call(s32[2]{0:T(128)} %pad_add_fusion.sc, bf16[128,2048]{1,0:T(8,128)(2,1)} %refs_0_.3, bf16[192,2048]{1,0:T(8,128)(2,1)} %shard_map.137.refs_1_, bf16[192,2048]{1,0:T(8,128)(2,1)} %copy-done.1, bf16[192,2048]{1,0:T(8,128)(2,1)} %collective-permute-done.4.refs_3_, bf16[192,2048]{1,0:T(8,128)(2,1)} %copy-done, ...), custom_call_target="tpu_custom_call" | custom-call | flops 1073741824 | bytes 7340032 | tf_op jit(solution)/shard_map/pallas_call | solution.py:60
  (89 shorter events, 4.8 us)
Async XLA Ops:
  27.6 4.7 %copy-start.3 = (bf16[2048,256]{1,0:T(8,128)(2,1)S(1)}, bf16[2048,256]{1,0:T(8,128)(2,1)}, u32[]{:S(2)}) copy-start(bf16[2048,256]{1,0:T(8,128)(2,1)} %param.14) | copy-start | bytes 3145732
  27.6 38.9 %all-to-all-start.1 = ((bf16[16,4,64,256]{3,2,1,0:T(8,128)(2,1)}), bf16[16,4,64,256]{3,2,1,0:T(8,128)(2,1)}, u32[]{:S(2)}, u32[]{:S(2)}) async-start(bf16[16,4,64,256]{3,2,1,0:T(8,128)(2,1)} %shard_map.140), calls=%async_computation.1 | async-start | bytes 4194304 | tf_op jit(solution)/shard_map/all_to_all | solution.py:427
  32.2 10.4 %copy-start.18 = (bf16[3,128]{1,0:T(4,128)(2,1)S(1)}, bf16[3,128]{1,0:T(4,128)(2,1)}, u32[]{:S(2)}) copy-start(bf16[3,128]{1,0:T(4,128)(2,1)} %refs_12_.1) | copy-start | bytes 2308
  32.2 17.0 %copy-start.4 = (bf16[2048,128]{1,0:T(8,128)(2,1)S(1)}, bf16[2048,128]{1,0:T(8,128)(2,1)}, u32[]{:S(2)}) copy-start(bf16[2048,128]{1,0:T(8,128)(2,1)} %refs_3_.1) | copy-start | bytes 1572868
  32.2 22.3 %copy-start.5 = (bf16[2048,128]{1,0:T(8,128)(2,1)S(1)}, bf16[2048,128]{1,0:T(8,128)(2,1)}, u32[]{:S(2)}) copy-start(bf16[2048,128]{1,0:T(8,128)(2,1)} %refs_4_.1) | copy-start | bytes 1572868
  32.2 33.5 %copy-start.2 = (bf16[128,2048]{1,0:T(8,128)(2,1)S(1)}, bf16[128,2048]{1,0:T(8,128)(2,1)}, u32[]{:S(2)}) copy-start(bf16[128,2048]{1,0:T(8,128)(2,1)} %refs_0_.2) | copy-start | bytes 1572868
  33.3 22.5 %collective-permute-start.13 = (bf16[1024,256]{1,0:T(8,128)(2,1)}, bf16[1024,256]{1,0:T(8,128)(2,1)}, u32[]{:S(2)}, u32[]{:S(2)}) collective-permute-start(bf16[1024,256]{1,0:T(8,128)(2,1)} %bitcast.16), channel_id=1, source_target_pairs={{0,1},{1,0},{2,3},{3,2},{4,5},{5,4},{6,7},{7,6},{8,9},{9,8},{10,11... | collective-permute-start | bytes 1572872 | tf_op jit(solution)/shard_map/ppermute | solution.py:44
  38.3 9.4 %collective-permute-start = (bf16[64,2048]{1,0:T(8,128)(2,1)}, bf16[64,2048]{1,0:T(8,128)(2,1)S(1)}, u32[]{:S(2)}, u32[]{:S(2)}) collective-permute-start(bf16[64,2048]{1,0:T(8,128)(2,1)} %shard_map.136), channel_id=1, source_target_pairs={{0,2},{1,3},{2,4},{3,5},{4,6},{5,7},{6,0},{7,1},{8,10},{9,11},{10,... | collective-permute-start | bytes 786440 | tf_op jit(solution)/shard_map/ppermute | solution.py:40
  39.5 9.6 %collective-permute-start.1 = (bf16[64,2048]{1,0:T(8,128)(2,1)}, bf16[64,2048]{1,0:T(8,128)(2,1)S(1)}, u32[]{:S(2)}, u32[]{:S(2)}) collective-permute-start(bf16[64,2048]{1,0:T(8,128)(2,1)} %shard_map.136), channel_id=1, source_target_pairs={{0,6},{1,7},{2,0},{3,1},{4,2},{5,3},{6,4},{7,5},{8,14},{9,15},{10,... | collective-permute-start | bytes 786440 | tf_op jit(solution)/shard_map/ppermute | solution.py:40
  41.0 13.6 %collective-permute-start.2 = (bf16[64,2048]{1,0:T(8,128)(2,1)}, bf16[64,2048]{1,0:T(8,128)(2,1)S(1)}, u32[]{:S(2)}, u32[]{:S(2)}) collective-permute-start(bf16[64,2048]{1,0:T(8,128)(2,1)} %shard_map.136), channel_id=1, source_target_pairs={{0,4},{1,5},{2,6},{3,7},{4,0},{5,1},{6,2},{7,3},{8,12},{9,13},{10,... | collective-permute-start | bytes 786440 | tf_op jit(solution)/shard_map/ppermute | solution.py:40
  42.6 1.7 %collective-permute-start.22 = (bf16[3,128]{1,0:T(4,128)(2,1)S(1)}, bf16[3,128]{1,0:T(4,128)(2,1)S(1)}, u32[]{:S(2)}, u32[]{:S(2)}) collective-permute-start(bf16[3,128]{1,0:T(4,128)(2,1)S(1)} %copy-done.18), channel_id=1, source_target_pairs={{0,1},{1,0},{2,3},{3,2},{4,5},{5,4},{6,7},{7,6},{8,9},{9,8},{10,11... | collective-permute-start | bytes 2312 | tf_op jit(solution)/shard_map/ppermute | solution.py:44
  44.3 64.8 %copy-start.19 = (bf16[3,128]{1,0:T(4,128)(2,1)}, bf16[3,128]{1,0:T(4,128)(2,1)S(1)}, u32[]{:S(2)}) copy-start(bf16[3,128]{1,0:T(4,128)(2,1)S(1)} %collective-permute-done.22.refs_13_) | copy-start | bytes 2308
  44.3 20.4 %collective-permute-start.11 = (bf16[1024,256]{1,0:T(8,128)(2,1)}, bf16[1024,256]{1,0:T(8,128)(2,1)S(1)}, u32[]{:S(2)}, u32[]{:S(2)}) collective-permute-start(bf16[1024,256]{1,0:T(8,128)(2,1)} %bitcast.28), channel_id=1, source_target_pairs={{0,2},{1,3},{2,4},{3,5},{4,6},{5,7},{6,0},{7,1},{8,10},{9,11},{10,... | collective-permute-start | bytes 1572872 | tf_op jit(solution)/shard_map/ppermute | solution.py:40
  47.7 21.9 %copy-start.8 = (bf16[64,2048]{1,0:T(8,128)(2,1)}, bf16[64,2048]{1,0:T(8,128)(2,1)S(1)}, u32[]{:S(2)}) copy-start(bf16[64,2048]{1,0:T(8,128)(2,1)S(1)} %collective-permute-done.a) | copy-start | bytes 786436
  47.7 18.0 %collective-permute-start.16 = (bf16[1024,256]{1,0:T(8,128)(2,1)}, bf16[1024,256]{1,0:T(8,128)(2,1)S(1)}, u32[]{:S(2)}, u32[]{:S(2)}) collective-permute-start(bf16[1024,256]{1,0:T(8,128)(2,1)} %bitcast.29), channel_id=1, source_target_pairs={{0,6},{1,7},{2,0},{3,1},{4,2},{5,3},{6,4},{7,5},{8,14},{9,15},{10,... | collective-permute-start | bytes 1572872 | tf_op jit(solution)/shard_map/ppermute | solution.py:40
  49.2 16.6 %copy-start.9 = (bf16[64,2048]{1,0:T(8,128)(2,1)}, bf16[64,2048]{1,0:T(8,128)(2,1)S(1)}, u32[]{:S(2)}) copy-start(bf16[64,2048]{1,0:T(8,128)(2,1)S(1)} %collective-permute-done.1.b) | copy-start | bytes 786436
  49.2 17.3 %collective-permute-start.18 = (bf16[2048,128]{1,0:T(8,128)(2,1)S(1)}, bf16[2048,128]{1,0:T(8,128)(2,1)}, u32[]{:S(2)}, u32[]{:S(2)}) collective-permute-start(bf16[2048,128]{1,0:T(8,128)(2,1)S(1)} %copy-done.4), channel_id=1, source_target_pairs={{0,1},{1,0},{2,3},{3,2},{4,5},{5,4},{6,7},{7,6},{8,9},{9,8},{10,11... | collective-permute-start | bytes 1572872 | tf_op jit(solution)/shard_map/ppermute | solution.py:44
  54.5 11.2 %copy-start.10 = (bf16[64,2048]{1,0:T(8,128)(2,1)}, bf16[64,2048]{1,0:T(8,128)(2,1)S(1)}, u32[]{:S(2)}) copy-start(bf16[64,2048]{1,0:T(8,128)(2,1)S(1)} %collective-permute-done.2.c) | copy-start | bytes 786436
  54.5 12.1 %collective-permute-start.19 = (bf16[2048,128]{1,0:T(8,128)(2,1)S(1)}, bf16[2048,128]{1,0:T(8,128)(2,1)S(1)}, u32[]{:S(2)}, u32[]{:S(2)}) collective-permute-start(bf16[2048,128]{1,0:T(8,128)(2,1)S(1)} %copy-done.5), channel_id=1, source_target_pairs={{0,1},{1,0},{2,3},{3,2},{4,5},{5,4},{6,7},{7,6},{8,9},{9,8},{10,11... | collective-permute-start | bytes 1572872 | tf_op jit(solution)/shard_map/ppermute | solution.py:44
  55.8 13.8 %collective-permute-start.20 = (bf16[2048,128]{1,0:T(8,128)(2,1)}, bf16[2048,128]{1,0:T(8,128)(2,1)}, u32[]{:S(2)}, u32[]{:S(2)}) collective-permute-start(bf16[2048,128]{1,0:T(8,128)(2,1)} %refs_5_.1), channel_id=1, source_target_pairs={{0,1},{1,0},{2,3},{3,2},{4,5},{5,4},{6,7},{7,6},{8,9},{9,8},{10,11... | collective-permute-start | bytes 1572872 | tf_op jit(solution)/shard_map/ppermute | solution.py:44
  64.7 4.9 %copy-start.20 = (bf16[1024,256]{1,0:T(8,128)(2,1)}, bf16[1024,256]{1,0:T(8,128)(2,1)S(1)}, u32[]{:S(2)}) copy-start(bf16[1024,256]{1,0:T(8,128)(2,1)S(1)} %collective-permute-done.11.refs_2_) | copy-start | bytes 1572868
  64.7 7.6 %collective-permute-start.21 = (bf16[2048,128]{1,0:T(8,128)(2,1)}, bf16[2048,128]{1,0:T(8,128)(2,1)}, u32[]{:S(2)}, u32[]{:S(2)}) collective-permute-start(bf16[2048,128]{1,0:T(8,128)(2,1)} %refs_6_.3), channel_id=1, source_target_pairs={{0,1},{1,0},{2,3},{3,2},{4,5},{5,4},{6,7},{7,6},{8,9},{9,8},{10,11... | collective-permute-start | bytes 1572872 | tf_op jit(solution)/shard_map/ppermute | solution.py:44
  65.7 9.7 %collective-permute-start.27 = (bf16[128,2048]{1,0:T(8,128)(2,1)S(1)}, bf16[128,2048]{1,0:T(8,128)(2,1)}, u32[]{:S(2)}, u32[]{:S(2)}) collective-permute-start(bf16[128,2048]{1,0:T(8,128)(2,1)S(1)} %copy-done.2), channel_id=1, source_target_pairs={{0,1},{1,0},{2,3},{3,2},{4,5},{5,4},{6,7},{7,6},{8,9},{9,8},{10,11... | collective-permute-start | bytes 1572872 | tf_op jit(solution)/shard_map/ppermute | solution.py:44
  66.5 65.4 %collective-permute-start.23 = (bf16[64,64,256]{2,1,0:T(8,128)(2,1)}, bf16[64,64,256]{2,1,0:T(8,128)(2,1)}, u32[]{:S(2)}, u32[]{:S(2)}) collective-permute-start(bf16[64,64,256]{2,1,0:T(8,128)(2,1)} %bitcast.21.tab_m), channel_id=1, source_target_pairs={{0,1},{1,0},{2,3},{3,2},{4,5},{5,4},{6,7},{7,6},{8,9},{9,8},{10,11... | collective-permute-start | bytes 6291464 | tf_op jit(solution)/shard_map/ppermute | solution.py:44
  67.4 13.7 %collective-permute-start.14 = (bf16[1024,256]{1,0:T(8,128)(2,1)}, bf16[1024,256]{1,0:T(8,128)(2,1)}, u32[]{:S(2)}, u32[]{:S(2)}) collective-permute-start(bf16[1024,256]{1,0:T(8,128)(2,1)} %collective-permute-done.13.refs_1_), channel_id=1, source_target_pairs={{0,6},{1,7},{2,0},{3,1},{4,2},{5,3},{6,4},{7,5},{8,14},{9,15},{10,... | collective-permute-start | bytes 1572872 | tf_op jit(solution)/shard_map/ppermute | solution.py:40
  69.6 14.7 %collective-permute-start.17 = (bf16[1024,256]{1,0:T(8,128)(2,1)}, bf16[1024,256]{1,0:T(8,128)(2,1)}, u32[]{:S(2)}, u32[]{:S(2)}) collective-permute-start(bf16[1024,256]{1,0:T(8,128)(2,1)} %collective-permute-done.13.refs_1_), channel_id=1, source_target_pairs={{0,2},{1,3},{2,4},{3,5},{4,6},{5,7},{6,0},{7,1},{8,10},{9,11},{10,... | collective-permute-start | bytes 1572872 | tf_op jit(solution)/shard_map/ppermute | solution.py:40
  72.3 24.3 %collective-permute-start.5 = (bf16[192,2048]{1,0:T(8,128)(2,1)}, bf16[192,2048]{1,0:T(8,128)(2,1)S(1)}, u32[]{:S(2)}, u32[]{:S(2)}) collective-permute-start(bf16[192,2048]{1,0:T(8,128)(2,1)} %shard_map.137.refs_1_), channel_id=1, source_target_pairs={{0,16},{1,65},{2,18},{3,67},{4,20},{5,69},{6,22},{7,71},{8,24},{9,... | collective-permute-start | bytes 2359304 | tf_op jit(solution)/shard_map/ppermute | solution.py:48
  75.3 20.1 %collective-permute-start.12 = (bf16[1024,256]{1,0:T(8,128)(2,1)}, bf16[1024,256]{1,0:T(8,128)(2,1)S(1)}, u32[]{:S(2)}, u32[]{:S(2)}) collective-permute-start(bf16[1024,256]{1,0:T(8,128)(2,1)} %copy-done.20), channel_id=1, source_target_pairs={{0,2},{1,3},{2,4},{3,5},{4,6},{5,7},{6,0},{7,1},{8,10},{9,11},{10,... | collective-permute-start | bytes 1572872 | tf_op jit(solution)/shard_map/ppermute | solution.py:40
  81.2 16.3 %collective-permute-start.3 = (bf16[192,2048]{1,0:T(8,128)(2,1)}, bf16[192,2048]{1,0:T(8,128)(2,1)S(1)}, u32[]{:S(2)}, u32[]{:S(2)}) collective-permute-start(bf16[192,2048]{1,0:T(8,128)(2,1)} %shard_map.137.refs_1_), channel_id=1, source_target_pairs={{0,8},{1,33},{2,10},{3,35},{4,12},{5,37},{6,14},{7,39},{8,16},{9,4... | collective-permute-start | bytes 2359304 | tf_op jit(solution)/shard_map/ppermute | solution.py:48
  84.3 13.9 %collective-permute-start.4 = (bf16[192,2048]{1,0:T(8,128)(2,1)}, bf16[192,2048]{1,0:T(8,128)(2,1)}, u32[]{:S(2)}, u32[]{:S(2)}) collective-permute-start(bf16[192,2048]{1,0:T(8,128)(2,1)} %shard_map.137.refs_1_), channel_id=1, source_target_pairs={{0,24},{1,97},{2,26},{3,99},{4,28},{5,101},{6,30},{7,103},{8,0},{9... | collective-permute-start | bytes 2359304 | tf_op jit(solution)/shard_map/ppermute | solution.py:48
  95.4 23.6 %collective-permute-start.7 = (bf16[192,2048]{1,0:T(8,128)(2,1)}, bf16[192,2048]{1,0:T(8,128)(2,1)}, u32[]{:S(2)}, u32[]{:S(2)}) collective-permute-start(bf16[192,2048]{1,0:T(8,128)(2,1)} %shard_map.137.refs_1_), channel_id=1, source_target_pairs={{0,1},{1,0},{2,3},{3,2},{4,5},{5,4},{6,7},{7,6},{8,9},{9,8},{10,11... | collective-permute-start | bytes 2359304 | tf_op jit(solution)/shard_map/ppermute | solution.py:44
  96.6 12.6 %copy-start = (bf16[192,2048]{1,0:T(8,128)(2,1)}, bf16[192,2048]{1,0:T(8,128)(2,1)S(1)}, u32[]{:S(2)}) copy-start(bf16[192,2048]{1,0:T(8,128)(2,1)S(1)} %collective-permute-done.5.refs_4_) | copy-start | bytes 2359300
  96.6 13.2 %collective-permute-start.15 = (bf16[1024,256]{1,0:T(8,128)(2,1)}, bf16[1024,256]{1,0:T(8,128)(2,1)}, u32[]{:S(2)}, u32[]{:S(2)}) collective-permute-start(bf16[1024,256]{1,0:T(8,128)(2,1)} %collective-permute-done.14.refs_5_), channel_id=1, source_target_pairs={{0,6},{1,7},{2,0},{3,1},{4,2},{5,3},{6,4},{7,5},{8,14},{9,15},{10,... | collective-permute-start | bytes 1572872 | tf_op jit(solution)/shard_map/ppermute | solution.py:40
  97.5 11.7 %copy-start.1 = (bf16[192,2048]{1,0:T(8,128)(2,1)}, bf16[192,2048]{1,0:T(8,128)(2,1)S(1)}, u32[]{:S(2)}) copy-start(bf16[192,2048]{1,0:T(8,128)(2,1)S(1)} %collective-permute-done.3.refs_2_) | copy-start | bytes 2359300
  97.5 42.1 %collective-permute-start.10 = (bf16[192,2048]{1,0:T(8,128)(2,1)S(1)}, bf16[192,2048]{1,0:T(8,128)(2,1)}, u32[]{:S(2)}, u32[]{:S(2)}) collective-permute-start(bf16[192,2048]{1,0:T(8,128)(2,1)S(1)} %collective-permute-done.5.refs_4_), channel_id=1, source_target_pairs={{0,1},{1,0},{2,3},{3,2},{4,5},{5,4},{6,7},{7,6},{8,9},{9,8},{10,11... | collective-permute-start | bytes 2359304 | tf_op jit(solution)/shard_map/ppermute | solution.py:44
  98.2 43.1 %collective-permute-start.8 = (bf16[192,2048]{1,0:T(8,128)(2,1)S(1)}, bf16[192,2048]{1,0:T(8,128)(2,1)}, u32[]{:S(2)}, u32[]{:S(2)}) collective-permute-start(bf16[192,2048]{1,0:T(8,128)(2,1)S(1)} %collective-permute-done.3.refs_2_), channel_id=1, source_target_pairs={{0,1},{1,0},{2,3},{3,2},{4,5},{5,4},{6,7},{7,6},{8,9},{9,8},{10,11... | collective-permute-start | bytes 2359304 | tf_op jit(solution)/shard_map/ppermute | solution.py:44
  109.7 32.5 %collective-permute-start.9 = (bf16[192,2048]{1,0:T(8,128)(2,1)}, bf16[192,2048]{1,0:T(8,128)(2,1)}, u32[]{:S(2)}, u32[]{:S(2)}) collective-permute-start(bf16[192,2048]{1,0:T(8,128)(2,1)} %collective-permute-done.4.refs_3_), channel_id=1, source_target_pairs={{0,1},{1,0},{2,3},{3,2},{4,5},{5,4},{6,7},{7,6},{8,9},{9,8},{10,11... | collective-permute-start | bytes 2359304 | tf_op jit(solution)/shard_map/ppermute | solution.py:44
  111.3 20.6 %copy-start.17 = (s32[16,2]{0,1:T(2,128)S(1)}, s32[16,2]{0,1:T(2,128)}, u32[]{:S(2)}) copy-start(s32[16,2]{0,1:T(2,128)} %param.16) | copy-start | bytes 388
  119.1 6.7 %collective-permute-start.28 = (bf16[256,256]{1,0:T(8,128)(2,1)}, bf16[256,256]{1,0:T(8,128)(2,1)S(1)}, u32[]{:S(2)}, u32[]{:S(2)}) collective-permute-start(bf16[256,256]{1,0:T(8,128)(2,1)} %get-tuple-element.26), channel_id=1, source_target_pairs={{0,2},{1,3},{2,4},{3,5},{4,6},{5,7},{6,0},{7,1},{8,10},{9,11},{10,... | collective-permute-start | bytes 393224 | tf_op jit(solution)/shard_map/ppermute | solution.py:40
  125.8 11.9 %copy-start.11 = (bf16[256,256]{1,0:T(8,128)(2,1)}, bf16[256,256]{1,0:T(8,128)(2,1)S(1)}, u32[]{:S(2)}) copy-start(bf16[256,256]{1,0:T(8,128)(2,1)S(1)} %collective-permute-done.28.refs_11_) | copy-start | bytes 393220
  125.8 4.4 %collective-permute-start.29 = (bf16[256,256]{1,0:T(8,128)(2,1)}, bf16[256,256]{1,0:T(8,128)(2,1)S(1)}, u32[]{:S(2)}, u32[]{:S(2)}) collective-permute-start(bf16[256,256]{1,0:T(8,128)(2,1)} %get-tuple-element.27), channel_id=1, source_target_pairs={{0,6},{1,7},{2,0},{3,1},{4,2},{5,3},{6,4},{7,5},{8,14},{9,15},{10,... | collective-permute-start | bytes 393224 | tf_op jit(solution)/shard_map/ppermute | solution.py:40
  130.2 7.5 %copy-start.12 = (bf16[256,256]{1,0:T(8,128)(2,1)}, bf16[256,256]{1,0:T(8,128)(2,1)S(1)}, u32[]{:S(2)}) copy-start(bf16[256,256]{1,0:T(8,128)(2,1)S(1)} %collective-permute-done.29.refs_12_) | copy-start | bytes 393220
  130.2 19.3 %collective-permute-start.6 = (bf16[128,2048]{1,0:T(8,128)(2,1)}, bf16[128,2048]{1,0:T(8,128)(2,1)}, u32[]{:S(2)}, u32[]{:S(2)}) collective-permute-start(bf16[128,2048]{1,0:T(8,128)(2,1)} %refs_0_.3), channel_id=1, source_target_pairs={{0,1},{1,0},{2,3},{3,2},{4,5},{5,4},{6,7},{7,6},{8,9},{9,8},{10,11... | collective-permute-start | bytes 1572872 | tf_op jit(solution)/shard_map/ppermute | solution.py:44
  131.9 6.7 %collective-permute-start.30 = (bf16[256,256]{1,0:T(8,128)(2,1)}, bf16[256,256]{1,0:T(8,128)(2,1)S(1)}, u32[]{:S(2)}, u32[]{:S(2)}) collective-permute-start(bf16[256,256]{1,0:T(8,128)(2,1)} %get-tuple-element.28), channel_id=1, source_target_pairs={{0,4},{1,5},{2,6},{3,7},{4,0},{5,1},{6,2},{7,3},{8,12},{9,13},{10,... | collective-permute-start | bytes 393224 | tf_op jit(solution)/shard_map/ppermute | solution.py:40
  138.6 3.6 %copy-start.13 = (bf16[256,256]{1,0:T(8,128)(2,1)}, bf16[256,256]{1,0:T(8,128)(2,1)S(1)}, u32[]{:S(2)}) copy-start(bf16[256,256]{1,0:T(8,128)(2,1)S(1)} %collective-permute-done.30.refs_13_) | copy-start | bytes 393220
  138.6 10.9 %collective-permute-start.24 = (bf16[256,256]{1,0:T(8,128)(2,1)}, bf16[256,256]{1,0:T(8,128)(2,1)S(1)}, u32[]{:S(2)}, u32[]{:S(2)}) collective-permute-start(bf16[256,256]{1,0:T(8,128)(2,1)} %get-tuple-element.21), channel_id=1, source_target_pairs={{0,2},{1,3},{2,4},{3,5},{4,6},{5,7},{6,0},{7,1},{8,10},{9,11},{10,... | collective-permute-start | bytes 393224 | tf_op jit(solution)/shard_map/ppermute | solution.py:40
  139.6 10.0 %collective-permute-start.25 = (bf16[256,256]{1,0:T(8,128)(2,1)}, bf16[256,256]{1,0:T(8,128)(2,1)S(1)}, u32[]{:S(2)}, u32[]{:S(2)}) collective-permute-start(bf16[256,256]{1,0:T(8,128)(2,1)} %get-tuple-element.22), channel_id=1, source_target_pairs={{0,6},{1,7},{2,0},{3,1},{4,2},{5,3},{6,4},{7,5},{8,14},{9,15},{10,... | collective-permute-start | bytes 393224 | tf_op jit(solution)/shard_map/ppermute | solution.py:40
  141.3 8.3 %collective-permute-start.26 = (bf16[256,256]{1,0:T(8,128)(2,1)}, bf16[256,256]{1,0:T(8,128)(2,1)S(1)}, u32[]{:S(2)}, u32[]{:S(2)}) collective-permute-start(bf16[256,256]{1,0:T(8,128)(2,1)} %get-tuple-element.23), channel_id=1, source_target_pairs={{0,4},{1,5},{2,6},{3,7},{4,0},{5,1},{6,2},{7,3},{8,12},{9,13},{10,... | collective-permute-start | bytes 393224 | tf_op jit(solution)/shard_map/ppermute | solution.py:40
  (6 other events, 4.8 us)

commit v3 on v2

v3 whole, which is shorter than its diff:
```python
import jax
import jax.numpy as jnp
from jax import lax
from jax.experimental import pallas as pl
from jax.experimental.pallas import tpu as pltpu
from jax.sharding import PartitionSpec as P

HEAD_SIZE = 128
SEQ_LEN = 256
BLOCK = 128
NPB = 2
PLEN = 64
N_Y = 4
N_X = 4
N_Z = 4
BF = jnp.bfloat16
F32 = jnp.float32
SERVE_VMEM, PROJECT_VMEM, ATTEND_VMEM, FINISH_VMEM, SMALL_VMEM = 58, 62, 8, 14, 6


SHIFT = {
    s: [(2 * y + c, 2 * ((y + s) % N_Y) + c) for y in range(N_Y) for c in range(2)]
    for s in (1, -1, 2)
}
SWAP = [(2 * y + c, 2 * y + 1 - c) for y in range(N_Y) for c in range(2)]


def plane_shift(s):
    pairs = []
    for z in range(N_Z):
        for x in range(N_X):
            for y in range(N_Y):
                for c in range(2):
                    z2, x2 = (z, (x + s) % N_X) if c == 0 else ((z + s) % N_Z, x)
                    pairs.append(((z * N_X + x) * 8 + 2 * y + c, (z2 * N_X + x2) * 8 + 2 * y + c))
    return pairs


def shift(a, s):
    return lax.ppermute(a, "tp", SHIFT[s])


def swap(a):
    return lax.ppermute(a, "tp", SWAP)


def plane(a, s):
    return lax.ppermute(a, ("st", "tp"), plane_shift(s))


def pick(a, index, axis=0):
    return lax.dynamic_index_in_dim(a, index, axis, keepdims=False)


def dot(a, b):
    return jnp.dot(a, b, preferred_element_type=F32)


def call(body, sc, ins, in_specs, outs, out_specs, scratch=(), grid=(1,), flops=0, bytes_=0, vmem=62):
    return pl.pallas_call(
        body,
        grid_spec=pltpu.PrefetchScalarGridSpec(
            num_scalar_prefetch=1,
            grid=grid,
            in_specs=in_specs,
            out_specs=out_specs,
            scratch_shapes=list(scratch),
        ),
        out_shape=[jax.ShapeDtypeStruct(shape, dtype) for shape, dtype in outs],
        compiler_params=pltpu.CompilerParams(vmem_limit_bytes=vmem * 2**20),
        cost_estimate=pl.CostEstimate(flops=flops, bytes_accessed=bytes_, transcendentals=0),
    )(sc, *ins)


def whole(a):
    return pl.BlockSpec(a.shape, lambda *_, n=a.ndim: (0,) * n)


def fixed(*shape):
    return pl.BlockSpec(shape, lambda *_, n=len(shape): (0,) * n)


HBM = pl.BlockSpec(memory_space=pl.ANY)


def start(copies):
    for c in copies:
        c.start()


def wait(copies):
    for c in copies:
        c.wait()


def prep_kernel(sc, tokens, conv_out, memory_out, slab, other, part, sems):
    core, quarter = sc[2], sc[0]
    n = N_Y * SEQ_LEN
    pairs = []
    for j in range(N_Y):
        own = pl.multiple_of((2 * j + core) * SEQ_LEN, SEQ_LEN)
        away = pl.multiple_of((2 * j + 1 - core) * SEQ_LEN, SEQ_LEN)
        dst = pl.ds(j * SEQ_LEN, SEQ_LEN)
        pairs.append((tokens.at[pl.ds(own, SEQ_LEN)], slab.at[dst]))
        pairs.append((tokens.at[pl.ds(away, SEQ_LEN)], other.at[dst]))
    rows = pl.ds(pl.multiple_of(quarter * 32, 32), 32)
    for i, w in enumerate((conv_out, memory_out)):
        for cb in range(8):
            src = w.at[rows, pl.ds(cb * 256, 256)]
            dst = cb * 64 + i * 32
            pairs.append((src, slab.at[pl.ds(n + dst, 32)]))
            pairs.append((src, part.at[pl.ds(dst, 32)]))
    copies = [pltpu.make_async_copy(x, y, sems.at[k]) for k, (x, y) in enumerate(pairs)]
    start(copies)
    wait(copies)


def prep(sc, tokens, conv_out, memory_out):
    n, k = N_Y * SEQ_LEN, tokens.shape[1]
    return call(
        prep_kernel, sc, (tokens, conv_out, memory_out), [HBM] * 3,
        [((n + 512, k), BF), ((n, k), BF), ((512, k), BF)],
        [fixed(n + 512, k), fixed(n, k), fixed(512, k)],
        scratch=[pltpu.SemaphoreType.DMA((40,))], bytes_=3 * 2**20, flops=10**8, vmem=6,
    )


def pack_kernel(sc, a, b, c, out):
    for d, (ref, first) in enumerate(((a, ref_rows(a)), (b, ref_rows(b)), (c, 0))):
        for cb in range(8):
            out[d * 64 : (d + 1) * 64, cb * 256 : (cb + 1) * 256] = ref[
                first + cb * 64 : first + (cb + 1) * 64
            ]


def ref_rows(ref):
    return ref.shape[0] - 512


def pack(sc, parts):
    tail = lambda a: pl.BlockSpec((512, a.shape[1]), lambda i, s, n=a.shape[0] // 512: (n - 1, 0))
    return call(
        pack_kernel, sc, parts, [tail(p) for p in parts],
        [((192, 2048), BF)], [fixed(192, 2048)], bytes_=2**20, flops=10**8, vmem=SMALL_VMEM,
    )[0]


def serve_kernel(sc, rows, kw, vw, out, table, w, sems):
    j = pl.program_id(0)
    H = kw.shape[1]

    @pl.when(j == 0)
    def _():
        w[:, :H] = kw[...]
        w[:, H:] = vw[...]

    per = rows.shape[0] // PLEN
    kv = dot(rows[...], w[...]).astype(BF)
    table[pl.ds(j * per, per)] = kv.reshape(per, PLEN, 2 * H)

    @pl.when(j == pl.num_programs(0) - 1)
    def _():
        n_own, cap = out.shape[0], out.shape[1]
        copies = [
            pltpu.make_async_copy(table.at[sc[o, k]], out.at[o, k], sems.at[o * cap + k])
            for o in range(n_own)
            for k in range(cap)
        ]
        for c in copies:
            c.start()
        for c in copies:
            c.wait()


def serve(wanted, store, kw, vw):
    n_own, cap = wanted.shape
    flat = store.reshape(-1, store.shape[-1])
    rows, d = flat.shape
    H = kw.shape[1]
    block = 512
    return call(
        serve_kernel, wanted, (flat, kw, vw),
        [pl.BlockSpec((block, d), lambda j, s: (j, 0)), whole(kw), whole(vw)],
        [((n_own, cap, PLEN, 2 * H), BF)], [HBM],
        scratch=[
            pltpu.VMEM((store.shape[0], PLEN, 2 * H), BF),
            pltpu.VMEM((d, 2 * H), BF),
            pltpu.SemaphoreType.DMA((n_own * cap,)),
        ],
        grid=(rows // block,), flops=2 * rows * d * 2 * H, bytes_=11 * 2**20, vmem=SERVE_VMEM,
    )[0]


def project_kernel(sc, *refs):
    pieces, weights = refs[:8], refs[8:16]
    gate, tm, to = refs[16:19]
    q_out, conv_outs, logit_ref = refs[19], refs[20:24], refs[24]
    lhs, w, acc, q_s, conv_s, lsem, wsem, osem = refs[25:]
    H = HEAD_SIZE
    n_rows = lhs.shape[0]
    lcopy = [
        pltpu.make_async_copy(
            p.at[pl.ds(0, n_rows)],
            lhs.at[:, pl.ds(pl.multiple_of(sc[k] * 256, 256), 256)],
            lsem.at[k],
        )
        for k, p in enumerate(pieces)
    ]
    wcopy = [
        pltpu.make_async_copy(p, w.at[n // 2, :, pl.ds(n % 2 * H, H)], wsem.at[n])
        for n, p in enumerate(weights)
    ]
    start(lcopy)
    start(wcopy)
    wait(lcopy)
    wait(wcopy)

    def product(n, carry):
        acc[n] = dot(lhs[...], w[n])
        return carry

    lax.fori_loop(0, 4, product, 0)
    ids = lax.broadcasted_iota(jnp.int32, (SEQ_LEN, H), 0)
    taps = [t[...].astype(F32) for t in (tm, to)]

    def convolve(j, carry):
        rows = pl.ds(pl.multiple_of(sc[8 + j] * SEQ_LEN, SEQ_LEN), SEQ_LEN)
        for side, t in enumerate(taps):
            prod = acc[2 * side + 1, rows, :H] * acc[2 * side + 1, rows, H:]
            back1 = jnp.where(ids >= 1, pltpu.roll(prod, 1, 0), 0.0)
            back2 = jnp.where(ids >= 2, pltpu.roll(prod, 2, 0), 0.0)
            filtered = t[0:1] * back2 + t[1:2] * back1 + t[2:3] * prod
            outer = acc[2 * side, rows, H:]
            conv_s[j, :, side * H : (side + 1) * H] = (outer * filtered).astype(BF)
        return carry

    lax.fori_loop(0, 4, convolve, 0)
    ocopy = [pltpu.make_async_copy(conv_s.at[j], conv_outs[j], osem.at[j]) for j in range(4)]
    start(ocopy)
    q_s[:, :H] = acc[0, :, :H].astype(BF)
    q_s[:, H:] = acc[2, :, :H].astype(BF)
    qcopy = [pltpu.make_async_copy(q_s, q_out, osem.at[4])]
    start(qcopy)
    own = pl.ds(pl.multiple_of(sc[11] * SEQ_LEN, SEQ_LEN), SEQ_LEN)
    logit_ref[...] = lax.dot_general(
        lhs[own, :], gate[...], (((1,), (1,)), ((), ())), preferred_element_type=F32
    )
    wait(ocopy)
    wait(qcopy)


def project(sc, pieces, weights, gate, tm, to):
    rows = N_Y * SEQ_LEN
    d = gate.shape[1]
    return call(
        project_kernel, sc, (*pieces, *weights, gate, tm, to),
        [HBM] * 16 + [whole(a) for a in (gate, tm, to)],
        [((rows, 256), BF)] + [((SEQ_LEN, 256), BF)] * 4 + [((SEQ_LEN, 2), F32)],
        [HBM] * 5 + [fixed(SEQ_LEN, 2)],
        scratch=[
            pltpu.VMEM((rows, d), BF),
            pltpu.VMEM((4, d, 256), BF),
            pltpu.VMEM((4, rows, 256), F32),
            pltpu.VMEM((rows, 256), BF),
            pltpu.VMEM((4, SEQ_LEN, 256), BF),
            pltpu.SemaphoreType.DMA((8,)),
            pltpu.SemaphoreType.DMA((8,)),
            pltpu.SemaphoreType.DMA((5,)),
        ],
        flops=2 * rows * d * 1024, bytes_=10 * 2**20, vmem=PROJECT_VMEM,
    )


def attend_kernel(sc, q_in, tab_m, tab_o, *refs):
    outs = refs[:4]
    q, kv, s_ref, p_ref, sems, qsem = refs[4:]
    H = HEAD_SIZE
    qcopy = pltpu.make_async_copy(q_in, q, qsem)
    qcopy.start()
    work, copies = [], []
    for j in range(4):
        for half in range(2):
            b = sc[16 + j] * 2 + half
            rows = pl.ds(pl.multiple_of(b * BLOCK, BLOCK), BLOCK)
            for h, tab in enumerate((tab_m, tab_o)):
                i = len(work)
                for n in range(NPB):
                    copies.append(
                        pltpu.make_async_copy(
                            tab.at[sc[NPB * b + n]],
                            kv.at[i, pl.ds(n * PLEN, PLEN)],
                            sems.at[NPB * i + n],
                        )
                    )
                work.append((j, half, h, rows))
    start(copies)
    qcopy.wait()
    wait(copies)
    n = len(work)
    for i, (j, half, h, rows) in enumerate(work):
        s_ref[i * BLOCK : (i + 1) * BLOCK] = lax.dot_general(
            q[rows, h * H : (h + 1) * H], kv[i, :, :H], (((1,), (1,)), ((), ())),
            preferred_element_type=F32,
        )
    for i in range(0, n, 4):
        part = slice(i * BLOCK, (i + 4) * BLOCK)
        s = s_ref[part] * (H**-0.5)
        e = jnp.exp(s - jnp.max(s, axis=-1, keepdims=True))
        p_ref[part] = (e / jnp.sum(e, axis=-1, keepdims=True)).astype(BF)
    for i, (j, half, h, rows) in enumerate(work):
        o = dot(p_ref[i * BLOCK : (i + 1) * BLOCK], kv[i, :, H:])
        outs[j][half * BLOCK : (half + 1) * BLOCK, h * H : (h + 1) * H] = o.astype(BF)


def attend(sc, q, tab_m, tab_o):
    n = 16
    return call(
        attend_kernel, sc, (q, tab_m, tab_o), [HBM] * 3,
        [((SEQ_LEN, 256), BF)] * 4, [fixed(SEQ_LEN, 256)] * 4,
        scratch=[
            pltpu.VMEM(q.shape, BF),
            pltpu.VMEM((n, NPB * PLEN, 256), BF),
            pltpu.VMEM((n * BLOCK, BLOCK), F32),
            pltpu.VMEM((n * BLOCK, BLOCK), BF),
            pltpu.SemaphoreType.DMA((n * NPB,)),
            pltpu.SemaphoreType.DMA,
        ],
        flops=10**9, bytes_=5 * 2**20, vmem=ATTEND_VMEM,
    )


def finish_kernel(branch, sc, *refs):
    sides = (refs[0:5], refs[5:10])
    parts, logits = refs[10:14], refs[14]
    before = None if branch == 0 else refs[15]
    out, w, x, o_s, sems, bsem, osem = refs[-7:]
    copies = []
    for side in range(2):
        own, e, r1, r2, r3 = sides[side]
        base = side * 128
        copies.append((own, w.at[pl.ds(base, 128)]))
        for src, back in ((e, 0), (r1, 3), (r2, 1), (r3, 2)):
            quarter = lax.rem(sc[side] + back, 4)
            row = pl.multiple_of(base + quarter * 32, 32)
            for d in range(3):
                copies.append(
                    (src.at[pl.ds(d * 64 + branch * 32, 32)], w.at[pl.ds((1 + d) * 256 + row, 32)])
                )
    for d in range(4):
        copies.append((parts[d], x.at[:, pl.ds(d * 256, 256)]))
    copies = [pltpu.make_async_copy(a, b, sems.at[n]) for n, (a, b) in enumerate(copies)]
    start(copies)
    if before is not None:
        bcopy = pltpu.make_async_copy(before, o_s, bsem)
        bcopy.start()
    mix = jax.nn.sigmoid(logits[:, branch : branch + 1])
    wait(copies)
    if before is not None:
        bcopy.wait()
    step = 512

    def product(i, carry):
        cols = pl.ds(pl.multiple_of(i * step, step), step)
        a = mix * dot(x[...], w[:, cols])
        if before is None:
            o_s[:, cols] = a
        else:
            refs[-8][:, cols] = (o_s[:, cols] + a).astype(BF)
        return carry

    lax.fori_loop(0, w.shape[1] // step, product, 0)
    ocopy = pltpu.make_async_copy(o_s if before is None else refs[-8], out, osem.at[0])
    ocopy.start()
    ocopy.wait()


def finish(branch, sc, mine, other, parts, logits, before=None):
    width = mine[0].shape[1]
    last = before is not None
    ins = (*mine, *other, *parts, logits) + ((before,) if last else ())
    scratch = [
        pltpu.VMEM((1024, width), BF),
        pltpu.VMEM((SEQ_LEN, 1024), BF),
        pltpu.VMEM((SEQ_LEN, width), F32),
        pltpu.SemaphoreType.DMA((30,)),
        pltpu.SemaphoreType.DMA,
        pltpu.SemaphoreType.DMA((width // 512,)),
    ]

    def body(*refs):
        if not last:
            return finish_kernel(branch, *refs)
        return finish_kernel(branch, *refs[:-8], refs[-1], *refs[-8:-1])

    return call(
        body, sc, ins,
        [HBM] * 14 + [whole(logits)] + ([HBM] if last else []),
        [((SEQ_LEN, width), BF if last else F32)], [HBM],
        scratch=scratch + ([pltpu.VMEM((SEQ_LEN, width), BF)] if last else []),
        flops=SEQ_LEN * 2048 * 2048, bytes_=7 * 2**20, vmem=FINISH_VMEM,
    )[0]


def local(
    tokens,
    store,
    passage_holder_index,
    passage_slot,
    query_weight,
    key_matrix,
    value_weight,
    outer_gate,
    inner_gate,
    conv_input,
    conv_taps,
    route_gate_projection,
    conv_out,
    memory_out,
):
    me = lax.axis_index("tp")
    st = lax.axis_index("st")
    y, c = me // 2, me % 2
    z, x = st // N_X, st % N_X
    HW = query_weight.shape[1]
    i32 = jnp.int32

    quarter = jnp.where(c == 0, x, z)
    quarter_other = jnp.where(c == 0, z, x)
    sc_quarter = jnp.stack([quarter, quarter_other, c]).astype(i32)
    slab, other, part = prep(sc_quarter, tokens, conv_out, memory_out)

    a0, b0 = shift(slab, 1), shift(slab, -1)
    h1 = swap(other)
    far_part = shift(part, 2)
    a1, b1 = shift(h1, 1), shift(h1, -1)
    c0, c1 = shift(a0, 1), shift(b1, -1)
    pieces = (slab, h1, a0, b0, a1, b1, c0, c1)

    e = pack(sc_quarter, (a0, b0, far_part))
    ring = [e, plane(e, 1), plane(e, -1), plane(e, 2)]
    ring_other = [swap(a) for a in ring]
    conv_out_other, memory_out_other = swap(conv_out), swap(memory_out)

    owners = passage_holder_index.reshape(-1)
    local_slots = passage_slot.reshape(-1)
    owner_count = lax.axis_size("st")
    request_count = owners.shape[0]
    capacity = max(2, 2 * request_count // owner_count)
    one_hot = (owners[:, None] == jnp.arange(owner_count, dtype=i32)[None, :]).astype(i32)
    before = jnp.cumsum(one_hot, axis=0) - one_hot
    position = jnp.sum(before * one_hot, axis=1)
    target = owners * capacity + position
    matches = (target[:, None] == jnp.arange(owner_count * capacity, dtype=i32)[None, :]).astype(i32)
    outgoing = jnp.sum(matches * local_slots[:, None], axis=0).reshape(owner_count, capacity)
    wanted = lax.all_to_all(outgoing, "st", split_axis=0, concat_axis=0)

    def slice_of(dy, flip):
        return 2 * ((y + dy) % N_Y) + (1 - c if flip else c)

    flips = ((0, False), (0, True), (-1, False), (1, False), (-1, True), (1, True), (2, False), (2, True))
    yord = [(y + d) % N_Y for d in (2, 1, -1, 0)]
    sc_project = jnp.stack([slice_of(*f) for f in flips] + yord).astype(i32)

    chosen = serve(wanted, store, key_matrix, value_weight)
    served = lax.all_to_all(chosen, "st", split_axis=0, concat_axis=0)
    tab_m = served.reshape(owner_count * capacity, PLEN, 2 * HW)
    tab_o = swap(tab_m)
    mine = pick(target.reshape(N_Y, 2, -1), c, 1).reshape(-1)
    sc_attend = jnp.concatenate([mine, jnp.stack(yord)]).astype(i32)

    w_mine = [query_weight, outer_gate, inner_gate, conv_input]
    weights = w_mine + [swap(w) for w in w_mine]
    taps_part = swap(conv_taps)
    gate = route_gate_projection.T

    q, *convs, logits = project(sc_project, pieces, weights, gate, conv_taps, taps_part)
    conv_all = [convs[3], shift(convs[1], 1), shift(convs[2], -1), shift(convs[0], 2)]
    half = finish(0, sc_quarter, [conv_out] + ring, [conv_out_other] + ring_other, conv_all, logits)
    mems = attend(sc_attend, q, tab_m, tab_o)
    mem_all = [mems[3], shift(mems[1], 1), shift(mems[2], -1), shift(mems[0], 2)]
    return finish(
        1, sc_quarter, [memory_out] + ring, [memory_out_other] + ring_other, mem_all, logits, half
    )


def solution(mesh):
    return jax.shard_map(
        local,
        mesh=mesh,
        in_specs=(
            P("st", "tp"),
            P("st", None, None),
            P("st", None),
            P("st", None),
            P(None, "tp"),
            P(None, "tp"),
            P(None, "tp"),
            P(None, "tp"),
            P(None, "tp"),
            P(None, "tp"),
            P(None, "tp"),
            P(),
            P("tp", None),
            P("tp", None),
        ),
        out_specs=P(("st", "tp"), None),
        check_vma=False,
    )
```

time: 159 us -> 153 us (0.962)
  Pallas kernels: 53.3 us -> 38.7 us
  starting transfers between devices: 37.7 us -> 45.4 us
  waiting for transfers between devices: 44.1 us -> 46.8 us
    pallas_call x8 -> x7, Pallas kernels: 53.3 us -> 38.7 us  [call(): pl.pallas_call(body, grid_spec=pltpu.PrefetchScalarGridSpec(num_scalar_pr...]
    all_to_all x1, waiting for transfers between devices: 0.01 us -> 5.9 us  [local(): served = lax.all_to_all(chosen, 'st', split_axis=0, concat_axis=0)]
    ppermute x15 -> x13, starting transfers between devices: 13 us -> 17.7 us  [shift(): return lax.ppermute(a, 'tp', SHIFT[s])]
    ppermute x13, starting transfers between devices: 12.9 us -> 17 us  [swap(): return lax.ppermute(a, 'tp', SWAP)]
    ppermute x15 -> x13, waiting for transfers between devices: 43.2 us -> 39.3 us  [shift(): return lax.ppermute(a, 'tp', SHIFT[s])]
    unnamed x46 -> x40, local copies, waits for them, and re-layouts: 3.81 us -> 4.38 us
  transfers between devices with their start and end apart: 32 -> 30, of which waited for: 11 -> 12; matrix products, arithmetic and copies ran while one was open for 2% -> 1% of each run, Pallas kernels for 22% -> 16%
where the time goes in v3:
time: 153 us; the launch traced here: 152 us
  waiting for transfers between devices  46.8 us (31%)
  starting transfers between devices  45.4 us (30%)
  Pallas kernels  38.7 us (25%)
  blocking collectives  14.6 us (10%)
  local copies, waits for them, and re-layouts  5.68 us (4%)
    ppermute x13, waiting for transfers between devices, shift(): return lax.ppermute(a, 'tp', SHIFT[s])  39.3 us
    pallas_call x7, Pallas kernels, call(): pl.pallas_call(body, grid_spec=pltpu.PrefetchScalarGridSpec(num_scalar_pr...  38.7 us
    ppermute x13, starting transfers between devices, shift(): return lax.ppermute(a, 'tp', SHIFT[s])  17.7 us
    ppermute x13, starting transfers between devices, swap(): return lax.ppermute(a, 'tp', SWAP)  17 us
    all_to_all x1, blocking collectives, local(): wanted = lax.all_to_all(outgoing, 'st', split_axis=0, concat_axis=0)  14.6 us
    ppermute x3, starting transfers between devices, plane(): return lax.ppermute(a, ('st', 'tp'), plane_shift(s))  6.07 us
    all_to_all x1, waiting for transfers between devices, local(): served = lax.all_to_all(chosen, 'st', split_axis=0, concat_axis=0)  5.9 us
    all_to_all x1, starting transfers between devices, local(): served = lax.all_to_all(chosen, 'st', split_axis=0, concat_axis=0)  4.57 us
  transfers between devices with their start and end apart: 30, of which 12 were waited for; matrix products, arithmetic and copies ran while one was open for 1% of the time, Pallas kernels for 16%

profile of v3, /device:TPU:1, one launch (start us, length us, event | category | flops | bytes accessed | tf_op | source)
XLA Modules:
  0.0 152.2 jit_solution(12136982901604257073)
XLA Ops:
  0.0 0.8 copy.32
  1.2 0.8 copy.33
  2.2 14.6 %all_to_all.16 = s32[16,1,4]{2,1,0:T(1,128)} all-to-all(s32[16,1,4]{2,1,0:T(1,128)S(1)} %bitcast.22), channel_id=1, replica_groups=mesh['st'=16,'tp'=8] {'st'}, dimensions={0} | all-to-all | bytes 512 | tf_op jit(solution)/shard_map/all_to_all | solution.py:455
  16.8 8.6 %shard_map.139 = bf16[16,4,64,256]{3,2,1,0:T(8,128)(2,1)} custom-call(s32[16,4]{1,0:T(8,128)} %bitcast.21, bf16[2048,2048]{1,0:T(8,128)(2,1)} %bitcast.20, bf16[2048,128]{1,0:T(8,128)(2,1)} %kw.1, bf16[2048,128]{1,0:T(8,128)(2,1)} %vw.1), custom_call_target="tpu_custom_call" | custom-call | flops 2147483648 | bytes 11534336 | tf_op jit(solution)/shard_map/pallas_call | solution.py:60
  25.5 4.6 %all-to-all-start.1 = ((bf16[16,4,64,256]{3,2,1,0:T(8,128)(2,1)}), bf16[16,4,64,256]{3,2,1,0:T(8,128)(2,1)}, u32[]{:S(2)}, u32[]{:S(2)}) async-start(bf16[16,4,64,256]{3,2,1,0:T(8,128)(2,1)} %shard_map.139), calls=%async_computation.1 | async-start | bytes 4194304 | tf_op jit(solution)/shard_map/all_to_all | solution.py:465
  30.2 2.5 %shard_map.136 = (bf16[1536,256]{1,0:T(8,128)(2,1)S(1)}, bf16[1024,256]{1,0:T(8,128)(2,1)S(1)}, bf16[512,256]{1,0:T(8,128)(2,1)S(1)}) custom-call(s32[3]{0:T(128)S(1)} %pad_add_fusion.sc.refs_0_, bf16[2048,256]{1,0:T(8,128)(2,1)S(1)} %copy-done.4, bf16[128,2048]{1,0:T(8,128)(2,1)S(1)} %copy-done, bf16[128,2048]{1,0:T(8,128)(2,1)S(1)} %copy-done.2), custom_call_target="tpu_custom_call" | custom-call | flops 100000000 | bytes 3145728 | tf_op jit(solution)/shard_map/pallas_call | solution.py:60
  32.7 2.3 %collective-permute-start.11 = (bf16[1024,256]{1,0:T(8,128)(2,1)S(1)}, bf16[1024,256]{1,0:T(8,128)(2,1)}, u32[]{:S(2)}, u32[]{:S(2)}) collective-permute-start(bf16[1024,256]{1,0:T(8,128)(2,1)S(1)} %get-tuple-element.20), channel_id=1, source_target_pairs={{0,1},{1,0},{2,3},{3,2},{4,5},{5,4},{6,7},{7,6},{8,9},{9,8},{10,11... | collective-permute-start | bytes 1572872 | tf_op jit(solution)/shard_map/ppermute | solution.py:44
  35.2 0.4 collective-permute-start.17
  35.6 2.9 %collective-permute-start.2 = (bf16[512,256]{1,0:T(8,128)(2,1)S(1)}, bf16[512,256]{1,0:T(8,128)(2,1)S(1)}, u32[]{:S(2)}, u32[]{:S(2)}) collective-permute-start(bf16[512,256]{1,0:T(8,128)(2,1)S(1)} %get-tuple-element.19), channel_id=1, source_target_pairs={{0,4},{1,5},{2,6},{3,7},{4,0},{5,1},{6,2},{7,3},{8,12},{9,13},{10,... | collective-permute-start | bytes 786440 | tf_op jit(solution)/shard_map/ppermute | solution.py:40
  38.5 0.4 collective-permute-start.20
  38.9 0.8 collective-permute-done.20.refs_18_
  39.7 0.4 collective-permute-start
  40.1 4.9 %collective-permute-done.2.c = bf16[512,256]{1,0:T(8,128)(2,1)S(1)} collective-permute-done((bf16[512,256]{1,0:T(8,128)(2,1)S(1)}, bf16[512,256]{1,0:T(8,128)(2,1)S(1)}, u32[]{:S(2)}, u32[]{:S(2)}) %collective-permute-start.2) | collective-permute-done | bytes 262176 | tf_op jit(solution)/shard_map/ppermute | solution.py:40
  45.0 2.7 %collective-permute-start.1 = (bf16[1536,256]{1,0:T(8,128)(2,1)S(1)}, bf16[1536,256]{1,0:T(8,128)(2,1)S(1)}, u32[]{:S(2)}, u32[]{:S(2)}) collective-permute-start(bf16[1536,256]{1,0:T(8,128)(2,1)S(1)} %get-tuple-element.18.refs_0_), channel_id=1, source_target_pairs={{0,6},{1,7},{2,0},{3,1},{4,2},{5,3},{6,4},{7,5},{8,14},{9,15},{10,... | collective-permute-start | bytes 2359304 | tf_op jit(solution)/shard_map/ppermute | solution.py:40
  47.7 1.1 collective-permute-start.18
  48.9 1.1 collective-permute-start.13
  50.0 0.7 collective-permute-done.18.refs_14_
  50.7 5.9 %all-to-all-done.1 = bf16[16,4,64,256]{3,2,1,0:T(8,128)(2,1)} async-done(((bf16[16,4,64,256]{3,2,1,0:T(8,128)(2,1)}), bf16[16,4,64,256]{3,2,1,0:T(8,128)(2,1)}, u32[]{:S(2)}, u32[]{:S(2)}) %all-to-all-start.1) | async-done | bytes 2097184 | tf_op jit(solution)/shard_map/all_to_all | solution.py:465
  56.6 5.0 %collective-permute-start.21 = (bf16[64,64,256]{2,1,0:T(8,128)(2,1)}, bf16[64,64,256]{2,1,0:T(8,128)(2,1)}, u32[]{:S(2)}, u32[]{:S(2)}) collective-permute-start(bf16[64,64,256]{2,1,0:T(8,128)(2,1)} %bitcast.19.tab_m), channel_id=1, source_target_pairs={{0,1},{1,0},{2,3},{3,2},{4,5},{5,4},{6,7},{7,6},{8,9},{9,8},{10,11... | collective-permute-start | bytes 6291464 | tf_op jit(solution)/shard_map/ppermute | solution.py:44
  61.6 0.6 collective-permute-done.a.refs_2_
  62.2 1.0 collective-permute-start.12
  63.2 11.9 %collective-permute-done.13.refs_5_ = bf16[1024,256]{1,0:T(8,128)(2,1)} collective-permute-done((bf16[1024,256]{1,0:T(8,128)(2,1)}, bf16[1024,256]{1,0:T(8,128)(2,1)}, u32[]{:S(2)}, u32[]{:S(2)}) %collective-permute-start.13) | collective-permute-done | bytes 524320 | tf_op jit(solution)/shard_map/ppermute | solution.py:40
  75.1 3.4 %collective-permute-start.15 = (bf16[1024,256]{1,0:T(8,128)(2,1)}, bf16[1024,256]{1,0:T(8,128)(2,1)S(1)}, u32[]{:S(2)}, u32[]{:S(2)}) collective-permute-start(bf16[1024,256]{1,0:T(8,128)(2,1)} %collective-permute-done.13.refs_5_), channel_id=1, source_target_pairs={{0,6},{1,7},{2,0},{3,1},{4,2},{5,3},{6,4},{7,5},{8,14},{9,15},{10,... | collective-permute-start | bytes 1572872 | tf_op jit(solution)/shard_map/ppermute | solution.py:40
  78.6 0.6 shard_map.137.refs_2_
  79.2 0.8 copy-done.8
  80.0 3.0 %collective-permute-start.5 = (bf16[192,2048]{1,0:T(8,128)(2,1)S(1)}, bf16[192,2048]{1,0:T(8,128)(2,1)S(1)}, u32[]{:S(2)}, u32[]{:S(2)}) collective-permute-start(bf16[192,2048]{1,0:T(8,128)(2,1)S(1)} %shard_map.137.refs_2_), channel_id=1, source_target_pairs={{0,16},{1,65},{2,18},{3,67},{4,20},{5,69},{6,22},{7,71},{8,24},{9,... | collective-permute-start | bytes 2359304 | tf_op jit(solution)/shard_map/ppermute | solution.py:48
  83.3 5.1 %collective-permute-done.15.refs_7_ = bf16[1024,256]{1,0:T(8,128)(2,1)S(1)} collective-permute-done((bf16[1024,256]{1,0:T(8,128)(2,1)}, bf16[1024,256]{1,0:T(8,128)(2,1)S(1)}, u32[]{:S(2)}, u32[]{:S(2)}) %collective-permute-start.15) | collective-permute-done | bytes 524320 | tf_op jit(solution)/shard_map/ppermute | solution.py:40
  88.4 2.7 %collective-permute-start.4 = (bf16[192,2048]{1,0:T(8,128)(2,1)S(1)}, bf16[192,2048]{1,0:T(8,128)(2,1)}, u32[]{:S(2)}, u32[]{:S(2)}) collective-permute-start(bf16[192,2048]{1,0:T(8,128)(2,1)S(1)} %shard_map.137.refs_2_), channel_id=1, source_target_pairs={{0,24},{1,97},{2,26},{3,99},{4,28},{5,101},{6,30},{7,103},{8,0},{9... | collective-permute-start | bytes 2359304 | tf_op jit(solution)/shard_map/ppermute | solution.py:48
  91.2 5.9 %collective-permute-done.14.refs_6_ = bf16[1536,256]{1,0:T(8,128)(2,1)S(1)} collective-permute-done((bf16[1536,256]{1,0:T(8,128)(2,1)S(1)}, bf16[1536,256]{1,0:T(8,128)(2,1)S(1)}, u32[]{:S(2)}, u32[]{:S(2)}) %collective-permute-start.14) | collective-permute-done | bytes 786464 | tf_op jit(solution)/shard_map/ppermute | solution.py:40
  97.0 1.0 copy-done.14
  98.0 2.7 %collective-permute-start.7 = (bf16[192,2048]{1,0:T(8,128)(2,1)S(1)}, bf16[192,2048]{1,0:T(8,128)(2,1)}, u32[]{:S(2)}, u32[]{:S(2)}) collective-permute-start(bf16[192,2048]{1,0:T(8,128)(2,1)S(1)} %shard_map.137.refs_2_), channel_id=1, source_target_pairs={{0,1},{1,0},{2,3},{3,2},{4,5},{5,4},{6,7},{7,6},{8,9},{9,8},{10,11... | collective-permute-start | bytes 2359304 | tf_op jit(solution)/shard_map/ppermute | solution.py:44
  100.7 0.6 stack.71.sc
  101.4 2.6 %collective-permute-start.8 = (bf16[192,2048]{1,0:T(8,128)(2,1)}, bf16[192,2048]{1,0:T(8,128)(2,1)}, u32[]{:S(2)}, u32[]{:S(2)}) collective-permute-start(bf16[192,2048]{1,0:T(8,128)(2,1)} %collective-permute-done.3.refs_3_), channel_id=1, source_target_pairs={{0,1},{1,0},{2,3},{3,2},{4,5},{5,4},{6,7},{7,6},{8,9},{9,8},{10,11... | collective-permute-start | bytes 2359304 | tf_op jit(solution)/shard_map/ppermute | solution.py:44
  104.2 12.4 %shard_map.138 = (bf16[1024,256]{1,0:T(8,128)(2,1)}, bf16[256,256]{1,0:T(8,128)(2,1)}, bf16[256,256]{1,0:T(8,128)(2,1)}, bf16[256,256]{1,0:T(8,128)(2,1)}, bf16[256,256]{1,0:T(8,128)(2,1)}, /*index=5*/f32[256,2]{1,0:T(8,128)}) custom-call(s32[12]{0:T(128)} %stack.71.sc, bf16[1536,256]{1,0:T(8,128)(2,1)} %copy-done.12, ...), custom_call_target="tpu_custom_call" | custom-call | flops 4294967296 | bytes 10485760 | tf_op jit(solution)/shard_map/pallas_call | solution.py:60
  116.6 6.6 %collective-permute-done.26.refs_12_ = bf16[256,256]{1,0:T(8,128)(2,1)S(1)} collective-permute-done((bf16[256,256]{1,0:T(8,128)(2,1)}, bf16[256,256]{1,0:T(8,128)(2,1)S(1)}, u32[]{:S(2)}, u32[]{:S(2)}) %collective-permute-start.26) | collective-permute-done | bytes 131104 | tf_op jit(solution)/shard_map/ppermute | solution.py:40
  123.3 1.2 collective-permute-start.27
  124.5 2.8 %collective-permute-done.27.refs_13_ = bf16[256,256]{1,0:T(8,128)(2,1)S(1)} collective-permute-done((bf16[256,256]{1,0:T(8,128)(2,1)}, bf16[256,256]{1,0:T(8,128)(2,1)S(1)}, u32[]{:S(2)}, u32[]{:S(2)}) %collective-permute-start.27) | collective-permute-done | bytes 131104 | tf_op jit(solution)/shard_map/ppermute | solution.py:40
  127.3 2.1 %collective-permute-start.6 = (bf16[128,2048]{1,0:T(8,128)(2,1)}, bf16[128,2048]{1,0:T(8,128)(2,1)S(1)}, u32[]{:S(2)}, u32[]{:S(2)}) collective-permute-start(bf16[128,2048]{1,0:T(8,128)(2,1)} %refs_1_.3), channel_id=1, source_target_pairs={{0,1},{1,0},{2,3},{3,2},{4,5},{5,4},{6,7},{7,6},{8,9},{9,8},{10,11... | collective-permute-start | bytes 1572872 | tf_op jit(solution)/shard_map/ppermute | solution.py:44
  129.4 0.9 collective-permute-start.28
  130.8 1.0 copy-done.10
  131.8 3.1 %shard_map.140 = (bf16[256,256]{1,0:T(8,128)(2,1)S(1)}, bf16[256,256]{1,0:T(8,128)(2,1)S(1)}, bf16[256,256]{1,0:T(8,128)(2,1)S(1)}, bf16[256,256]{1,0:T(8,128)(2,1)S(1)}) custom-call(s32[20]{0:T(128)S(1)} %concatenate.3.sc, bf16[1024,256]{1,0:T(8,128)(2,1)S(1)} %copy-done.10, bf16[64,64,256]{2,1,0:T(8,128)(2,1)} %bitcast.19.tab_m, ...), custom_call_target="tpu_custom_call" | custom-call | flops 1000000000 | bytes 5242880 | tf_op jit(solution)/shard_map/pallas_call | solution.py:60
  135.0 1.2 collective-permute-done.28.refs_14_
  136.2 1.2 collective-permute-start.22
  137.4 1.5 collective-permute-start.23
  138.8 1.3 collective-permute-start.24
  140.2 5.3 %shard_map.141.refs_16_ = f32[256,2048]{1,0:T(8,128)S(1)} custom-call(s32[3]{0:T(128)S(1)} %pad_add_fusion.sc.refs_0_, bf16[128,2048]{1,0:T(8,128)(2,1)S(1)} %copy-done.1, bf16[192,2048]{1,0:T(8,128)(2,1)S(1)} %shard_map.137.refs_2_, bf16[192,2048]{1,0:T(8,128)(2,1)} %collective-permute-done.3.refs_3_, bf16[192,2048]{1,0:T(8,128)(2,1)} %collective-permute-done.4.refs_4_, ...), custom_call_target="tpu_custom_call" | custom-call | flops 1073741824 | bytes 7340032 | tf_op jit(solution)/shard_map/pallas_call | solution.py:60
  145.5 0.3 collective-permute-done.24.refs_14_
  145.9 6.2 %shard_map.142 = bf16[256,2048]{1,0:T(8,128)(2,1)} custom-call(s32[3]{0:T(128)S(1)} %pad_add_fusion.sc.refs_0_, bf16[128,2048]{1,0:T(8,128)(2,1)S(1)} %copy-done.3, bf16[192,2048]{1,0:T(8,128)(2,1)S(1)} %shard_map.137.refs_2_, bf16[192,2048]{1,0:T(8,128)(2,1)} %collective-permute-done.3.refs_3_, bf16[192,2048]{1,0:T(8,128)(2,1)} %collective-permute-done.4.refs_4_, ...), custom_call_target="tpu_custom_call" | custom-call | flops 1073741824 | bytes 7340032 | tf_op jit(solution)/shard_map/pallas_call | solution.py:60
  (77 shorter events, 2.1 us)
Async XLA Ops:
  25.5 4.7 %copy-start = (bf16[128,2048]{1,0:T(8,128)(2,1)S(1)}, bf16[128,2048]{1,0:T(8,128)(2,1)}, u32[]{:S(2)}) copy-start(bf16[128,2048]{1,0:T(8,128)(2,1)} %refs_1_.2) | copy-start | bytes 1572868
  25.5 4.7 %copy-start.2 = (bf16[128,2048]{1,0:T(8,128)(2,1)S(1)}, bf16[128,2048]{1,0:T(8,128)(2,1)}, u32[]{:S(2)}) copy-start(bf16[128,2048]{1,0:T(8,128)(2,1)} %refs_1_.3) | copy-start | bytes 1572868
  25.5 4.7 %copy-start.4 = (bf16[2048,256]{1,0:T(8,128)(2,1)S(1)}, bf16[2048,256]{1,0:T(8,128)(2,1)}, u32[]{:S(2)}) copy-start(bf16[2048,256]{1,0:T(8,128)(2,1)} %tokens.1) | copy-start | bytes 3145732
  25.5 31.1 %all-to-all-start.1 = ((bf16[16,4,64,256]{3,2,1,0:T(8,128)(2,1)}), bf16[16,4,64,256]{3,2,1,0:T(8,128)(2,1)}, u32[]{:S(2)}, u32[]{:S(2)}) async-start(bf16[16,4,64,256]{3,2,1,0:T(8,128)(2,1)} %shard_map.139), calls=%async_computation.1 | async-start | bytes 4194304 | tf_op jit(solution)/shard_map/all_to_all | solution.py:465
  30.1 8.4 %copy-start.17 = (bf16[3,128]{1,0:T(4,128)(2,1)S(1)}, bf16[3,128]{1,0:T(4,128)(2,1)}, u32[]{:S(2)}) copy-start(bf16[3,128]{1,0:T(4,128)(2,1)} %refs_17_.1) | copy-start | bytes 2308
  32.7 45.8 %copy-start.12 = (bf16[1536,256]{1,0:T(8,128)(2,1)}, bf16[1536,256]{1,0:T(8,128)(2,1)S(1)}, u32[]{:S(2)}) copy-start(bf16[1536,256]{1,0:T(8,128)(2,1)S(1)} %get-tuple-element.18.refs_0_) | copy-start | bytes 2359300
  32.7 15.0 %collective-permute-start.11 = (bf16[1024,256]{1,0:T(8,128)(2,1)S(1)}, bf16[1024,256]{1,0:T(8,128)(2,1)}, u32[]{:S(2)}, u32[]{:S(2)}) collective-permute-start(bf16[1024,256]{1,0:T(8,128)(2,1)S(1)} %get-tuple-element.20), channel_id=1, source_target_pairs={{0,1},{1,0},{2,3},{3,2},{4,5},{5,4},{6,7},{7,6},{8,9},{9,8},{10,11... | collective-permute-start | bytes 1572872 | tf_op jit(solution)/shard_map/ppermute | solution.py:44
  35.1 13.8 %collective-permute-start.16 = (bf16[2048,128]{1,0:T(8,128)(2,1)}, bf16[2048,128]{1,0:T(8,128)(2,1)}, u32[]{:S(2)}, u32[]{:S(2)}) collective-permute-start(bf16[2048,128]{1,0:T(8,128)(2,1)} %refs_8_.1), channel_id=1, source_target_pairs={{0,1},{1,0},{2,3},{3,2},{4,5},{5,4},{6,7},{7,6},{8,9},{9,8},{10,11... | collective-permute-start | bytes 1572872 | tf_op jit(solution)/shard_map/ppermute | solution.py:44
  35.2 13.8 %collective-permute-start.17 = (bf16[2048,128]{1,0:T(8,128)(2,1)}, bf16[2048,128]{1,0:T(8,128)(2,1)}, u32[]{:S(2)}, u32[]{:S(2)}) collective-permute-start(bf16[2048,128]{1,0:T(8,128)(2,1)} %refs_9_.1), channel_id=1, source_target_pairs={{0,1},{1,0},{2,3},{3,2},{4,5},{5,4},{6,7},{7,6},{8,9},{9,8},{10,11... | collective-permute-start | bytes 1572872 | tf_op jit(solution)/shard_map/ppermute | solution.py:44
  35.6 9.4 %collective-permute-start.2 = (bf16[512,256]{1,0:T(8,128)(2,1)S(1)}, bf16[512,256]{1,0:T(8,128)(2,1)S(1)}, u32[]{:S(2)}, u32[]{:S(2)}) collective-permute-start(bf16[512,256]{1,0:T(8,128)(2,1)S(1)} %get-tuple-element.19), channel_id=1, source_target_pairs={{0,4},{1,5},{2,6},{3,7},{4,0},{5,1},{6,2},{7,3},{8,12},{9,13},{10,... | collective-permute-start | bytes 786440 | tf_op jit(solution)/shard_map/ppermute | solution.py:40
  38.5 1.2 collective-permute-start.20
  39.7 64.5 %copy-start.18 = (bf16[3,128]{1,0:T(4,128)(2,1)}, bf16[3,128]{1,0:T(4,128)(2,1)S(1)}, u32[]{:S(2)}) copy-start(bf16[3,128]{1,0:T(4,128)(2,1)S(1)} %collective-permute-done.20.refs_18_) | copy-start | bytes 2308
  39.7 22.5 %collective-permute-start = (bf16[1536,256]{1,0:T(8,128)(2,1)S(1)}, bf16[1536,256]{1,0:T(8,128)(2,1)S(1)}, u32[]{:S(2)}, u32[]{:S(2)}) collective-permute-start(bf16[1536,256]{1,0:T(8,128)(2,1)S(1)} %get-tuple-element.18.refs_0_), channel_id=1, source_target_pairs={{0,2},{1,3},{2,4},{3,5},{4,6},{5,7},{6,0},{7,1},{8,10},{9,11},{10,... | collective-permute-start | bytes 2359304 | tf_op jit(solution)/shard_map/ppermute | solution.py:40
  45.0 33.5 %collective-permute-start.1 = (bf16[1536,256]{1,0:T(8,128)(2,1)S(1)}, bf16[1536,256]{1,0:T(8,128)(2,1)S(1)}, u32[]{:S(2)}, u32[]{:S(2)}) collective-permute-start(bf16[1536,256]{1,0:T(8,128)(2,1)S(1)} %get-tuple-element.18.refs_0_), channel_id=1, source_target_pairs={{0,6},{1,7},{2,0},{3,1},{4,2},{5,3},{6,4},{7,5},{8,14},{9,15},{10,... | collective-permute-start | bytes 2359304 | tf_op jit(solution)/shard_map/ppermute | solution.py:40
  47.7 3.0 %collective-permute-start.18 = (bf16[2048,128]{1,0:T(8,128)(2,1)}, bf16[2048,128]{1,0:T(8,128)(2,1)}, u32[]{:S(2)}, u32[]{:S(2)}) collective-permute-start(bf16[2048,128]{1,0:T(8,128)(2,1)} %refs_10_.1), channel_id=1, source_target_pairs={{0,1},{1,0},{2,3},{3,2},{4,5},{5,4},{6,7},{7,6},{8,9},{9,8},{10,11... | collective-permute-start | bytes 1572872 | tf_op jit(solution)/shard_map/ppermute | solution.py:44
  48.8 12.7 %collective-permute-start.19 = (bf16[2048,128]{1,0:T(8,128)(2,1)}, bf16[2048,128]{1,0:T(8,128)(2,1)}, u32[]{:S(2)}, u32[]{:S(2)}) collective-permute-start(bf16[2048,128]{1,0:T(8,128)(2,1)} %refs_11_.1), channel_id=1, source_target_pairs={{0,1},{1,0},{2,3},{3,2},{4,5},{5,4},{6,7},{7,6},{8,9},{9,8},{10,11... | collective-permute-start | bytes 1572872 | tf_op jit(solution)/shard_map/ppermute | solution.py:44
  48.9 26.2 %collective-permute-start.13 = (bf16[1024,256]{1,0:T(8,128)(2,1)}, bf16[1024,256]{1,0:T(8,128)(2,1)}, u32[]{:S(2)}, u32[]{:S(2)}) collective-permute-start(bf16[1024,256]{1,0:T(8,128)(2,1)} %collective-permute-done.11.refs_1_), channel_id=1, source_target_pairs={{0,6},{1,7},{2,0},{3,1},{4,2},{5,3},{6,4},{7,5},{8,14},{9,15},{10,... | collective-permute-start | bytes 1572872 | tf_op jit(solution)/shard_map/ppermute | solution.py:40
  56.6 72.8 %collective-permute-start.21 = (bf16[64,64,256]{2,1,0:T(8,128)(2,1)}, bf16[64,64,256]{2,1,0:T(8,128)(2,1)}, u32[]{:S(2)}, u32[]{:S(2)}) collective-permute-start(bf16[64,64,256]{2,1,0:T(8,128)(2,1)} %bitcast.19.tab_m), channel_id=1, source_target_pairs={{0,1},{1,0},{2,3},{3,2},{4,5},{5,4},{6,7},{7,6},{8,9},{9,8},{10,11... | collective-permute-start | bytes 6291464 | tf_op jit(solution)/shard_map/ppermute | solution.py:44
  61.6 17.6 %collective-permute-start.25 = (bf16[128,2048]{1,0:T(8,128)(2,1)S(1)}, bf16[128,2048]{1,0:T(8,128)(2,1)S(1)}, u32[]{:S(2)}, u32[]{:S(2)}) collective-permute-start(bf16[128,2048]{1,0:T(8,128)(2,1)S(1)} %copy-done), channel_id=1, source_target_pairs={{0,1},{1,0},{2,3},{3,2},{4,5},{5,4},{6,7},{7,6},{8,9},{9,8},{10,11... | collective-permute-start | bytes 1572872 | tf_op jit(solution)/shard_map/ppermute | solution.py:44
  62.2 41.8 %copy-start.5 = (bf16[1536,256]{1,0:T(8,128)(2,1)}, bf16[1536,256]{1,0:T(8,128)(2,1)S(1)}, u32[]{:S(2)}) copy-start(bf16[1536,256]{1,0:T(8,128)(2,1)S(1)} %collective-permute-done.a.refs_2_) | copy-start | bytes 2359300
  62.2 20.8 %collective-permute-start.12 = (bf16[1024,256]{1,0:T(8,128)(2,1)}, bf16[1024,256]{1,0:T(8,128)(2,1)S(1)}, u32[]{:S(2)}, u32[]{:S(2)}) collective-permute-start(bf16[1024,256]{1,0:T(8,128)(2,1)} %collective-permute-done.11.refs_1_), channel_id=1, source_target_pairs={{0,2},{1,3},{2,4},{3,5},{4,6},{5,7},{6,0},{7,1},{8,10},{9,11},{10,... | collective-permute-start | bytes 1572872 | tf_op jit(solution)/shard_map/ppermute | solution.py:40
  75.1 13.3 %collective-permute-start.15 = (bf16[1024,256]{1,0:T(8,128)(2,1)}, bf16[1024,256]{1,0:T(8,128)(2,1)S(1)}, u32[]{:S(2)}, u32[]{:S(2)}) collective-permute-start(bf16[1024,256]{1,0:T(8,128)(2,1)} %collective-permute-done.13.refs_5_), channel_id=1, source_target_pairs={{0,6},{1,7},{2,0},{3,1},{4,2},{5,3},{6,4},{7,5},{8,14},{9,15},{10,... | collective-permute-start | bytes 1572872 | tf_op jit(solution)/shard_map/ppermute | solution.py:40
  78.5 25.7 %copy-start.6 = (bf16[1536,256]{1,0:T(8,128)(2,1)}, bf16[1536,256]{1,0:T(8,128)(2,1)S(1)}, u32[]{:S(2)}) copy-start(bf16[1536,256]{1,0:T(8,128)(2,1)S(1)} %collective-permute-done.1.b.refs_3_) | copy-start | bytes 2359300
  78.5 18.5 %collective-permute-start.14 = (bf16[1536,256]{1,0:T(8,128)(2,1)S(1)}, bf16[1536,256]{1,0:T(8,128)(2,1)S(1)}, u32[]{:S(2)}, u32[]{:S(2)}) collective-permute-start(bf16[1536,256]{1,0:T(8,128)(2,1)S(1)} %collective-permute-done.a.refs_2_), channel_id=1, source_target_pairs={{0,2},{1,3},{2,4},{3,5},{4,6},{5,7},{6,0},{7,1},{8,10},{9,11},{10,... | collective-permute-start | bytes 2359304 | tf_op jit(solution)/shard_map/ppermute | solution.py:40
  80.0 21.4 %collective-permute-start.5 = (bf16[192,2048]{1,0:T(8,128)(2,1)S(1)}, bf16[192,2048]{1,0:T(8,128)(2,1)S(1)}, u32[]{:S(2)}, u32[]{:S(2)}) collective-permute-start(bf16[192,2048]{1,0:T(8,128)(2,1)S(1)} %shard_map.137.refs_2_), channel_id=1, source_target_pairs={{0,16},{1,65},{2,18},{3,67},{4,20},{5,69},{6,22},{7,71},{8,24},{9,... | collective-permute-start | bytes 2359304 | tf_op jit(solution)/shard_map/ppermute | solution.py:48
  83.0 14.0 %copy-start.15 = (bf16[1024,256]{1,0:T(8,128)(2,1)}, bf16[1024,256]{1,0:T(8,128)(2,1)S(1)}, u32[]{:S(2)}) copy-start(bf16[1024,256]{1,0:T(8,128)(2,1)S(1)} %collective-permute-done.12.refs_4_) | copy-start | bytes 1572868
  83.0 18.4 %collective-permute-start.3 = (bf16[192,2048]{1,0:T(8,128)(2,1)S(1)}, bf16[192,2048]{1,0:T(8,128)(2,1)}, u32[]{:S(2)}, u32[]{:S(2)}) collective-permute-start(bf16[192,2048]{1,0:T(8,128)(2,1)S(1)} %shard_map.137.refs_2_), channel_id=1, source_target_pairs={{0,8},{1,33},{2,10},{3,35},{4,12},{5,37},{6,14},{7,39},{8,16},{9,4... | collective-permute-start | bytes 2359304 | tf_op jit(solution)/shard_map/ppermute | solution.py:48
  88.4 8.6 %copy-start.16 = (bf16[1024,256]{1,0:T(8,128)(2,1)}, bf16[1024,256]{1,0:T(8,128)(2,1)S(1)}, u32[]{:S(2)}) copy-start(bf16[1024,256]{1,0:T(8,128)(2,1)S(1)} %collective-permute-done.15.refs_7_) | copy-start | bytes 1572868
  88.4 15.6 %collective-permute-start.4 = (bf16[192,2048]{1,0:T(8,128)(2,1)S(1)}, bf16[192,2048]{1,0:T(8,128)(2,1)}, u32[]{:S(2)}, u32[]{:S(2)}) collective-permute-start(bf16[192,2048]{1,0:T(8,128)(2,1)S(1)} %shard_map.137.refs_2_), channel_id=1, source_target_pairs={{0,24},{1,97},{2,26},{3,99},{4,28},{5,101},{6,30},{7,103},{8,0},{9... | collective-permute-start | bytes 2359304 | tf_op jit(solution)/shard_map/ppermute | solution.py:48
  97.0 1.0 copy-start.14
  98.0 18.6 %collective-permute-start.7 = (bf16[192,2048]{1,0:T(8,128)(2,1)S(1)}, bf16[192,2048]{1,0:T(8,128)(2,1)}, u32[]{:S(2)}, u32[]{:S(2)}) collective-permute-start(bf16[192,2048]{1,0:T(8,128)(2,1)S(1)} %shard_map.137.refs_2_), channel_id=1, source_target_pairs={{0,1},{1,0},{2,3},{3,2},{4,5},{5,4},{6,7},{7,6},{8,9},{9,8},{10,11... | collective-permute-start | bytes 2359304 | tf_op jit(solution)/shard_map/ppermute | solution.py:44
  101.4 36.0 %collective-permute-start.10 = (bf16[192,2048]{1,0:T(8,128)(2,1)S(1)}, bf16[192,2048]{1,0:T(8,128)(2,1)}, u32[]{:S(2)}, u32[]{:S(2)}) collective-permute-start(bf16[192,2048]{1,0:T(8,128)(2,1)S(1)} %collective-permute-done.5.refs_5_), channel_id=1, source_target_pairs={{0,1},{1,0},{2,3},{3,2},{4,5},{5,4},{6,7},{7,6},{8,9},{9,8},{10,11... | collective-permute-start | bytes 2359304 | tf_op jit(solution)/shard_map/ppermute | solution.py:44
  101.4 37.5 %collective-permute-start.8 = (bf16[192,2048]{1,0:T(8,128)(2,1)}, bf16[192,2048]{1,0:T(8,128)(2,1)}, u32[]{:S(2)}, u32[]{:S(2)}) collective-permute-start(bf16[192,2048]{1,0:T(8,128)(2,1)} %collective-permute-done.3.refs_3_), channel_id=1, source_target_pairs={{0,1},{1,0},{2,3},{3,2},{4,5},{5,4},{6,7},{7,6},{8,9},{9,8},{10,11... | collective-permute-start | bytes 2359304 | tf_op jit(solution)/shard_map/ppermute | solution.py:44
  104.0 36.1 %collective-permute-start.9 = (bf16[192,2048]{1,0:T(8,128)(2,1)}, bf16[192,2048]{1,0:T(8,128)(2,1)}, u32[]{:S(2)}, u32[]{:S(2)}) collective-permute-start(bf16[192,2048]{1,0:T(8,128)(2,1)} %collective-permute-done.4.refs_4_), channel_id=1, source_target_pairs={{0,1},{1,0},{2,3},{3,2},{4,5},{5,4},{6,7},{7,6},{8,9},{9,8},{10,11... | collective-permute-start | bytes 2359304 | tf_op jit(solution)/shard_map/ppermute | solution.py:44
  104.2 26.1 %copy-start.13 = (s32[16,2]{0,1:T(2,128)S(1)}, s32[16,2]{0,1:T(2,128)}, u32[]{:S(2)}) copy-start(s32[16,2]{0,1:T(2,128)} %param.16) | copy-start | bytes 388
  116.6 6.7 %collective-permute-start.26 = (bf16[256,256]{1,0:T(8,128)(2,1)}, bf16[256,256]{1,0:T(8,128)(2,1)S(1)}, u32[]{:S(2)}, u32[]{:S(2)}) collective-permute-start(bf16[256,256]{1,0:T(8,128)(2,1)} %get-tuple-element.28), channel_id=1, source_target_pairs={{0,2},{1,3},{2,4},{3,5},{4,6},{5,7},{6,0},{7,1},{8,10},{9,11},{10,... | collective-permute-start | bytes 393224 | tf_op jit(solution)/shard_map/ppermute | solution.py:40
  123.3 4.0 %collective-permute-start.27 = (bf16[256,256]{1,0:T(8,128)(2,1)}, bf16[256,256]{1,0:T(8,128)(2,1)S(1)}, u32[]{:S(2)}, u32[]{:S(2)}) collective-permute-start(bf16[256,256]{1,0:T(8,128)(2,1)} %get-tuple-element.29), channel_id=1, source_target_pairs={{0,6},{1,7},{2,0},{3,1},{4,2},{5,3},{6,4},{7,5},{8,14},{9,15},{10,... | collective-permute-start | bytes 393224 | tf_op jit(solution)/shard_map/ppermute | solution.py:40
  127.3 18.2 %collective-permute-start.6 = (bf16[128,2048]{1,0:T(8,128)(2,1)}, bf16[128,2048]{1,0:T(8,128)(2,1)S(1)}, u32[]{:S(2)}, u32[]{:S(2)}) collective-permute-start(bf16[128,2048]{1,0:T(8,128)(2,1)} %refs_1_.3), channel_id=1, source_target_pairs={{0,1},{1,0},{2,3},{3,2},{4,5},{5,4},{6,7},{7,6},{8,9},{9,8},{10,11... | collective-permute-start | bytes 1572872 | tf_op jit(solution)/shard_map/ppermute | solution.py:44
  129.4 6.8 %collective-permute-start.28 = (bf16[256,256]{1,0:T(8,128)(2,1)}, bf16[256,256]{1,0:T(8,128)(2,1)S(1)}, u32[]{:S(2)}, u32[]{:S(2)}) collective-permute-start(bf16[256,256]{1,0:T(8,128)(2,1)} %get-tuple-element.30), channel_id=1, source_target_pairs={{0,4},{1,5},{2,6},{3,7},{4,0},{5,1},{6,2},{7,3},{8,12},{9,13},{10,... | collective-permute-start | bytes 393224 | tf_op jit(solution)/shard_map/ppermute | solution.py:40
  130.8 1.0 copy-start.10
  131.8 8.3 %copy-start.1 = (bf16[128,2048]{1,0:T(8,128)(2,1)S(1)}, bf16[128,2048]{1,0:T(8,128)(2,1)}, u32[]{:S(2)}) copy-start(bf16[128,2048]{1,0:T(8,128)(2,1)} %refs_1_.2) | copy-start | bytes 1572868
  131.8 8.3 %copy-start.7 = (f32[256,2]{1,0:T(8,128)S(1)}, f32[256,2]{1,0:T(8,128)}, u32[]{:S(2)}) copy-start(f32[256,2]{1,0:T(8,128)} %get-tuple-element.26.refs_15_) | copy-start | bytes 6148
  131.8 8.3 %copy-start.9 = (bf16[128,2048]{1,0:T(8,128)(2,1)S(1)}, bf16[128,2048]{1,0:T(8,128)(2,1)}, u32[]{:S(2)}) copy-start(bf16[128,2048]{1,0:T(8,128)(2,1)} %copy-done.8) | copy-start | bytes 1572868
  131.8 8.3 %copy-start.11 = (bf16[256,256]{1,0:T(8,128)(2,1)S(1)}, bf16[256,256]{1,0:T(8,128)(2,1)}, u32[]{:S(2)}) copy-start(bf16[256,256]{1,0:T(8,128)(2,1)} %get-tuple-element.27.refs_11_) | copy-start | bytes 393220
  136.2 9.4 %collective-permute-start.22 = (bf16[256,256]{1,0:T(8,128)(2,1)S(1)}, bf16[256,256]{1,0:T(8,128)(2,1)S(1)}, u32[]{:S(2)}, u32[]{:S(2)}) collective-permute-start(bf16[256,256]{1,0:T(8,128)(2,1)S(1)} %get-tuple-element.23), channel_id=1, source_target_pairs={{0,2},{1,3},{2,4},{3,5},{4,6},{5,7},{6,0},{7,1},{8,10},{9,11},{10,... | collective-permute-start | bytes 393224 | tf_op jit(solution)/shard_map/ppermute | solution.py:40
  137.4 8.2 %collective-permute-start.23 = (bf16[256,256]{1,0:T(8,128)(2,1)S(1)}, bf16[256,256]{1,0:T(8,128)(2,1)S(1)}, u32[]{:S(2)}, u32[]{:S(2)}) collective-permute-start(bf16[256,256]{1,0:T(8,128)(2,1)S(1)} %get-tuple-element.24), channel_id=1, source_target_pairs={{0,6},{1,7},{2,0},{3,1},{4,2},{5,3},{6,4},{7,5},{8,14},{9,15},{10,... | collective-permute-start | bytes 393224 | tf_op jit(solution)/shard_map/ppermute | solution.py:40
  138.8 7.0 %collective-permute-start.24 = (bf16[256,256]{1,0:T(8,128)(2,1)S(1)}, bf16[256,256]{1,0:T(8,128)(2,1)S(1)}, u32[]{:S(2)}, u32[]{:S(2)}) collective-permute-start(bf16[256,256]{1,0:T(8,128)(2,1)S(1)} %get-tuple-element.25), channel_id=1, source_target_pairs={{0,4},{1,5},{2,6},{3,7},{4,0},{5,1},{6,2},{7,3},{8,12},{9,13},{10,... | collective-permute-start | bytes 393224 | tf_op jit(solution)/shard_map/ppermute | solution.py:40
  140.1 5.7 %copy-start.3 = (bf16[128,2048]{1,0:T(8,128)(2,1)S(1)}, bf16[128,2048]{1,0:T(8,128)(2,1)}, u32[]{:S(2)}) copy-start(bf16[128,2048]{1,0:T(8,128)(2,1)} %refs_1_.3) | copy-start | bytes 1572868
  (1 other events, 0.8 us)

commit v4 on v3

--- a/solution.py
+++ b/solution.py
@@ -15,7 +15,7 @@
 N_Z = 4
 BF = jnp.bfloat16
 F32 = jnp.float32
-SERVE_VMEM, PROJECT_VMEM, ATTEND_VMEM, FINISH_VMEM, SMALL_VMEM = 58, 62, 8, 14, 6
+SERVE_VMEM, PROJECT_VMEM, ATTEND_VMEM, FINISH_VMEM, SMALL_VMEM, PREP_VMEM = 58, 62, 8, 14, 6, 62
 
 
 SHIFT = {
@@ -93,26 +93,28 @@
         c.wait()
 
 
-def prep_kernel(sc, tokens, conv_out, memory_out, slab, other, part, sems):
+def prep_kernel(sc, tokens, conv_out, memory_out, slab, other, part, quarter_s, sems):
     core, quarter = sc[2], sc[0]
     n = N_Y * SEQ_LEN
-    pairs = []
+    rows = pl.ds(pl.multiple_of(quarter * 32, 32), 32)
+    pairs = [
+        (conv_out.at[rows], quarter_s.at[pl.ds(0, 32)]),
+        (memory_out.at[rows], quarter_s.at[pl.ds(32, 32)]),
+    ]
     for j in range(N_Y):
         own = pl.multiple_of((2 * j + core) * SEQ_LEN, SEQ_LEN)
         away = pl.multiple_of((2 * j + 1 - core) * SEQ_LEN, SEQ_LEN)
         dst = pl.ds(j * SEQ_LEN, SEQ_LEN)
         pairs.append((tokens.at[pl.ds(own, SEQ_LEN)], slab.at[dst]))
         pairs.append((tokens.at[pl.ds(away, SEQ_LEN)], other.at[dst]))
-    rows = pl.ds(pl.multiple_of(quarter * 32, 32), 32)
-    for i, w in enumerate((conv_out, memory_out)):
-        for cb in range(8):
-            src = w.at[rows, pl.ds(cb * 256, 256)]
-            dst = cb * 64 + i * 32
-            pairs.append((src, slab.at[pl.ds(n + dst, 32)]))
-            pairs.append((src, part.at[pl.ds(dst, 32)]))
     copies = [pltpu.make_async_copy(x, y, sems.at[k]) for k, (x, y) in enumerate(pairs)]
     start(copies)
-    wait(copies)
+    wait(copies[:2])
+    for cb in range(8):
+        piece = quarter_s[:, cb * 256 : (cb + 1) * 256]
+        slab[n + cb * 64 : n + (cb + 1) * 64] = piece
+        part[cb * 64 : (cb + 1) * 64] = piece
+    wait(copies[2:])
 
 
 def prep(sc, tokens, conv_out, memory_out):
@@ -121,7 +123,8 @@
         prep_kernel, sc, (tokens, conv_out, memory_out), [HBM] * 3,
         [((n + 512, k), BF), ((n, k), BF), ((512, k), BF)],
         [fixed(n + 512, k), fixed(n, k), fixed(512, k)],
-        scratch=[pltpu.SemaphoreType.DMA((40,))], bytes_=3 * 2**20, flops=10**8, vmem=6,
+        scratch=[pltpu.VMEM((64, 2048), BF), pltpu.SemaphoreType.DMA((10,))],
+        bytes_=3 * 2**20, flops=10**8, vmem=PREP_VMEM,
     )
 
 
@@ -207,15 +210,15 @@
         for k, p in enumerate(pieces)
     ]
     wcopy = [
-        pltpu.make_async_copy(p, w.at[n // 2, :, pl.ds(n % 2 * H, H)], wsem.at[n])
+        pltpu.make_async_copy(p, w.at[n // 2, :, pl.ds(n % 2 * H, H)], wsem.at[n // 2])
         for n, p in enumerate(weights)
     ]
     start(lcopy)
     start(wcopy)
     wait(lcopy)
-    wait(wcopy)
 
     def product(n, carry):
+        pltpu.make_async_copy(w.at[n], w.at[n], wsem.at[n]).wait()
         acc[n] = dot(lhs[...], w[n])
         return carry
 
@@ -264,7 +267,7 @@
             pltpu.VMEM((rows, 256), BF),
             pltpu.VMEM((4, SEQ_LEN, 256), BF),
             pltpu.SemaphoreType.DMA((8,)),
-            pltpu.SemaphoreType.DMA((8,)),
+            pltpu.SemaphoreType.DMA((4,)),
             pltpu.SemaphoreType.DMA((5,)),
         ],
         flops=2 * rows * d * 1024, bytes_=10 * 2**20, vmem=PROJECT_VMEM,
@@ -329,75 +332,107 @@
     )
 
 
-def finish_kernel(branch, sc, *refs):
-    sides = (refs[0:5], refs[5:10])
-    parts, logits = refs[10:14], refs[14]
-    before = None if branch == 0 else refs[15]
-    out, w, x, o_s, sems, bsem, osem = refs[-7:]
-    copies = []
-    for side in range(2):
-        own, e, r1, r2, r3 = sides[side]
-        base = side * 128
-        copies.append((own, w.at[pl.ds(base, 128)]))
-        for src, back in ((e, 0), (r1, 3), (r2, 1), (r3, 2)):
-            quarter = lax.rem(sc[side] + back, 4)
-            row = pl.multiple_of(base + quarter * 32, 32)
-            for d in range(3):
-                copies.append(
-                    (src.at[pl.ds(d * 64 + branch * 32, 32)], w.at[pl.ds((1 + d) * 256 + row, 32)])
-                )
-    for d in range(4):
-        copies.append((parts[d], x.at[:, pl.ds(d * 256, 256)]))
-    copies = [pltpu.make_async_copy(a, b, sems.at[n]) for n, (a, b) in enumerate(copies)]
-    start(copies)
-    if before is not None:
-        bcopy = pltpu.make_async_copy(before, o_s, bsem)
-        bcopy.start()
+VM = pl.BlockSpec(memory_space=pltpu.VMEM)
+SM = pl.BlockSpec(memory_space=pltpu.SMEM)
+
+
+def plain_call(body, ins, in_specs, outs, out_specs, scratch, vmem):
+    return pl.pallas_call(
+        body,
+        in_specs=in_specs,
+        out_specs=out_specs,
+        out_shape=[jax.ShapeDtypeStruct(shape, dtype) for shape, dtype in outs],
+        scratch_shapes=scratch,
+        compiler_params=pltpu.CompilerParams(vmem_limit_bytes=vmem * 2**20),
+        cost_estimate=pl.CostEstimate(
+            flops=SEQ_LEN * 2048 * 2048, bytes_accessed=7 * 2**20, transcendentals=0
+        ),
+    )(*ins)
+
+
+def branch_product(parts, logits, branch, w, write):
     mix = jax.nn.sigmoid(logits[:, branch : branch + 1])
-    wait(copies)
-    if before is not None:
-        bcopy.wait()
+    x = jnp.concatenate([p[...] for p in parts], axis=1)
     step = 512
 
     def product(i, carry):
         cols = pl.ds(pl.multiple_of(i * step, step), step)
-        a = mix * dot(x[...], w[:, cols])
-        if before is None:
-            o_s[:, cols] = a
-        else:
-            refs[-8][:, cols] = (o_s[:, cols] + a).astype(BF)
+        write(i, cols, mix * dot(x, w[:, cols]))
         return carry
 
     lax.fori_loop(0, w.shape[1] // step, product, 0)
-    ocopy = pltpu.make_async_copy(o_s if before is None else refs[-8], out, osem.at[0])
-    ocopy.start()
-    ocopy.wait()
-
-
-def finish(branch, sc, mine, other, parts, logits, before=None):
-    width = mine[0].shape[1]
-    last = before is not None
-    ins = (*mine, *other, *parts, logits) + ((before,) if last else ())
-    scratch = [
-        pltpu.VMEM((1024, width), BF),
-        pltpu.VMEM((SEQ_LEN, 1024), BF),
-        pltpu.VMEM((SEQ_LEN, width), F32),
-        pltpu.SemaphoreType.DMA((30,)),
-        pltpu.SemaphoreType.DMA,
-        pltpu.SemaphoreType.DMA((width // 512,)),
-    ]
-
-    def body(*refs):
-        if not last:
-            return finish_kernel(branch, *refs)
-        return finish_kernel(branch, *refs[:-8], refs[-1], *refs[-8:-1])
-
-    return call(
-        body, sc, ins,
-        [HBM] * 14 + [whole(logits)] + ([HBM] if last else []),
-        [((SEQ_LEN, width), BF if last else F32)], [HBM],
-        scratch=scratch + ([pltpu.VMEM((SEQ_LEN, width), BF)] if last else []),
-        flops=SEQ_LEN * 2048 * 2048, bytes_=7 * 2**20, vmem=FINISH_VMEM,
+
+
+def finish0_kernel(sc, *refs):
+    owns, rings = refs[0:4], (refs[4:8], refs[8:12])
+    parts, logits = refs[12:16], refs[16]
+    acc, w1, w0, sems = refs[17:]
+    groups = []
+    for branch, w in enumerate((w0, w1)):
+        pairs = []
+        for side in range(2):
+            base = side * 128
+            pairs.append((owns[2 * branch + side], w.at[pl.ds(base, 128)]))
+            for src, back in zip(rings[side], (0, 3, 1, 2)):
+                quarter = lax.rem(sc[side] + back, 4)
+                row = pl.multiple_of(base + quarter * 32, 32)
+                for d in range(3):
+                    pairs.append(
+                        (
+                            src.at[pl.ds(d * 64 + branch * 32, 32)],
+                            w.at[pl.ds((1 + d) * 256 + row, 32)],
+                        )
+                    )
+        groups.append(
+            [
+                pltpu.make_async_copy(a, b, sems.at[branch * 26 + n])
+                for n, (a, b) in enumerate(pairs)
+            ]
+        )
+    start(groups[0])
+    start(groups[1])
+    wait(groups[0])
+
+    def write(i, cols, a):
+        acc[:, cols] = a
+
+    branch_product(parts, logits, 0, w0, write)
+    wait(groups[1])
+
+
+def finish0(sc, owns, ring, ring_other, parts, logits):
+    width = owns[0].shape[1]
+    return plain_call(
+        finish0_kernel, (sc, *owns, *ring, *ring_other, *parts, logits),
+        [SM] + [HBM] * 12 + [VM] * 5,
+        [((SEQ_LEN, width), F32), ((1024, width), BF)], [VM, VM],
+        [pltpu.VMEM((1024, width), BF), pltpu.SemaphoreType.DMA((52,))], FINISH_VMEM,
+    )
+
+
+def finish1_kernel(*refs):
+    parts, logits, acc, w1 = refs[0:4], refs[4], refs[5], refs[6]
+    out, rows, sems = refs[7:]
+
+    def chunk(i):
+        cols = pl.ds(pl.multiple_of(i * 512, 512), 512)
+        return pltpu.make_async_copy(rows.at[:, cols], out.at[:, cols], sems.at[i])
+
+    def write(i, cols, a):
+        rows[:, cols] = (acc[:, cols] + a).astype(BF)
+        chunk(i).start()
+
+    branch_product(parts, logits, 1, w1, write)
+    for i in range(rows.shape[1] // 512):
+        chunk(i).wait()
+
+
+def finish1(parts, logits, acc, w1):
+    width = w1.shape[1]
+    return plain_call(
+        finish1_kernel, (*parts, logits, acc, w1), [VM] * 7,
+        [((SEQ_LEN, width), BF)], [HBM],
+        [pltpu.VMEM((SEQ_LEN, width), BF), pltpu.SemaphoreType.DMA((width // 512,))], FINISH_VMEM,
     )[0]
 
 
@@ -433,7 +468,7 @@
     h1 = swap(other)
     far_part = shift(part, 2)
     a1, b1 = shift(h1, 1), shift(h1, -1)
-    c0, c1 = shift(a0, 1), shift(b1, -1)
+    c0, c1 = shift(a0[: N_Y * SEQ_LEN], 1), shift(b1, -1)
     pieces = (slab, h1, a0, b0, a1, b1, c0, c1)
 
     e = pack(sc_quarter, (a0, b0, far_part))
@@ -475,12 +510,11 @@
 
     q, *convs, logits = project(sc_project, pieces, weights, gate, conv_taps, taps_part)
     conv_all = [convs[3], shift(convs[1], 1), shift(convs[2], -1), shift(convs[0], 2)]
-    half = finish(0, sc_quarter, [conv_out] + ring, [conv_out_other] + ring_other, conv_all, logits)
+    owns = (conv_out, conv_out_other, memory_out, memory_out_other)
+    acc, w1 = finish0(sc_quarter, owns, ring, ring_other, conv_all, logits)
     mems = attend(sc_attend, q, tab_m, tab_o)
     mem_all = [mems[3], shift(mems[1], 1), shift(mems[2], -1), shift(mems[0], 2)]
-    return finish(
-        1, sc_quarter, [memory_out] + ring, [memory_out_other] + ring_other, mem_all, logits, half
-    )
+    return finish1(mem_all, logits, acc, w1)
 
 
 def solution(mesh):

time: 153 us -> 145 us (0.948)
  waiting for transfers between devices: 46.8 us -> 43.4 us
  starting transfers between devices: 45.4 us -> 42.3 us
  Pallas kernels: 38.7 us -> 35.8 us
    pallas_call x7 -> x5, Pallas kernels: 38.7 us -> 28 us  [call(): pl.pallas_call(body, grid_spec=pltpu.PrefetchScalarGridSpec(num_scalar_pr...]
    ppermute x13, waiting for transfers between devices: 39.3 us -> 30.6 us  [shift(): return lax.ppermute(a, 'tp', SHIFT[s])]
    pallas_call x0 -> x2, Pallas kernels: none -> 7.81 us  [plain_call(): pl.pallas_call(body, in_specs=in_specs, out_specs=out_specs, out_shape=[j...]
    ppermute x3, waiting for transfers between devices: 0.01 us -> 6.89 us  [plane(): return lax.ppermute(a, ('st', 'tp'), plane_shift(s))]
    ppermute x13, starting transfers between devices: 17 us -> 14.4 us  [swap(): return lax.ppermute(a, 'tp', SWAP)]
    all_to_all x1, waiting for transfers between devices: 5.9 us -> 4.22 us  [local(): served = lax.all_to_all(chosen, 'st', split_axis=0, concat_axis=0)]
    unnamed x40 -> x48, local copies, waits for them, and re-layouts: 4.38 us -> 4.31 us
  transfers between devices with their start and end apart: 30 -> 30, of which waited for: 12 -> 10; matrix products, arithmetic and copies ran while one was open for 1% -> 1% of each run, Pallas kernels for 16% -> 17%
where the time goes in v4:
time: 145 us; the launch traced here: 143 us
  waiting for transfers between devices  43.4 us (30%)
  starting transfers between devices  42.3 us (29%)
  Pallas kernels  35.8 us (25%)
  blocking collectives  14.6 us (10%)
  local copies, waits for them, and re-layouts  5.68 us (4%)
    ppermute x13, waiting for transfers between devices, shift(): return lax.ppermute(a, 'tp', SHIFT[s])  30.6 us
    pallas_call x5, Pallas kernels, call(): pl.pallas_call(body, grid_spec=pltpu.PrefetchScalarGridSpec(num_scalar_pr...  28 us
    ppermute x13, starting transfers between devices, shift(): return lax.ppermute(a, 'tp', SHIFT[s])  17.6 us
    all_to_all x1, blocking collectives, local(): wanted = lax.all_to_all(outgoing, 'st', split_axis=0, concat_axis=0)  14.6 us
    ppermute x13, starting transfers between devices, swap(): return lax.ppermute(a, 'tp', SWAP)  14.4 us
    pallas_call x2, Pallas kernels, plain_call(): pl.pallas_call(body, in_specs=in_specs, out_specs=out_specs, out_shape=[j...  7.81 us
    ppermute x3, waiting for transfers between devices, plane(): return lax.ppermute(a, ('st', 'tp'), plane_shift(s))  6.89 us
    ppermute x3, starting transfers between devices, plane(): return lax.ppermute(a, ('st', 'tp'), plane_shift(s))  5.83 us
  transfers between devices with their start and end apart: 30, of which 10 were waited for; matrix products, arithmetic and copies ran while one was open for 1% of the time, Pallas kernels for 17%

profile of v4, /device:TPU:1, one launch (start us, length us, event | category | flops | bytes accessed | tf_op | source)
XLA Modules:
  0.0 143.4 jit_solution(4037225621810911921)
XLA Ops:
  0.0 0.8 copy.32
  1.2 0.8 copy.33
  2.2 14.6 %all_to_all.16 = s32[16,1,4]{2,1,0:T(1,128)} all-to-all(s32[16,1,4]{2,1,0:T(1,128)S(1)} %bitcast.22), channel_id=1, replica_groups=mesh['st'=16,'tp'=8] {'st'}, dimensions={0} | all-to-all | bytes 512 | tf_op jit(solution)/shard_map/all_to_all | solution.py:490
  16.8 8.6 %shard_map.138 = bf16[16,4,64,256]{3,2,1,0:T(8,128)(2,1)} custom-call(s32[16,4]{1,0:T(8,128)} %bitcast.21, bf16[2048,2048]{1,0:T(8,128)(2,1)} %bitcast.20, bf16[2048,128]{1,0:T(8,128)(2,1)} %kw.1, bf16[2048,128]{1,0:T(8,128)(2,1)} %vw.1), custom_call_target="tpu_custom_call" | custom-call | flops 2147483648 | bytes 11534336 | tf_op jit(solution)/shard_map/pallas_call | solution.py:60
  25.4 4.4 %all-to-all-start.1 = ((bf16[16,4,64,256]{3,2,1,0:T(8,128)(2,1)}), bf16[16,4,64,256]{3,2,1,0:T(8,128)(2,1)}, u32[]{:S(2)}, u32[]{:S(2)}) async-start(bf16[16,4,64,256]{3,2,1,0:T(8,128)(2,1)} %shard_map.138), calls=%async_computation.1 | async-start | bytes 4194304 | tf_op jit(solution)/shard_map/all_to_all | solution.py:500
  30.0 0.7 pad_add_fusion.sc
  30.6 3.4 %shard_map.136 = (bf16[1536,256]{1,0:T(8,128)(2,1)}, bf16[1024,256]{1,0:T(8,128)(2,1)}, bf16[512,256]{1,0:T(8,128)(2,1)}) custom-call(s32[3]{0:T(128)} %pad_add_fusion.sc, bf16[2048,256]{1,0:T(8,128)(2,1)} %tokens.1, bf16[128,2048]{1,0:T(8,128)(2,1)} %refs_0_.1, bf16[128,2048]{1,0:T(8,128)(2,1)} %refs_2_.1), custom_call_target="tpu_custom_call" | custom-call | flops 100000000 | bytes 3145728 | tf_op jit(solution)/shard_map/pallas_call | solution.py:60
  34.0 2.3 %collective-permute-start = (bf16[1024,256]{1,0:T(8,128)(2,1)}, bf16[1024,256]{1,0:T(8,128)(2,1)S(1)}, u32[]{:S(2)}, u32[]{:S(2)}) collective-permute-start(bf16[1024,256]{1,0:T(8,128)(2,1)} %get-tuple-element.21), channel_id=1, source_target_pairs={{0,1},{1,0},{2,3},{3,2},{4,5},{5,4},{6,7},{7,6},{8,9},{9,8},{10,11... | collective-permute-start | bytes 1572872 | tf_op jit(solution)/shard_map/ppermute | solution.py:44
  36.5 0.4 collective-permute-start.8
  36.9 2.9 %collective-permute-start.18 = (bf16[512,256]{1,0:T(8,128)(2,1)}, bf16[512,256]{1,0:T(8,128)(2,1)S(1)}, u32[]{:S(2)}, u32[]{:S(2)}) collective-permute-start(bf16[512,256]{1,0:T(8,128)(2,1)} %get-tuple-element.28), channel_id=1, source_target_pairs={{0,4},{1,5},{2,6},{3,7},{4,0},{5,1},{6,2},{7,3},{8,12},{9,13},{10,... | collective-permute-start | bytes 786440 | tf_op jit(solution)/shard_map/ppermute | solution.py:40
  40.2 0.8 collective-permute-done.11.refs_18_
  41.0 0.4 collective-permute-start.1
  41.4 5.1 %collective-permute-done.18.c = bf16[512,256]{1,0:T(8,128)(2,1)S(1)} collective-permute-done((bf16[512,256]{1,0:T(8,128)(2,1)}, bf16[512,256]{1,0:T(8,128)(2,1)S(1)}, u32[]{:S(2)}, u32[]{:S(2)}) %collective-permute-start.18) | collective-permute-done | bytes 262176 | tf_op jit(solution)/shard_map/ppermute | solution.py:40
  46.5 2.7 %collective-permute-start.2 = (bf16[1536,256]{1,0:T(8,128)(2,1)}, bf16[1536,256]{1,0:T(8,128)(2,1)S(1)}, u32[]{:S(2)}, u32[]{:S(2)}) collective-permute-start(bf16[1536,256]{1,0:T(8,128)(2,1)} %get-tuple-element.20.refs_0_), channel_id=1, source_target_pairs={{0,6},{1,7},{2,0},{3,1},{4,2},{5,3},{6,4},{7,5},{8,14},{9,15},{10,... | collective-permute-start | bytes 2359304 | tf_op jit(solution)/shard_map/ppermute | solution.py:40
  49.2 1.1 collective-permute-start.9
  50.5 0.8 collective-permute-start.16
  51.3 0.9 collective-permute-done.9.refs_14_
  52.2 4.2 %all-to-all-done.1 = bf16[16,4,64,256]{3,2,1,0:T(8,128)(2,1)} async-done(((bf16[16,4,64,256]{3,2,1,0:T(8,128)(2,1)}), bf16[16,4,64,256]{3,2,1,0:T(8,128)(2,1)}, u32[]{:S(2)}, u32[]{:S(2)}) %all-to-all-start.1) | async-done | bytes 2097184 | tf_op jit(solution)/shard_map/all_to_all | solution.py:500
  56.4 5.0 %collective-permute-start.12 = (bf16[64,64,256]{2,1,0:T(8,128)(2,1)}, bf16[64,64,256]{2,1,0:T(8,128)(2,1)}, u32[]{:S(2)}, u32[]{:S(2)}) collective-permute-start(bf16[64,64,256]{2,1,0:T(8,128)(2,1)} %bitcast.19.tab_m), channel_id=1, source_target_pairs={{0,1},{1,0},{2,3},{3,2},{4,5},{5,4},{6,7},{7,6},{8,9},{9,8},{10,11... | collective-permute-start | bytes 6291464 | tf_op jit(solution)/shard_map/ppermute | solution.py:44
  61.4 2.3 %collective-permute-done.1.refs_2_.a = bf16[1536,256]{1,0:T(8,128)(2,1)S(1)} collective-permute-done((bf16[1536,256]{1,0:T(8,128)(2,1)}, bf16[1536,256]{1,0:T(8,128)(2,1)S(1)}, u32[]{:S(2)}, u32[]{:S(2)}) %collective-permute-start.1) | collective-permute-done | bytes 786464 | tf_op jit(solution)/shard_map/ppermute | solution.py:40
  63.7 0.4 collective-permute-start.4
  64.2 0.7 collective-permute-start.17
  64.9 1.2 collective-permute-start.3
  66.1 1.5 %collective-permute-start.5 = (bf16[1024,256]{1,0:T(8,128)(2,1)S(1)}, bf16[1024,256]{1,0:T(8,128)(2,1)S(1)}, u32[]{:S(2)}, u32[]{:S(2)}) collective-permute-start(bf16[1024,256]{1,0:T(8,128)(2,1)S(1)} %slice.4), channel_id=1, source_target_pairs={{0,2},{1,3},{2,4},{3,5},{4,6},{5,7},{6,0},{7,1},{8,10},{9,11},{10,... | collective-permute-start | bytes 1572872 | tf_op jit(solution)/shard_map/ppermute | solution.py:40
  67.5 9.4 %collective-permute-done.4.refs_5_ = bf16[1024,256]{1,0:T(8,128)(2,1)S(1)} collective-permute-done((bf16[1024,256]{1,0:T(8,128)(2,1)}, bf16[1024,256]{1,0:T(8,128)(2,1)S(1)}, u32[]{:S(2)}, u32[]{:S(2)}) %collective-permute-start.4) | collective-permute-done | bytes 524320 | tf_op jit(solution)/shard_map/ppermute | solution.py:40
  76.9 3.2 %collective-permute-start.6 = (bf16[1024,256]{1,0:T(8,128)(2,1)S(1)}, bf16[1024,256]{1,0:T(8,128)(2,1)S(1)}, u32[]{:S(2)}, u32[]{:S(2)}) collective-permute-start(bf16[1024,256]{1,0:T(8,128)(2,1)S(1)} %collective-permute-done.4.refs_5_), channel_id=1, source_target_pairs={{0,6},{1,7},{2,0},{3,1},{4,2},{5,3},{6,4},{7,5},{8,14},{9,15},{10,... | collective-permute-start | bytes 1572872 | tf_op jit(solution)/shard_map/ppermute | solution.py:40
  80.1 0.6 shard_map.140.refs_4_
  80.7 0.8 copy-done.8
  81.6 1.3 collective-permute-start.19
  82.8 1.5 %collective-permute-start.20 = (bf16[192,2048]{1,0:T(8,128)(2,1)S(1)}, bf16[192,2048]{1,0:T(8,128)(2,1)}, u32[]{:S(2)}, u32[]{:S(2)}) collective-permute-start(bf16[192,2048]{1,0:T(8,128)(2,1)S(1)} %shard_map.140.refs_4_), channel_id=1, source_target_pairs={{0,24},{1,97},{2,26},{3,99},{4,28},{5,101},{6,30},{7,103},{8,0},{9... | collective-permute-start | bytes 2359304 | tf_op jit(solution)/shard_map/ppermute | solution.py:48
  84.4 7.1 %collective-permute-done.5.refs_6_ = bf16[1024,256]{1,0:T(8,128)(2,1)S(1)} collective-permute-done((bf16[1024,256]{1,0:T(8,128)(2,1)S(1)}, bf16[1024,256]{1,0:T(8,128)(2,1)S(1)}, u32[]{:S(2)}, u32[]{:S(2)}) %collective-permute-start.5) | collective-permute-done | bytes 524320 | tf_op jit(solution)/shard_map/ppermute | solution.py:40
  91.5 3.0 %collective-permute-start.21 = (bf16[192,2048]{1,0:T(8,128)(2,1)S(1)}, bf16[192,2048]{1,0:T(8,128)(2,1)}, u32[]{:S(2)}, u32[]{:S(2)}) collective-permute-start(bf16[192,2048]{1,0:T(8,128)(2,1)S(1)} %shard_map.140.refs_4_), channel_id=1, source_target_pairs={{0,16},{1,65},{2,18},{3,67},{4,20},{5,69},{6,22},{7,71},{8,24},{9,... | collective-permute-start | bytes 2359304 | tf_op jit(solution)/shard_map/ppermute | solution.py:48
  94.5 0.8 copy-done.20
  95.4 0.9 collective-permute-start.22
  96.2 0.7 stack.67.sc
  96.9 0.5 collective-permute-start.24
  97.4 6.9 %collective-permute-done.21.refs_7_ = bf16[192,2048]{1,0:T(8,128)(2,1)} collective-permute-done((bf16[192,2048]{1,0:T(8,128)(2,1)S(1)}, bf16[192,2048]{1,0:T(8,128)(2,1)}, u32[]{:S(2)}, u32[]{:S(2)}) %collective-permute-start.21) | collective-permute-done | bytes 786464 | tf_op jit(solution)/shard_map/ppermute | solution.py:48
  104.3 2.2 %collective-permute-start.25 = (bf16[192,2048]{1,0:T(8,128)(2,1)}, bf16[192,2048]{1,0:T(8,128)(2,1)}, u32[]{:S(2)}, u32[]{:S(2)}) collective-permute-start(bf16[192,2048]{1,0:T(8,128)(2,1)} %collective-permute-done.21.refs_7_), channel_id=1, source_target_pairs={{0,1},{1,0},{2,3},{3,2},{4,5},{5,4},{6,7},{7,6},{8,9},{9,8},{10,11... | collective-permute-start | bytes 2359304 | tf_op jit(solution)/shard_map/ppermute | solution.py:44
  106.5 12.1 %shard_map.137 = (bf16[1024,256]{1,0:T(8,128)(2,1)}, bf16[256,256]{1,0:T(8,128)(2,1)}, bf16[256,256]{1,0:T(8,128)(2,1)}, bf16[256,256]{1,0:T(8,128)(2,1)}, bf16[256,256]{1,0:T(8,128)(2,1)}, /*index=5*/f32[256,2]{1,0:T(8,128)}) custom-call(s32[12]{0:T(128)} %stack.67.sc, bf16[1536,256]{1,0:T(8,128)(2,1)} %get-tuple-element.20.refs_0_, ...), custom_call_target="tpu_custom_call" | custom-call | flops 4294967296 | bytes 10485760 | tf_op jit(solution)/shard_map/pallas_call | solution.py:60
  118.7 6.4 %collective-permute-done.26.refs_13_ = bf16[256,256]{1,0:T(8,128)(2,1)S(1)} collective-permute-done((bf16[256,256]{1,0:T(8,128)(2,1)}, bf16[256,256]{1,0:T(8,128)(2,1)S(1)}, u32[]{:S(2)}, u32[]{:S(2)}) %collective-permute-start.26) | collective-permute-done | bytes 131104 | tf_op jit(solution)/shard_map/ppermute | solution.py:40
  125.2 0.9 collective-permute-start.28
  126.5 1.0 copy-done.10
  127.6 3.2 %shard_map.139 = (bf16[256,256]{1,0:T(8,128)(2,1)S(1)}, bf16[256,256]{1,0:T(8,128)(2,1)S(1)}, bf16[256,256]{1,0:T(8,128)(2,1)S(1)}, bf16[256,256]{1,0:T(8,128)(2,1)S(1)}) custom-call(s32[20]{0:T(128)S(1)} %concatenate.3.sc, bf16[1024,256]{1,0:T(8,128)(2,1)S(1)} %copy-done.10, bf16[64,64,256]{2,1,0:T(8,128)(2,1)} %bitcast.19.tab_m, ...), custom_call_target="tpu_custom_call" | custom-call | flops 1000000000 | bytes 5242880 | tf_op jit(solution)/shard_map/pallas_call | solution.py:60
  130.8 0.7 collective-permute-start.13
  131.5 3.3 %collective-permute-start.14 = (bf16[256,256]{1,0:T(8,128)(2,1)S(1)}, bf16[256,256]{1,0:T(8,128)(2,1)S(1)}, u32[]{:S(2)}, u32[]{:S(2)}) collective-permute-start(bf16[256,256]{1,0:T(8,128)(2,1)S(1)} %get-tuple-element.25), channel_id=1, source_target_pairs={{0,6},{1,7},{2,0},{3,1},{4,2},{5,3},{6,4},{7,5},{8,14},{9,15},{10,... | collective-permute-start | bytes 393224 | tf_op jit(solution)/shard_map/ppermute | solution.py:40
  134.7 0.4 collective-permute-start.15
  135.2 5.2 %shard_map.141 = (f32[256,2048]{1,0:T(8,128)S(1)}, bf16[1024,2048]{1,0:T(8,128)(2,1)S(1)}) custom-call(s32[3]{0:T(128)S(1)} %copy-done.12, bf16[128,2048]{1,0:T(8,128)(2,1)S(1)} %copy-done.2, bf16[128,2048]{1,0:T(8,128)(2,1)S(1)} %copy-done.7, bf16[128,2048]{1,0:T(8,128)(2,1)S(1)} %copy-done.3, bf16[128,2048]{1,0:T(8,128)(2,1)S(1)} %copy-done.9, ...), custom_call_target="tpu_custom_call" | custom-call | flops 1073741824 | bytes 7340032 | tf_op jit(solution)/shard_map/pallas_call | solution.py:340
  140.7 2.6 %shard_map.142 = bf16[256,2048]{1,0:T(8,128)(2,1)} custom-call(bf16[256,256]{1,0:T(8,128)(2,1)S(1)} %get-tuple-element.23.refs_0_, bf16[256,256]{1,0:T(8,128)(2,1)S(1)} %collective-permute-done.13.refs_1_, bf16[256,256]{1,0:T(8,128)(2,1)S(1)} %collective-permute-done.14.refs_2_, bf16[256,256]{1,0:T(8,128)(2,1)S(1)} %collective-permute-done.15.refs_3_, ...), custom_call_target="tpu_custom_call" | custom-call | flops 1073741824 | bytes 7340032 | tf_op jit(solution)/shard_map/pallas_call | solution.py:340
  (86 shorter events, 2.2 us)
Async XLA Ops:
  25.4 31.0 %all-to-all-start.1 = ((bf16[16,4,64,256]{3,2,1,0:T(8,128)(2,1)}), bf16[16,4,64,256]{3,2,1,0:T(8,128)(2,1)}, u32[]{:S(2)}, u32[]{:S(2)}) async-start(bf16[16,4,64,256]{3,2,1,0:T(8,128)(2,1)} %shard_map.138), calls=%async_computation.1 | async-start | bytes 4194304 | tf_op jit(solution)/shard_map/all_to_all | solution.py:500
  29.9 9.9 %copy-start.21 = (bf16[3,128]{1,0:T(4,128)(2,1)S(1)}, bf16[3,128]{1,0:T(4,128)(2,1)}, u32[]{:S(2)}) copy-start(bf16[3,128]{1,0:T(4,128)(2,1)} %refs_17_.1) | copy-start | bytes 2308
  29.9 20.5 %copy-start.1 = (bf16[128,2048]{1,0:T(8,128)(2,1)S(1)}, bf16[128,2048]{1,0:T(8,128)(2,1)}, u32[]{:S(2)}) copy-start(bf16[128,2048]{1,0:T(8,128)(2,1)} %refs_0_.1) | copy-start | bytes 1572868
  30.6 49.5 %copy-start.12 = (s32[3]{0:T(128)S(1)}, s32[3]{0:T(128)}, u32[]{:S(2)}) copy-start(s32[3]{0:T(128)} %pad_add_fusion.sc) | copy-start | bytes 40
  34.0 15.2 %collective-permute-start = (bf16[1024,256]{1,0:T(8,128)(2,1)}, bf16[1024,256]{1,0:T(8,128)(2,1)S(1)}, u32[]{:S(2)}, u32[]{:S(2)}) collective-permute-start(bf16[1024,256]{1,0:T(8,128)(2,1)} %get-tuple-element.21), channel_id=1, source_target_pairs={{0,1},{1,0},{2,3},{3,2},{4,5},{5,4},{6,7},{7,6},{8,9},{9,8},{10,11... | collective-permute-start | bytes 1572872 | tf_op jit(solution)/shard_map/ppermute | solution.py:44
  36.4 14.0 %collective-permute-start.7 = (bf16[2048,128]{1,0:T(8,128)(2,1)}, bf16[2048,128]{1,0:T(8,128)(2,1)S(1)}, u32[]{:S(2)}, u32[]{:S(2)}) collective-permute-start(bf16[2048,128]{1,0:T(8,128)(2,1)} %refs_8_.1), channel_id=1, source_target_pairs={{0,1},{1,0},{2,3},{3,2},{4,5},{5,4},{6,7},{7,6},{8,9},{9,8},{10,11... | collective-permute-start | bytes 1572872 | tf_op jit(solution)/shard_map/ppermute | solution.py:44
  36.5 14.0 %collective-permute-start.8 = (bf16[2048,128]{1,0:T(8,128)(2,1)}, bf16[2048,128]{1,0:T(8,128)(2,1)S(1)}, u32[]{:S(2)}, u32[]{:S(2)}) collective-permute-start(bf16[2048,128]{1,0:T(8,128)(2,1)} %refs_9_.1), channel_id=1, source_target_pairs={{0,1},{1,0},{2,3},{3,2},{4,5},{5,4},{6,7},{7,6},{8,9},{9,8},{10,11... | collective-permute-start | bytes 1572872 | tf_op jit(solution)/shard_map/ppermute | solution.py:44
  36.9 9.6 %collective-permute-start.18 = (bf16[512,256]{1,0:T(8,128)(2,1)}, bf16[512,256]{1,0:T(8,128)(2,1)S(1)}, u32[]{:S(2)}, u32[]{:S(2)}) collective-permute-start(bf16[512,256]{1,0:T(8,128)(2,1)} %get-tuple-element.28), channel_id=1, source_target_pairs={{0,4},{1,5},{2,6},{3,7},{4,0},{5,1},{6,2},{7,3},{8,12},{9,13},{10,... | collective-permute-start | bytes 786440 | tf_op jit(solution)/shard_map/ppermute | solution.py:40
  39.8 1.2 collective-permute-start.11
  41.0 65.5 %copy-start.22 = (bf16[3,128]{1,0:T(4,128)(2,1)}, bf16[3,128]{1,0:T(4,128)(2,1)S(1)}, u32[]{:S(2)}) copy-start(bf16[3,128]{1,0:T(4,128)(2,1)S(1)} %collective-permute-done.11.refs_18_) | copy-start | bytes 2308
  41.0 22.7 %collective-permute-start.1 = (bf16[1536,256]{1,0:T(8,128)(2,1)}, bf16[1536,256]{1,0:T(8,128)(2,1)S(1)}, u32[]{:S(2)}, u32[]{:S(2)}) collective-permute-start(bf16[1536,256]{1,0:T(8,128)(2,1)} %get-tuple-element.20.refs_0_), channel_id=1, source_target_pairs={{0,2},{1,3},{2,4},{3,5},{4,6},{5,7},{6,0},{7,1},{8,10},{9,11},{10,... | collective-permute-start | bytes 2359304 | tf_op jit(solution)/shard_map/ppermute | solution.py:40
  46.5 19.6 %collective-permute-start.2 = (bf16[1536,256]{1,0:T(8,128)(2,1)}, bf16[1536,256]{1,0:T(8,128)(2,1)S(1)}, u32[]{:S(2)}, u32[]{:S(2)}) collective-permute-start(bf16[1536,256]{1,0:T(8,128)(2,1)} %get-tuple-element.20.refs_0_), channel_id=1, source_target_pairs={{0,6},{1,7},{2,0},{3,1},{4,2},{5,3},{6,4},{7,5},{8,14},{9,15},{10,... | collective-permute-start | bytes 2359304 | tf_op jit(solution)/shard_map/ppermute | solution.py:40
  49.2 1.2 copy-start.14
  49.2 3.0 %collective-permute-start.9 = (bf16[2048,128]{1,0:T(8,128)(2,1)}, bf16[2048,128]{1,0:T(8,128)(2,1)}, u32[]{:S(2)}, u32[]{:S(2)}) collective-permute-start(bf16[2048,128]{1,0:T(8,128)(2,1)} %refs_10_.1), channel_id=1, source_target_pairs={{0,1},{1,0},{2,3},{3,2},{4,5},{5,4},{6,7},{7,6},{8,9},{9,8},{10,11... | collective-permute-start | bytes 1572872 | tf_op jit(solution)/shard_map/ppermute | solution.py:44
  50.3 13.8 %collective-permute-start.10 = (bf16[2048,128]{1,0:T(8,128)(2,1)}, bf16[2048,128]{1,0:T(8,128)(2,1)}, u32[]{:S(2)}, u32[]{:S(2)}) collective-permute-start(bf16[2048,128]{1,0:T(8,128)(2,1)} %refs_11_.1), channel_id=1, source_target_pairs={{0,1},{1,0},{2,3},{3,2},{4,5},{5,4},{6,7},{7,6},{8,9},{9,8},{10,11... | collective-permute-start | bytes 1572872 | tf_op jit(solution)/shard_map/ppermute | solution.py:44
  50.5 14.4 %collective-permute-start.16 = (bf16[128,2048]{1,0:T(8,128)(2,1)S(1)}, bf16[128,2048]{1,0:T(8,128)(2,1)S(1)}, u32[]{:S(2)}, u32[]{:S(2)}) collective-permute-start(bf16[128,2048]{1,0:T(8,128)(2,1)S(1)} %copy-done.1), channel_id=1, source_target_pairs={{0,1},{1,0},{2,3},{3,2},{4,5},{5,4},{6,7},{7,6},{8,9},{9,8},{10,11... | collective-permute-start | bytes 1572872 | tf_op jit(solution)/shard_map/ppermute | solution.py:44
  56.4 68.7 %collective-permute-start.12 = (bf16[64,64,256]{2,1,0:T(8,128)(2,1)}, bf16[64,64,256]{2,1,0:T(8,128)(2,1)}, u32[]{:S(2)}, u32[]{:S(2)}) collective-permute-start(bf16[64,64,256]{2,1,0:T(8,128)(2,1)} %bitcast.19.tab_m), channel_id=1, source_target_pairs={{0,1},{1,0},{2,3},{3,2},{4,5},{5,4},{6,7},{7,6},{8,9},{9,8},{10,11... | collective-permute-start | bytes 6291464 | tf_op jit(solution)/shard_map/ppermute | solution.py:44
  63.7 42.8 %copy-start = (bf16[1536,256]{1,0:T(8,128)(2,1)}, bf16[1536,256]{1,0:T(8,128)(2,1)S(1)}, u32[]{:S(2)}) copy-start(bf16[1536,256]{1,0:T(8,128)(2,1)S(1)} %collective-permute-done.1.refs_2_.a) | copy-start | bytes 2359300
  63.7 13.2 %collective-permute-start.4 = (bf16[1024,256]{1,0:T(8,128)(2,1)}, bf16[1024,256]{1,0:T(8,128)(2,1)S(1)}, u32[]{:S(2)}, u32[]{:S(2)}) collective-permute-start(bf16[1024,256]{1,0:T(8,128)(2,1)} %copy-done.14), channel_id=1, source_target_pairs={{0,6},{1,7},{2,0},{3,1},{4,2},{5,3},{6,4},{7,5},{8,14},{9,15},{10,... | collective-permute-start | bytes 1572872 | tf_op jit(solution)/shard_map/ppermute | solution.py:40
  64.2 16.5 %collective-permute-start.17 = (bf16[128,2048]{1,0:T(8,128)(2,1)}, bf16[128,2048]{1,0:T(8,128)(2,1)S(1)}, u32[]{:S(2)}, u32[]{:S(2)}) collective-permute-start(bf16[128,2048]{1,0:T(8,128)(2,1)} %refs_2_.1), channel_id=1, source_target_pairs={{0,1},{1,0},{2,3},{3,2},{4,5},{5,4},{6,7},{7,6},{8,9},{9,8},{10,11... | collective-permute-start | bytes 1572872 | tf_op jit(solution)/shard_map/ppermute | solution.py:44
  64.9 41.6 %copy-start.6 = (bf16[128,2048]{1,0:T(8,128)(2,1)}, bf16[128,2048]{1,0:T(8,128)(2,1)S(1)}, u32[]{:S(2)}) copy-start(bf16[128,2048]{1,0:T(8,128)(2,1)S(1)} %collective-permute-done.16.refs_1_) | copy-start | bytes 1572868
  64.9 18.0 %collective-permute-start.3 = (bf16[1024,256]{1,0:T(8,128)(2,1)}, bf16[1024,256]{1,0:T(8,128)(2,1)S(1)}, u32[]{:S(2)}, u32[]{:S(2)}) collective-permute-start(bf16[1024,256]{1,0:T(8,128)(2,1)} %copy-done.14), channel_id=1, source_target_pairs={{0,2},{1,3},{2,4},{3,5},{4,6},{5,7},{6,0},{7,1},{8,10},{9,11},{10,... | collective-permute-start | bytes 1572872 | tf_op jit(solution)/shard_map/ppermute | solution.py:40
  66.1 38.2 %copy-start.4 = (bf16[1536,256]{1,0:T(8,128)(2,1)}, bf16[1536,256]{1,0:T(8,128)(2,1)S(1)}, u32[]{:S(2)}) copy-start(bf16[1536,256]{1,0:T(8,128)(2,1)S(1)} %collective-permute-done.2.refs_3_.b) | copy-start | bytes 2359300
  66.1 25.4 %collective-permute-start.5 = (bf16[1024,256]{1,0:T(8,128)(2,1)S(1)}, bf16[1024,256]{1,0:T(8,128)(2,1)S(1)}, u32[]{:S(2)}, u32[]{:S(2)}) collective-permute-start(bf16[1024,256]{1,0:T(8,128)(2,1)S(1)} %slice.4), channel_id=1, source_target_pairs={{0,2},{1,3},{2,4},{3,5},{4,6},{5,7},{6,0},{7,1},{8,10},{9,11},{10,... | collective-permute-start | bytes 1572872 | tf_op jit(solution)/shard_map/ppermute | solution.py:40
  76.9 17.6 %copy-start.17 = (bf16[1024,256]{1,0:T(8,128)(2,1)}, bf16[1024,256]{1,0:T(8,128)(2,1)S(1)}, u32[]{:S(2)}) copy-start(bf16[1024,256]{1,0:T(8,128)(2,1)S(1)} %collective-permute-done.4.refs_5_) | copy-start | bytes 1572868
  76.9 17.6 %collective-permute-start.6 = (bf16[1024,256]{1,0:T(8,128)(2,1)S(1)}, bf16[1024,256]{1,0:T(8,128)(2,1)S(1)}, u32[]{:S(2)}, u32[]{:S(2)}) collective-permute-start(bf16[1024,256]{1,0:T(8,128)(2,1)S(1)} %collective-permute-done.4.refs_5_), channel_id=1, source_target_pairs={{0,6},{1,7},{2,0},{3,1},{4,2},{5,3},{6,4},{7,5},{8,14},{9,15},{10,... | collective-permute-start | bytes 1572872 | tf_op jit(solution)/shard_map/ppermute | solution.py:40
  81.6 15.3 %collective-permute-start.19 = (bf16[192,2048]{1,0:T(8,128)(2,1)S(1)}, bf16[192,2048]{1,0:T(8,128)(2,1)}, u32[]{:S(2)}, u32[]{:S(2)}) collective-permute-start(bf16[192,2048]{1,0:T(8,128)(2,1)S(1)} %shard_map.140.refs_4_), channel_id=1, source_target_pairs={{0,8},{1,33},{2,10},{3,35},{4,12},{5,37},{6,14},{7,39},{8,16},{9,4... | collective-permute-start | bytes 2359304 | tf_op jit(solution)/shard_map/ppermute | solution.py:48
  82.8 11.7 %copy-start.18 = (bf16[1024,256]{1,0:T(8,128)(2,1)}, bf16[1024,256]{1,0:T(8,128)(2,1)S(1)}, u32[]{:S(2)}) copy-start(bf16[1024,256]{1,0:T(8,128)(2,1)S(1)} %collective-permute-done.3.refs_4_) | copy-start | bytes 1572868
  82.8 14.1 %collective-permute-start.20 = (bf16[192,2048]{1,0:T(8,128)(2,1)S(1)}, bf16[192,2048]{1,0:T(8,128)(2,1)}, u32[]{:S(2)}, u32[]{:S(2)}) collective-permute-start(bf16[192,2048]{1,0:T(8,128)(2,1)S(1)} %shard_map.140.refs_4_), channel_id=1, source_target_pairs={{0,24},{1,97},{2,26},{3,99},{4,28},{5,101},{6,30},{7,103},{8,0},{9... | collective-permute-start | bytes 2359304 | tf_op jit(solution)/shard_map/ppermute | solution.py:48
  91.5 3.0 %copy-start.19 = (bf16[1024,256]{1,0:T(8,128)(2,1)}, bf16[1024,256]{1,0:T(8,128)(2,1)S(1)}, u32[]{:S(2)}) copy-start(bf16[1024,256]{1,0:T(8,128)(2,1)S(1)} %collective-permute-done.5.refs_6_) | copy-start | bytes 1572868
  91.5 12.8 %collective-permute-start.21 = (bf16[192,2048]{1,0:T(8,128)(2,1)S(1)}, bf16[192,2048]{1,0:T(8,128)(2,1)}, u32[]{:S(2)}, u32[]{:S(2)}) collective-permute-start(bf16[192,2048]{1,0:T(8,128)(2,1)S(1)} %shard_map.140.refs_4_), channel_id=1, source_target_pairs={{0,16},{1,65},{2,18},{3,67},{4,20},{5,69},{6,22},{7,71},{8,24},{9,... | collective-permute-start | bytes 2359304 | tf_op jit(solution)/shard_map/ppermute | solution.py:48
  95.4 23.3 %collective-permute-start.22 = (bf16[192,2048]{1,0:T(8,128)(2,1)S(1)}, bf16[192,2048]{1,0:T(8,128)(2,1)}, u32[]{:S(2)}, u32[]{:S(2)}) collective-permute-start(bf16[192,2048]{1,0:T(8,128)(2,1)S(1)} %shard_map.140.refs_4_), channel_id=1, source_target_pairs={{0,1},{1,0},{2,3},{3,2},{4,5},{5,4},{6,7},{7,6},{8,9},{9,8},{10,11... | collective-permute-start | bytes 2359304 | tf_op jit(solution)/shard_map/ppermute | solution.py:44
  96.9 37.9 %collective-permute-start.23 = (bf16[192,2048]{1,0:T(8,128)(2,1)}, bf16[192,2048]{1,0:T(8,128)(2,1)}, u32[]{:S(2)}, u32[]{:S(2)}) collective-permute-start(bf16[192,2048]{1,0:T(8,128)(2,1)} %collective-permute-done.19.refs_5_), channel_id=1, source_target_pairs={{0,1},{1,0},{2,3},{3,2},{4,5},{5,4},{6,7},{7,6},{8,9},{9,8},{10,11... | collective-permute-start | bytes 2359304 | tf_op jit(solution)/shard_map/ppermute | solution.py:44
  96.9 38.2 %collective-permute-start.24 = (bf16[192,2048]{1,0:T(8,128)(2,1)}, bf16[192,2048]{1,0:T(8,128)(2,1)}, u32[]{:S(2)}, u32[]{:S(2)}) collective-permute-start(bf16[192,2048]{1,0:T(8,128)(2,1)} %collective-permute-done.20.refs_6_), channel_id=1, source_target_pairs={{0,1},{1,0},{2,3},{3,2},{4,5},{5,4},{6,7},{7,6},{8,9},{9,8},{10,11... | collective-permute-start | bytes 2359304 | tf_op jit(solution)/shard_map/ppermute | solution.py:44
  104.3 30.8 %collective-permute-start.25 = (bf16[192,2048]{1,0:T(8,128)(2,1)}, bf16[192,2048]{1,0:T(8,128)(2,1)}, u32[]{:S(2)}, u32[]{:S(2)}) collective-permute-start(bf16[192,2048]{1,0:T(8,128)(2,1)} %collective-permute-done.21.refs_7_), channel_id=1, source_target_pairs={{0,1},{1,0},{2,3},{3,2},{4,5},{5,4},{6,7},{7,6},{8,9},{9,8},{10,11... | collective-permute-start | bytes 2359304 | tf_op jit(solution)/shard_map/ppermute | solution.py:44
  106.5 19.6 %copy-start.13 = (s32[16,2]{0,1:T(2,128)S(1)}, s32[16,2]{0,1:T(2,128)}, u32[]{:S(2)}) copy-start(s32[16,2]{0,1:T(2,128)} %param.16) | copy-start | bytes 388
  118.6 6.5 %collective-permute-start.26 = (bf16[256,256]{1,0:T(8,128)(2,1)}, bf16[256,256]{1,0:T(8,128)(2,1)S(1)}, u32[]{:S(2)}, u32[]{:S(2)}) collective-permute-start(bf16[256,256]{1,0:T(8,128)(2,1)} %get-tuple-element.30), channel_id=1, source_target_pairs={{0,2},{1,3},{2,4},{3,5},{4,6},{5,7},{6,0},{7,1},{8,10},{9,11},{10,... | collective-permute-start | bytes 393224 | tf_op jit(solution)/shard_map/ppermute | solution.py:40
  125.2 5.6 %collective-permute-start.27 = (bf16[256,256]{1,0:T(8,128)(2,1)}, bf16[256,256]{1,0:T(8,128)(2,1)S(1)}, u32[]{:S(2)}, u32[]{:S(2)}) collective-permute-start(bf16[256,256]{1,0:T(8,128)(2,1)} %get-tuple-element.31), channel_id=1, source_target_pairs={{0,6},{1,7},{2,0},{3,1},{4,2},{5,3},{6,4},{7,5},{8,14},{9,15},{10,... | collective-permute-start | bytes 393224 | tf_op jit(solution)/shard_map/ppermute | solution.py:40
  125.2 6.3 %collective-permute-start.28 = (bf16[256,256]{1,0:T(8,128)(2,1)}, bf16[256,256]{1,0:T(8,128)(2,1)S(1)}, u32[]{:S(2)}, u32[]{:S(2)}) collective-permute-start(bf16[256,256]{1,0:T(8,128)(2,1)} %get-tuple-element.32), channel_id=1, source_target_pairs={{0,4},{1,5},{2,6},{3,7},{4,0},{5,1},{6,2},{7,3},{8,12},{9,13},{10,... | collective-permute-start | bytes 393224 | tf_op jit(solution)/shard_map/ppermute | solution.py:40
  127.5 7.6 %copy-start.2 = (bf16[128,2048]{1,0:T(8,128)(2,1)S(1)}, bf16[128,2048]{1,0:T(8,128)(2,1)}, u32[]{:S(2)}) copy-start(bf16[128,2048]{1,0:T(8,128)(2,1)} %refs_0_.1) | copy-start | bytes 1572868
  127.5 7.6 %copy-start.3 = (bf16[128,2048]{1,0:T(8,128)(2,1)S(1)}, bf16[128,2048]{1,0:T(8,128)(2,1)}, u32[]{:S(2)}) copy-start(bf16[128,2048]{1,0:T(8,128)(2,1)} %refs_2_.1) | copy-start | bytes 1572868
  127.5 7.6 %copy-start.5 = (f32[256,2]{1,0:T(8,128)S(1)}, f32[256,2]{1,0:T(8,128)}, u32[]{:S(2)}) copy-start(f32[256,2]{1,0:T(8,128)} %get-tuple-element.27.refs_16_.refs_4_) | copy-start | bytes 6148
  127.5 7.6 %copy-start.7 = (bf16[128,2048]{1,0:T(8,128)(2,1)S(1)}, bf16[128,2048]{1,0:T(8,128)(2,1)}, u32[]{:S(2)}) copy-start(bf16[128,2048]{1,0:T(8,128)(2,1)} %copy-done.6) | copy-start | bytes 1572868
  127.5 7.6 %copy-start.9 = (bf16[128,2048]{1,0:T(8,128)(2,1)S(1)}, bf16[128,2048]{1,0:T(8,128)(2,1)}, u32[]{:S(2)}) copy-start(bf16[128,2048]{1,0:T(8,128)(2,1)} %copy-done.8) | copy-start | bytes 1572868
  127.6 7.6 %copy-start.11 = (bf16[256,256]{1,0:T(8,128)(2,1)S(1)}, bf16[256,256]{1,0:T(8,128)(2,1)}, u32[]{:S(2)}) copy-start(bf16[256,256]{1,0:T(8,128)(2,1)} %get-tuple-element.29.refs_12_) | copy-start | bytes 393220
  130.8 9.7 %collective-permute-start.13 = (bf16[256,256]{1,0:T(8,128)(2,1)S(1)}, bf16[256,256]{1,0:T(8,128)(2,1)S(1)}, u32[]{:S(2)}, u32[]{:S(2)}) collective-permute-start(bf16[256,256]{1,0:T(8,128)(2,1)S(1)} %get-tuple-element.24), channel_id=1, source_target_pairs={{0,2},{1,3},{2,4},{3,5},{4,6},{5,7},{6,0},{7,1},{8,10},{9,11},{10,... | collective-permute-start | bytes 393224 | tf_op jit(solution)/shard_map/ppermute | solution.py:40
  131.5 9.0 %collective-permute-start.14 = (bf16[256,256]{1,0:T(8,128)(2,1)S(1)}, bf16[256,256]{1,0:T(8,128)(2,1)S(1)}, u32[]{:S(2)}, u32[]{:S(2)}) collective-permute-start(bf16[256,256]{1,0:T(8,128)(2,1)S(1)} %get-tuple-element.25), channel_id=1, source_target_pairs={{0,6},{1,7},{2,0},{3,1},{4,2},{5,3},{6,4},{7,5},{8,14},{9,15},{10,... | collective-permute-start | bytes 393224 | tf_op jit(solution)/shard_map/ppermute | solution.py:40
  134.7 5.9 %collective-permute-start.15 = (bf16[256,256]{1,0:T(8,128)(2,1)S(1)}, bf16[256,256]{1,0:T(8,128)(2,1)S(1)}, u32[]{:S(2)}, u32[]{:S(2)}) collective-permute-start(bf16[256,256]{1,0:T(8,128)(2,1)S(1)} %get-tuple-element.26), channel_id=1, source_target_pairs={{0,4},{1,5},{2,6},{3,7},{4,0},{5,1},{6,2},{7,3},{8,12},{9,13},{10,... | collective-permute-start | bytes 393224 | tf_op jit(solution)/shard_map/ppermute | solution.py:40
  (5 other events, 4.5 us)
